TPU v7x, 256 devices: a 8x8x2 block of a 8x8x16 slice. The times are simulated.
256 devices in a mesh: grp: 2 (over z), sp: 64 (over y, x), tp: 2 (over core).
Axes of the slice: x: 8, y: 8, z: 2, core: 2. Of those that a mesh axis runs over, the one named last changes fastest.
The devices are a block of a 8x8x16 slice.
Arguments:
- probe_preactivation: bfloat16 [32768, 2048], P(('grp', 'sp'), 'tp'), parts along dimension 0, may hold values from -6 to 6
- retention_preactivation: bfloat16 [32768, 2048], P(('grp', 'sp'), 'tp'), parts along dimension 0, may hold values from -5 to 5.5
- source_entries: bfloat16 [32768, 2048], P(('grp', 'sp'), 'tp'), parts along dimension 0, may hold values from -6 to 6
- extra_log_retention: float32 [32768, 16], P(('grp', 'sp'), 'tp'), parts along dimension 0, may hold values from -1.39 to 0
- retention_slack: float32 [2048], P('tp'), as said below
- group_normalizer_gain: float32 [128], replicated, may hold values from 0.1 to 1.9
- readout_mapping_matrix: bfloat16 [2048, 2048], P('tp'), may hold values from -0.125 to 0.125
Outputs:
- mixed: bfloat16 [32768, 2048], P(('grp', 'sp', 'tp')), parts along dimension 0
There are 2 independent parts, one for each index of `grp`. A program takes and returns all parts, laid end to end along the dimension named above; an argument that names none is the same for every part. Nothing has to cross between parts.
Inputs may be any that keep to these rules, and one draw needn't show every extreme that they name: `retention_slack`: every entry is positive.
All inputs are finite; a program needn't handle non-finite values.
Results may differ from a plain program's by a relative error of at most 0.014.
Values may be sent and summed in bfloat16 or wider, within the bound.
No kernel may reach another device: no remote copies, remote signals or barrier semaphores. Data moves between devices by JAX's collectives and lax.ppermute only.
A program may use at most 128 MiB of HBM per device.

v0:
```python
import jax
import jax.numpy as jnp
from jax import lax
from jax.sharding import Mesh
from jax.sharding import PartitionSpec as P

SPAN = 128
SP = ("sp_0", "sp_1")
GRP_SP = ("grp", "sp_0", "sp_1")
GRP_SP_TP = ("grp", "sp_0", "sp_1", "tp")


def filled_with(x, identity):
    return jax.tree.map(
        lambda a, e: jnp.broadcast_to(jnp.asarray(e, a.dtype), a.shape), x, identity
    )


def entering(x, axes, combine, identity):
    before = start = filled_with(x, identity)
    total = x
    for axis in reversed(axes):
        devices, position = (lax.axis_size(axis), lax.axis_index(axis))
        pieces = jax.tree.map(
            lambda part, kind: lax.all_gather(part.astype(kind), axis),
            total,
            (jnp.bfloat16, jnp.bfloat16),
        )
        inside, total = (start, start)
        for k in range(devices):
            passed = k < position
            total = combine(
                total, jax.tree.map(lambda part, own: part[k].astype(own.dtype), pieces, x)
            )
            inside = jax.tree.map(lambda new, old: jnp.where(passed, new, old), total, inside)
        before = combine(inside, before)
    return before


def in_blocks(x, dim, devices):
    before, after = (x.shape[:dim], x.shape[dim + 1 :])
    return jnp.moveaxis(x.reshape(*before, devices, -1, *after), dim, 0)


def summed_on_arrival(x, axis, dim):
    pieces = in_blocks(x, dim, lax.axis_size(axis))
    arrived = lax.all_to_all(pieces, axis, split_axis=0, concat_axis=0, tiled=True)
    return arrived.astype(jnp.float32).sum(axis=0)


def assemble_arguments(
    probe_preactivation,
    retention_preactivation,
    source_entries,
    extra_log_retention,
    retention_slack,
):
    tokens_here = probe_preactivation.shape[0]
    group_count = extra_log_retention.shape[1]
    head_dim = probe_preactivation.shape[1] // group_count
    probe_matrix = jax.nn.silu(probe_preactivation.astype(jnp.float32)).reshape(
        tokens_here, group_count, head_dim
    )
    scaled_address_matrix = (
        retention_slack * jax.nn.sigmoid(-retention_preactivation.astype(jnp.float32))
    ).reshape(tokens_here, group_count, head_dim)
    log_retention_factor = jnp.log1p(-scaled_address_matrix) + extra_log_retention[:, :, None]
    content_matrix = source_entries.reshape(tokens_here, group_count, head_dim)
    return (probe_matrix, scaled_address_matrix, content_matrix, log_retention_factor)


def advance(carried_state, scaled_address_matrix, content_matrix, running):
    final_running_sum = running[-1]
    passed_state = (scaled_address_matrix * jnp.exp(final_running_sum[None] - running)).astype(
        jnp.bfloat16
    )
    return jnp.exp(final_running_sum)[:, :, None] * carried_state + jnp.einsum(
        "wcf,wcz->cfz", passed_state, content_matrix, preferred_element_type=jnp.float32
    )


def block_pass(carried_state, pieces):
    probe_matrix, scaled_address_matrix, content_matrix, log_retention_factor = pieces
    span_len = probe_matrix.shape[0]
    running = jnp.cumsum(log_retention_factor, axis=0)
    raised_values = (probe_matrix * jnp.exp(running)).astype(jnp.bfloat16)
    lowered = (scaled_address_matrix * jnp.exp(-running)).astype(jnp.bfloat16)
    scores = jnp.einsum("thk,shk->hts", raised_values, lowered, preferred_element_type=jnp.float32)
    row_index = lax.broadcasted_iota(jnp.int32, (span_len, span_len), 0)
    col_index = lax.broadcasted_iota(jnp.int32, (span_len, span_len), 1)
    scores = jnp.where((row_index >= col_index)[None], scores, jnp.zeros_like(scores)).astype(
        jnp.bfloat16
    )
    final_output = jnp.einsum(
        "hts,shv->thv", scores, content_matrix, preferred_element_type=jnp.float32
    )
    final_output = final_output + jnp.einsum(
        "csq,sqd->csd",
        raised_values,
        carried_state.astype(jnp.bfloat16),
        preferred_element_type=jnp.float32,
    )
    carried_state = advance(carried_state, scaled_address_matrix, content_matrix, running)
    return (carried_state, (final_output, running))


def finish(mixer_out, group_normalizer_gain):
    scale = lax.rsqrt(jnp.mean(mixer_out * mixer_out, axis=-1, keepdims=True) + 1e-06)
    normed = (mixer_out * scale * group_normalizer_gain).astype(jnp.bfloat16)
    return normed.reshape(mixer_out.shape[0], mixer_out.shape[1] * mixer_out.shape[2])


def combine(earlier, later):
    return (earlier[0] * later[0], later[0][:, :, None] * earlier[1] + later[1])


def hand_along(totals, local_state):
    neutral = (jnp.ones_like(totals), jnp.zeros_like(local_state))
    return entering((totals, local_state), SP, combine, neutral)[1]


def body(
    probe_preactivation,
    retention_preactivation,
    source_entries,
    extra_log_retention,
    retention_slack,
    group_normalizer_gain,
    readout_mapping_matrix,
):
    probe_matrix, scaled_address_matrix, content_matrix, log_retention_factor = assemble_arguments(
        probe_preactivation,
        retention_preactivation,
        source_entries,
        extra_log_retention,
        retention_slack,
    )
    tokens_here, group_count, head_dim = probe_matrix.shape
    blocks = tokens_here // SPAN
    pieces = tuple(
        (
            a.reshape(blocks, SPAN, group_count, head_dim)
            for a in (probe_matrix, scaled_address_matrix, content_matrix, log_retention_factor)
        )
    )
    empty = jnp.zeros((group_count, head_dim, head_dim), jnp.float32)
    zero_rate = jnp.zeros((group_count, head_dim), jnp.float32)

    def state_step(carry, piece):
        carried_state, offset = carry
        running = jnp.cumsum(piece[3], axis=0)
        carried_state = advance(carried_state, piece[1], piece[2], running)
        return ((carried_state, offset + running[-1]), None)

    (local_state, offset), _ = lax.scan(state_step, (empty, zero_rate), pieces)
    incoming = hand_along(jnp.exp(offset), local_state)
    _, (mixer_out, _) = lax.scan(block_pass, incoming, pieces)
    mixer_out = mixer_out.reshape(tokens_here, group_count, head_dim)
    normed = finish(mixer_out, group_normalizer_gain)
    mixed = summed_on_arrival(
        jnp.dot(normed, readout_mapping_matrix, preferred_element_type=jnp.float32).astype(
            jnp.bfloat16
        ),
        "tp",
        0,
    )
    return mixed.astype(jnp.bfloat16)


def solution(mesh):
    finer = Mesh(
        mesh.devices.reshape(mesh.shape["grp"], 8, 8, mesh.shape["tp"]),
        ("grp", "sp_0", "sp_1", "tp"),
    )
    in_specs = (
        P(GRP_SP, "tp"),
        P(GRP_SP, "tp"),
        P(GRP_SP, "tp"),
        P(GRP_SP, "tp"),
        P("tp"),
        P(),
        P("tp", None),
    )
    out_specs = P(GRP_SP_TP, None)
    return jax.shard_map(body, mesh=finer, in_specs=in_specs, out_specs=out_specs, check_vma=False)
```

profile of v0, /device:TPU:513, one launch (start us, length us, event | category | flops | bytes accessed | tf_op | source)
XLA Modules:
  0.0 155.3 jit_solution(13402946859580898582)
XLA Ops:
  6.5 0.0 copy-start
  6.6 0.0 copy-start.2
  6.6 0.0 all-gather.7.cloned.1.call-start
  6.6 0.9 copy.41
  7.4 1.3 multiply_bitcast_fusion
  8.8 0.2 copy.48
  9.0 0.0 copy-done.2
  9.0 0.1 copy.49
  9.1 0.1 copy.42
  9.2 1.4 log-plus-one_add_fusion
  10.6 3.4 %while.26 = (s32[]{:T(128)}, f32[8,128,128]{2,1,0:T(8,128)S(1)}, f32[8,128]{1,0:T(8,128)S(1)}, f32[2,128,8,128]{3,2,1,0:T(8,128)}, f32[2,128,8,128]{3,2,1,0:T(8,...) while((s32[]{:T(128)}, f32[8,128,128]{2,1,0:T(8,128)S(1)}, ...), condition=%wide.region_2.3_spmd.clone, body=%wide.region_0.2_spmd.clone.sunk | while | flops 50989056 | bytes 3965044 | solution.py:155
  10.6 1.2 fusion.134
  11.8 0.1 fusion.135
  11.9 0.4 convolution_add_fusion.5
  12.3 1.2 fusion.134
  13.5 0.1 fusion.135
  13.6 0.4 convolution_add_fusion.5
  14.0 0.0 copy-start.1
  14.0 0.7 convert_element_type.415
  14.7 0.1 all-gather.7.cloned.1.call-update
  14.8 0.1 all-gather.5.cloned.1.call-start
  14.9 19.5 %all-gather = bf16[64,128]{1,0:T(8,128)(2,1)S(1)} all-gather(bf16[8,128]{1,0:T(8,128)(2,1)S(1)} %exponential_convert_fusion), channel_id=2, replica_groups=mesh['grp'=2,'sp_0'=8,'sp_1'=8,'tp'=2] {'sp_1'}, dimensions={0}, use_global_device_ids=true | all-gather | bytes 18432 | tf_op jit(solution)/shard_map/all_gather | solution.py:25
  34.5 37.4 %all-gather.7.cloned.1.call-done = bf16[64,128,128]{2,1,0:T(8,128)(2,1)} async-done(((bf16[8,128,128]{2,1,0:T(8,128)(2,1)}), bf16[64,128,128]{2,1,0:T(8,128)(2,1)}) %all-gather.7.cloned.1.call-update) | async-done | bytes 2097168 | tf_op jit(solution)/shard_map/all_gather | solution.py:25
  71.8 3.2 %fusion.81 = bf16[1,8,128,128]{3,2,1,0:T(8,128)(2,1)} fusion(f32[8,128]{1,0:T(8,128)S(1)} %get-tuple-element.170, f32[8,128]{1,0:T(8,128)S(1)} %get-tuple-element.184, f32[8,128]{1,0:T(8,128)S(1)} %get-tuple-element.183, f32[8,128]{1,0:T(8,128)S(1)} %get-tuple-element.182, f32[8,128]{1,0:T(8,128)S(1)} %get-tuple-element.181, ...), kind=kLoop, calls=%fused_computation.123 | loop fusion | flops 3145728 | bytes 2392064 | tf_op jit(solution)/shard_map/convert_element_type | solution.py:25
  75.0 0.1 all-gather.5.cloned.1.call-update
  75.1 0.0 copy-done.1
  75.1 0.3 fusion.41
  75.4 1.2 copy.50
  76.7 18.0 %all_gather.22 = bf16[8,8,128]{2,1,0:T(8,128)(2,1)S(1)} all-gather(bf16[1,8,128]{2,1,0:T(8,128)(2,1)S(1)} %fusion.89), channel_id=1, replica_groups=mesh['grp'=2,'sp_0'=8,'sp_1'=8,'tp'=2] {'sp_0'}, dimensions={0}, use_global_device_ids=true | all-gather | bytes 18432 | tf_op jit(solution)/shard_map/all_gather | solution.py:25
  94.7 0.0 copy-done
  94.7 21.3 %all-gather.5.cloned.1.call-done = bf16[8,8,128,128]{3,2,1,0:T(8,128)(2,1)} async-done(((bf16[1,8,128,128]{3,2,1,0:T(8,128)(2,1)}), bf16[8,8,128,128]{3,2,1,0:T(8,128)(2,1)}) %all-gather.5.cloned.1.call-update) | async-done | bytes 2097168 | tf_op jit(solution)/shard_map/all_gather | solution.py:25
  116.1 6.0 %fusion.53 = f32[8,128,128]{2,1,0:T(8,128)S(1)} fusion(bf16[8,8,128,128]{3,2,1,0:T(8,128)(2,1)} %all-gather.5.cloned.1.call-done, f32[8,128]{1,0:T(8,128)S(1)} %get-tuple-element.170, f32[8,128]{1,0:T(8,128)S(1)} %get-tuple-element.184, f32[8,128]{1,0:T(8,128)S(1)} %get-tuple-element.183, f32[8,128]{1,0:T(8,128)S(1)} %get-tuple-element.182, ...), kind=kLoop, calls=%fused_computation.88 | loop fusion | flops 8388608 | bytes 4788240 | tf_op jit(solution)/shard_map/add | solution.py:114
  122.0 9.2 %while.25 = (s32[]{:T(128)}, f32[8,128,128]{2,1,0:T(8,128)S(1)}, f32[2,128,8,128]{1,3,2,0:T(8,128)}, f32[2,128,8,128]{3,2,1,0:T(8,128)}, f32[2,128,8,128]{3,2,1,...) while((s32[]{:T(128)}, f32[8,128,128]{2,1,0:T(8,128)S(1)}, ...), condition=%wide.region_5.6_spmd, body=%wide.region_3.5_spmd.sunk | while | flops 152715264 | bytes 8184937 | solution.py:157
  122.0 1.2 fusion.127
  123.2 1.3 fusion.128
  124.5 0.3 convolution_bitcast_fusion.3
  124.9 0.4 convolution_add_fusion.4
  125.3 1.3 fusion.130
  126.6 1.2 fusion.127
  127.8 1.3 fusion.128
  129.1 0.3 convolution_bitcast_fusion.3
  129.4 0.4 convolution_add_fusion.4
  129.9 1.3 fusion.130
  131.2 1.3 multiply_reduce_fusion
  132.5 1.6 %copy.44 = f32[2,128,8,128]{3,2,1,0:T(8,128)S(1)} copy(f32[2,128,8,128]{1,3,2,0:T(8,128)} %get-tuple-element.77) | data formatting | bytes 2097152 | tf_op jit(solution)/shard_map/while | solution.py:157
  134.1 0.1 copy.45
  134.3 0.3 mul.384
  134.6 3.6 %convolution_convert_fusion = bf16[256,2048]{1,0:T(8,128)(2,1)S(1)} fusion(bf16[1024,2048]{1,0:T(8,128)(2,1)} %param.17, f32[32,8,8,128]{3,2,1,0:T(8,128)S(1)} %bitcast.277, f32[32,8,8,128]{3,2,1,0:T(8,128)S(1)} %bitcast.278, f32[1024]{0:T(1024)S(1)} %broadcast_bitcast_fusion), kind=kOutput, calls=%fused_computation.50 | convolution fusion | flops 1075052544 | bytes 7344128 | tf_op jit(solution)/shard_map/dot_general | solution.py:161
  138.2 9.1 %all_to_all.5 = bf16[2,128,2048]{2,1,0:T(8,128)(2,1)S(1)} all-to-all(bf16[2,128,2048]{2,1,0:T(8,128)(2,1)S(1)} %bitcast.279), channel_id=1, replica_groups=mesh['grp'=2,'sp_0'=8,'sp_1'=8,'tp'=2] {'tp'}, dimensions={0} | all-to-all | bytes 2097152 | tf_op jit(solution)/shard_map/all_to_all | solution.py:47
  147.3 1.1 reduce_sum.22
  (21 shorter events, 0.1 us)
Async XLA Ops:
  6.5 88.1 %copy-start = (f32[128]{0:T(128)S(1)}, f32[128]{0:T(128)}, u32[]{:S(2)}) copy-start(f32[128]{0:T(128)} %param.16) | copy-start | bytes 1540
  6.6 2.4 %copy-start.2 = (bf16[256,1024]{1,0:T(8,128)(2,1)S(1)}, bf16[256,1024]{1,0:T(8,128)(2,1)}, u32[]{:S(2)}) copy-start(bf16[256,1024]{1,0:T(8,128)(2,1)} %param.13) | copy-start | bytes 1572868
  6.6 65.3 %all-gather.7.cloned.1.call-start = ((), (), s32[]{:S(2)}) async-start(), calls=%async_computation.2 | async-start | bytes 2359296 | tf_op jit(solution)/shard_map/all_gather | solution.py:25
  14.0 61.2 %copy-start.1 = (bf16[256,1024]{1,0:T(8,128)(2,1)S(1)}, bf16[256,1024]{1,0:T(8,128)(2,1)}, u32[]{:S(2)}) copy-start(bf16[256,1024]{1,0:T(8,128)(2,1)} %param.11) | copy-start | bytes 1572868
  14.8 101.3 %all-gather.5.cloned.1.call-start = ((), (), s32[]{:S(2)}) async-start(), calls=%async_computation.1 | async-start | bytes 2359296 | tf_op jit(solution)/shard_map/all_gather | solution.py:25
Sparse Core Ops, SparseCore 0:
  14.9 56.8 all-gather.6
  75.2 40.7 all-gather.4
where the time goes:
time: 156 us; the launch traced here: 155 us
  waiting for transfers between devices  58.8 us (38%)
  blocking collectives  46.7 us (30%)
  other arithmetic  22.9 us (15%)
  between operations  13.6 us (9%)
  matrix products  8.46 us (5%)
  local copies, waits for them, and re-layouts  4.58 us (3%)
    all_gather x2, waiting for transfers between devices, entering(): lax.all_gather(part.astype(kind), axis)  58.7 us
    all_gather x2, blocking collectives, entering(): lax.all_gather(part.astype(kind), axis)  37.6 us
    all_to_all x1, blocking collectives, summed_on_arrival(): lax.all_to_all(pieces, axis, split_axis=0, concat_axis=0, tiled=True)  9.12 us
    add x1, other arithmetic, combine(): return (earlier[0] * later[0], later[0][:, :, None] * earlier[1] + later[1])  5.96 us
    convert_element_type x4, other arithmetic, entering(): part.astype(kind)  3.99 us
    dot_general x1, matrix products, body(): jnp.dot(normed, readout_mapping_matrix, preferred_element_type=jnp.float32)  3.58 us
  transfers between devices with their start and end apart: 2, of which 2 were waited for; matrix products, arithmetic and copies ran while one was open for 1% of the time, Pallas kernels for 0%

commit v1 on v0

v1 whole, which is shorter than its diff:
```python
import functools

import jax
import jax.numpy as jnp
from jax import lax
from jax.experimental import pallas as pl
from jax.experimental.pallas import tpu as pltpu
from jax.sharding import Mesh
from jax.sharding import PartitionSpec as P

SPAN = 128
HEAD = 128
SP = ("sp_0", "sp_1")
GRP_SP = ("grp", "sp_0", "sp_1")
GRP_SP_TP = ("grp", "sp_0", "sp_1", "tp")
F32 = jnp.float32
BF16 = jnp.bfloat16


def dot(a, b, contract):
    return lax.dot_general(a, b, (contract, ((), ())), preferred_element_type=F32)


def three_parts(x):
    high = x.astype(BF16)
    rest = x - high.astype(F32)
    middle = rest.astype(BF16)
    low = (rest - middle.astype(F32)).astype(BF16)
    return high, middle, low


def summed_rows(selection, x):
    return sum(dot(selection, part, ((1,), (0,))) for part in three_parts(x))


def keyed_and_log_decay(retention, slack, extra):
    keyed = slack * jax.nn.sigmoid(-retention.astype(F32))
    return keyed, jnp.log1p(-keyed) + extra


def ones_where(shape, compare):
    rows = lax.broadcasted_iota(jnp.int32, shape, 0)
    columns = lax.broadcasted_iota(jnp.int32, shape, 1)
    return compare(rows, columns)


def state_kernel(slabs, retention, source, extra, slack, message):
    tokens, channels = retention.shape
    later = ones_where((tokens, tokens), lambda r, c: c > r).astype(BF16)
    rows = HEAD // slabs
    for h in range(channels // HEAD):
        lanes = slice(h * HEAD, (h + 1) * HEAD)
        keyed, log_decay = keyed_and_log_decay(
            retention[:, lanes], slack[:, lanes], extra[:, h : h + 1]
        )
        ahead = summed_rows(later, log_decay)
        sent = (keyed * jnp.exp(ahead)).astype(BF16)
        state = dot(sent, source[:, lanes], ((0,), (0,)))
        message[h * slabs : (h + 1) * slabs, :rows, :] = state.astype(BF16).reshape(
            slabs, rows, HEAD
        )
        total = ahead[:1] + log_decay[:1]
        parts = jnp.concatenate(three_parts(total) + (jnp.zeros((5, HEAD), BF16),), axis=0)
        message[h * slabs : (h + 1) * slabs, rows:, :] = jnp.broadcast_to(
            parts[None], (slabs, 8, HEAD)
        )


def scan_kernel(slab, message, entering, by_channel):
    positions, rows, _ = entering.shape
    parts = message[:, rows:, :].astype(F32)
    decay = jnp.exp(parts[:, 0] + parts[:, 1] + parts[:, 2])
    by_channel[...] = decay.T
    start = pl.multiple_of(slab[0] * rows, rows)
    mine = by_channel[pl.ds(start, rows), :]
    state = jnp.zeros((rows, HEAD), F32)
    for i in range(positions):
        entering[i] = state.astype(BF16)
        if i + 1 < positions:
            state = mine[:, i : i + 1] * state + message[i, :rows, :].astype(F32)


def local_kernel(probe, retention, source, extra, slack, inside, reading):
    tokens, channels = retention.shape
    upto = ones_where((SPAN, SPAN), lambda r, c: c <= r)
    upto_ones = upto.astype(BF16)
    for h in range(channels // HEAD):
        lanes = slice(h * HEAD, (h + 1) * HEAD)
        before, decayed = None, None
        for b in range(tokens // SPAN):
            span = slice(b * SPAN, (b + 1) * SPAN)
            keyed, log_decay = keyed_and_log_decay(
                retention[span, lanes], slack[:, lanes], extra[span, h : h + 1]
            )
            values = source[span, lanes]
            pre = probe[span, lanes].astype(F32)
            query = pre / (1.0 + jnp.exp(-pre))
            running = summed_rows(upto_ones, log_decay)
            last = running[SPAN - 1 :]
            raised = query * jnp.exp(running)
            lifted = raised.astype(BF16)
            lowered = (keyed * jnp.exp(-running)).astype(BF16)
            scores = dot(lifted, lowered, ((1,), (1,)))
            weights = jnp.where(upto, scores, 0.0).astype(BF16)
            out = dot(weights, values, ((1,), (0,)))
            if before is not None:
                out = out + dot(lifted, before.astype(BF16), ((1,), (0,)))
                reading[span, lanes] = (query * jnp.exp(running + decayed)).astype(BF16)
            else:
                reading[span, lanes] = lifted
            inside[span, lanes] = out
            if (b + 1) * SPAN < tokens:
                sent = (keyed * jnp.exp(last - running)).astype(BF16)
                added = dot(sent, values, ((0,), (0,)))
                if before is None:
                    before, decayed = added, last
                else:
                    before = jnp.exp(last).reshape(HEAD, 1) * before + added
                    decayed = decayed + last


def output_kernel(half, inside, reading, entering, gain, matrix, out, normed):
    tokens = out.shape[0]
    start = pl.multiple_of(half[0] * tokens, tokens)
    rows = pl.ds(start, tokens)
    for h in range(entering.shape[0]):
        lanes = slice(h * HEAD, (h + 1) * HEAD)
        mixer = inside[rows, lanes] + dot(reading[rows, lanes], entering[h], ((1,), (0,)))
        scale = lax.rsqrt(jnp.mean(mixer * mixer, axis=-1, keepdims=True) + 1e-06)
        normed[:, lanes] = (mixer * scale * gain[...]).astype(BF16)
    out[...] = dot(normed[...], matrix[...], ((1,), (0,))).astype(out.dtype)


def in_vmem(count):
    return [pl.BlockSpec(memory_space=pltpu.VMEM)] * count


SCALAR = pl.BlockSpec(memory_space=pltpu.SMEM)


def call(kernel, name, inputs, out_shape, flops, scratch=(), scalars=0):
    moved = sum(a.size * a.dtype.itemsize for a in inputs)
    multiple = isinstance(out_shape, (list, tuple))
    outs = out_shape if multiple else [out_shape]
    moved += sum(a.size * a.dtype.itemsize for a in outs)
    return pl.pallas_call(
        kernel,
        name=name,
        out_shape=out_shape,
        in_specs=[SCALAR] * scalars + in_vmem(len(inputs) - scalars),
        out_specs=in_vmem(len(outs)) if multiple else in_vmem(1)[0],
        scratch_shapes=scratch,
        compiler_params=pltpu.CompilerParams(vmem_limit_bytes=48 << 20),
        cost_estimate=pl.CostEstimate(flops=flops, bytes_accessed=moved, transcendentals=0),
    )(*inputs)


def body(
    probe_preactivation,
    retention_preactivation,
    source_entries,
    extra_log_retention,
    retention_slack,
    group_normalizer_gain,
    readout_mapping_matrix,
):
    tokens, channels = probe_preactivation.shape
    heads = channels // HEAD
    positions = lax.axis_size(SP)
    slabs = positions // heads
    rows = HEAD // slabs
    width = readout_mapping_matrix.shape[1]
    slack = retention_slack.reshape(1, channels)
    gain = group_normalizer_gain.reshape(1, HEAD)
    flops = 2 * tokens * channels * HEAD

    message = call(
        functools.partial(state_kernel, slabs),
        "state",
        (retention_preactivation, source_entries, extra_log_retention, slack),
        jax.ShapeDtypeStruct((positions, rows + 8, HEAD), BF16),
        4 * flops,
    )
    arrived = lax.all_to_all(message, SP, split_axis=0, concat_axis=0, tiled=True)
    inside, reading = call(
        local_kernel,
        "local",
        (
            probe_preactivation,
            retention_preactivation,
            source_entries,
            extra_log_retention,
            slack,
        ),
        [
            jax.ShapeDtypeStruct((tokens, channels), F32),
            jax.ShapeDtypeStruct((tokens, channels), BF16),
        ],
        6 * flops,
    )
    slab = (lax.axis_index(SP) % slabs).astype(jnp.int32).reshape(1)
    scanned = call(
        scan_kernel,
        "scan",
        (slab, arrived),
        jax.ShapeDtypeStruct((positions, rows, HEAD), BF16),
        flops,
        scratch=[pltpu.VMEM((HEAD, positions), F32)],
        scalars=1,
    )
    entering = lax.all_to_all(scanned, SP, split_axis=0, concat_axis=0, tiled=True)
    entering = entering.reshape(heads, HEAD, HEAD)

    mine = lax.axis_index("tp").astype(jnp.int32)
    half = tokens // lax.axis_size("tp")

    def projected(which, dtype):
        return call(
            output_kernel,
            "output",
            (which.reshape(1), inside, reading, entering, gain, readout_mapping_matrix),
            jax.ShapeDtypeStruct((half, width), dtype),
            half * channels * width * 2,
            scratch=[pltpu.VMEM((half, channels), BF16)],
            scalars=1,
        )

    away = projected(1 - mine, BF16)
    received = lax.ppermute(away, "tp", [(0, 1), (1, 0)])
    kept = projected(mine, F32)
    return (kept + received.astype(F32)).astype(BF16)


def solution(mesh):
    finer = Mesh(
        mesh.devices.reshape(mesh.shape["grp"], 8, 8, mesh.shape["tp"]),
        ("grp", "sp_0", "sp_1", "tp"),
    )
    in_specs = (
        P(GRP_SP, "tp"),
        P(GRP_SP, "tp"),
        P(GRP_SP, "tp"),
        P(GRP_SP, "tp"),
        P("tp"),
        P(),
        P("tp", None),
    )
    out_specs = P(GRP_SP_TP, None)
    return jax.shard_map(body, mesh=finer, in_specs=in_specs, out_specs=out_specs, check_vma=False)
```

time: 156 us -> 75.4 us (0.48)
  blocking collectives: 46.7 us -> 0 us
  waiting for transfers between devices: 58.8 us -> 15 us
  starting transfers between devices: 0.07 us -> 35.7 us
  other arithmetic: 22.9 us -> 0.93 us
  Pallas kernels: 0 us -> 15.6 us
  between operations: 13.6 us -> 0.1 us
  matrix products: 8.46 us -> 0 us
  local copies, waits for them, and re-layouts: 4.58 us -> 7.41 us
    all_gather x2 -> x0, waiting for transfers between devices: 58.7 us -> none  [entering(): lax.all_gather(part.astype(kind), axis)]
    all_gather x2 -> x0, blocking collectives: 37.6 us -> none  [entering(): lax.all_gather(part.astype(kind), axis)]
    all_to_all x0 -> x2, starting transfers between devices: none -> 28.3 us  [the longest x1 21.8 us: body(): lax.all_to_all(message, SP, split_axis=0, concat_axis=0, tiled=True)]
    pallas_call x0 -> x5, Pallas kernels: none -> 15.6 us  [call(): pl.pallas_call(kernel, name=name, out_shape=out_shape, in_specs=[SCALAR]...]
    all_to_all x0 -> x2, waiting for transfers between devices: none -> 15 us  [the longest x1 12.1 us: body(): lax.all_to_all(message, SP, split_axis=0, concat_axis=0, tiled=True)]
    all_to_all x1 -> x0, blocking collectives: 9.12 us -> none  [summed_on_arrival(): lax.all_to_all(pieces, axis, split_axis=0, concat_axis=0, tiled=True)]
    dot_general x9 -> x0, matrix products: 8.46 us -> none  [the longest x1 3.58 us: body(): jnp.dot(normed, readout_mapping_matrix, preferred_element_type=jnp.float32)]
    ppermute x0 -> x1, starting transfers between devices: none -> 7.42 us  [body(): received = lax.ppermute(away, 'tp', [(0, 1), (1, 0)])]
  transfers between devices with their start and end apart: 2 -> 3, of which waited for: 2 -> 2; matrix products, arithmetic and copies ran while one was open for 1% -> 0% of each run, Pallas kernels for 0% -> 10%
where the time goes in v1:
time: 75.4 us; the launch traced here: 74.8 us
  starting transfers between devices  35.7 us (47%)
  Pallas kernels  15.6 us (21%)
  waiting for transfers between devices  15 us (20%)
  local copies, waits for them, and re-layouts  7.41 us (10%)
  other arithmetic  0.93 us (1%)
    all_to_all x1, starting transfers between devices, body(): lax.all_to_all(message, SP, split_axis=0, concat_axis=0, tiled=True)  21.8 us
    pallas_call x5, Pallas kernels, call(): pl.pallas_call(kernel, name=name, out_shape=out_shape, in_specs=[SCALAR]...  15.6 us
    all_to_all x1, waiting for transfers between devices, body(): lax.all_to_all(message, SP, split_axis=0, concat_axis=0, tiled=True)  12.1 us
    ppermute x1, starting transfers between devices, body(): received = lax.ppermute(away, 'tp', [(0, 1), (1, 0)])  7.42 us
    unnamed x17, local copies, waits for them, and re-layouts  7.41 us
    all_to_all x1, starting transfers between devices, body(): lax.all_to_all(scanned, SP, split_axis=0, concat_axis=0, tiled=True)  6.48 us
    all_to_all x1, waiting for transfers between devices, body(): lax.all_to_all(scanned, SP, split_axis=0, concat_axis=0, tiled=True)  2.92 us
  transfers between devices with their start and end apart: 3, of which 2 were waited for; matrix products, arithmetic and copies ran while one was open for 0% of the time, Pallas kernels for 10%

profile of v1, /device:TPU:513, one launch (start us, length us, event | category | flops | bytes accessed | tf_op | source)
XLA Modules:
  0.0 74.8 jit_solution(5274351492124519217)
XLA Ops:
  0.0 0.0 copy-start.7
  0.0 0.8 %copy.8.extra = f32[256,8]{1,0:T(8,128)S(1)} copy(f32[256,8]{0,1:T(8,128)} %param.10) | data formatting | bytes 16384 | tf_op args[3]
  0.8 0.0 copy-start
  0.9 1.0 %copy-done = bf16[256,1024]{1,0:T(8,128)(2,1)S(1)} copy-done((bf16[256,1024]{1,0:T(8,128)(2,1)S(1)}, bf16[256,1024]{1,0:T(8,128)(2,1)}, u32[]{:S(2)}) %copy-start) | copy-done | bytes 524312
  1.9 0.0 copy-start.2
  1.9 1.0 %copy-done.2 = bf16[256,1024]{1,0:T(8,128)(2,1)S(1)} copy-done((bf16[256,1024]{1,0:T(8,128)(2,1)S(1)}, bf16[256,1024]{1,0:T(8,128)(2,1)}, u32[]{:S(2)}) %copy-start.2) | copy-done | bytes 524312
  2.9 0.0 copy-start.5
  2.9 0.7 copy-done.5
  3.6 3.8 %state.1 = bf16[64,24,128]{2,1,0:T(8,128)(2,1)} custom-call(bf16[256,1024]{1,0:T(8,128)(2,1)S(1)} %copy-done, bf16[256,1024]{1,0:T(8,128)(2,1)S(1)} %copy-done.2, f32[256,8]{1,0:T(8,128)S(1)} %copy.8.extra, f32[1,1024]{1,0:T(1,128)S(1)} %bitcast.8), custom_call_target="tpu_custom_call" | custom-call | flops 268435456 | bytes 1454080 | tf_op jit(solution)/shard_map/state/pallas_call | solution.py:146
  7.5 21.8 %all-to-all-start = ((bf16[64,24,128]{2,1,0:T(8,128)(2,1)}), bf16[64,24,128]{2,1,0:T(8,128)(2,1)S(1)}, u32[]{:S(2)}, u32[]{:S(2)}) async-start(bf16[64,24,128]{2,1,0:T(8,128)(2,1)} %state.1), calls=%async_computation | async-start | bytes 786432 | tf_op jit(solution)/shard_map/all_to_all | solution.py:184
  29.3 12.1 %all-to-all-done.message = bf16[64,24,128]{2,1,0:T(8,128)(2,1)S(1)} async-done(((bf16[64,24,128]{2,1,0:T(8,128)(2,1)}), bf16[64,24,128]{2,1,0:T(8,128)(2,1)S(1)}, u32[]{:S(2)}, u32[]{:S(2)}) %all-to-all-start) | async-done | bytes 393248 | tf_op jit(solution)/shard_map/all_to_all | solution.py:184
  41.4 1.2 %scan.1 = bf16[64,16,128]{2,1,0:T(8,128)(2,1)} custom-call(s32[1]{0:T(128)} %bitcast.2.slab, bf16[64,24,128]{2,1,0:T(8,128)(2,1)S(1)} %all-to-all-done.message), custom_call_target="tpu_custom_call" | custom-call | flops 67108864 | bytes 655364 | tf_op jit(solution)/shard_map/scan/pallas_call | solution.py:146
  42.5 6.5 %all-to-all-start.1 = ((bf16[64,16,128]{2,1,0:T(8,128)(2,1)}), bf16[64,16,128]{2,1,0:T(8,128)(2,1)S(1)}, u32[]{:S(2)}, u32[]{:S(2)}) async-start(bf16[64,16,128]{2,1,0:T(8,128)(2,1)} %scan.1), calls=%async_computation.1 | async-start | bytes 524288 | tf_op jit(solution)/shard_map/all_to_all | solution.py:211
  49.0 0.0 copy-start.1
  49.0 1.0 %copy-done.1 = bf16[256,1024]{1,0:T(8,128)(2,1)S(1)} copy-done((bf16[256,1024]{1,0:T(8,128)(2,1)S(1)}, bf16[256,1024]{1,0:T(8,128)(2,1)}, u32[]{:S(2)}) %copy-start.1) | copy-done | bytes 524312
  50.1 0.0 copy-start.3
  50.1 1.0 %copy-done.3 = bf16[256,1024]{1,0:T(8,128)(2,1)S(1)} copy-done((bf16[256,1024]{1,0:T(8,128)(2,1)S(1)}, bf16[256,1024]{1,0:T(8,128)(2,1)}, u32[]{:S(2)}) %copy-start.3) | copy-done | bytes 524312
  51.1 0.0 copy-start.4
  51.1 1.0 %copy-done.4 = bf16[256,1024]{1,0:T(8,128)(2,1)S(1)} copy-done((bf16[256,1024]{1,0:T(8,128)(2,1)S(1)}, bf16[256,1024]{1,0:T(8,128)(2,1)}, u32[]{:S(2)}) %copy-start.4) | copy-done | bytes 524312
  52.1 0.0 copy-start.6
  52.1 0.7 copy-done.6
  52.8 4.3 %local.1 = (f32[256,1024]{1,0:T(8,128)S(1)}, bf16[256,1024]{1,0:T(8,128)(2,1)S(1)}) custom-call(bf16[256,1024]{1,0:T(8,128)(2,1)S(1)} %copy-done.4, bf16[256,1024]{1,0:T(8,128)(2,1)S(1)} %copy-done.1, bf16[256,1024]{1,0:T(8,128)(2,1)S(1)} %copy-done.3, f32[256,8]{1,0:T(8,128)S(1)} %copy.8.extra, f32[1,1024]{1,0:T(1,128)S(1)} %bitcast.9), custom_call_target="tpu_custom_call" | custom-call | flops 402653184 | bytes 3158016 | tf_op jit(solution)/shard_map/local/pallas_call | solution.py:146
  57.1 2.9 %all-to-all-done.1 = bf16[64,16,128]{2,1,0:T(8,128)(2,1)S(1)} async-done(((bf16[64,16,128]{2,1,0:T(8,128)(2,1)}), bf16[64,16,128]{2,1,0:T(8,128)(2,1)S(1)}, u32[]{:S(2)}, u32[]{:S(2)}) %all-to-all-start.1) | async-done | bytes 262176 | tf_op jit(solution)/shard_map/all_to_all | solution.py:211
  60.0 0.0 copy-done.7
  60.0 3.2 %output.3 = bf16[128,2048]{1,0:T(8,128)(2,1)S(1)} custom-call(s32[1]{0:T(128)} %bitcast.5.half, f32[256,1024]{1,0:T(8,128)S(1)} %get-tuple-element.7.inside, bf16[256,1024]{1,0:T(8,128)(2,1)S(1)} %get-tuple-element.8.reading, bf16[8,128,128]{2,1,0:T(8,128)(2,1)S(1)} %bitcast.6, f32[1,128]{1,0:T(1,128)S(1)} %bitcast.10, bf16[1024,2048]{1,0:T(8,128)(2,1)} %matrix.3), custom_call_target="tpu_custom_call" | custom-call | flops 536870912 | bytes 6554116 | tf_op jit(solution)/shard_map/output/pallas_call | solution.py:146
  63.2 7.4 %collective-permute-start = (bf16[128,2048]{1,0:T(8,128)(2,1)S(1)}, bf16[128,2048]{1,0:T(8,128)(2,1)S(1)}, u32[]{:S(2)}, u32[]{:S(2)}) collective-permute-start(bf16[128,2048]{1,0:T(8,128)(2,1)S(1)} %output.3), channel_id=1, source_target_pairs={{0,1},{1,0},{2,3},{3,2},{4,5},{5,4},{6,7},{7,6},{8,9},{9,8},{10,11... | collective-permute-start | bytes 1572872 | tf_op jit(solution)/shard_map/ppermute | solution.py:229
  70.6 3.2 %output.2 = f32[128,2048]{1,0:T(8,128)S(1)} custom-call(s32[1]{0:T(128)} %bitcast.half, f32[256,1024]{1,0:T(8,128)S(1)} %get-tuple-element.7.inside, bf16[256,1024]{1,0:T(8,128)(2,1)S(1)} %get-tuple-element.8.reading, bf16[8,128,128]{2,1,0:T(8,128)(2,1)S(1)} %bitcast.7, f32[1,128]{1,0:T(1,128)S(1)} %bitcast.11, bf16[1024,2048]{1,0:T(8,128)(2,1)} %matrix.3), custom_call_target="tpu_custom_call" | custom-call | flops 536870912 | bytes 7078404 | tf_op jit(solution)/shard_map/output/pallas_call | solution.py:146
  73.8 0.0 collective-permute-done
  73.8 0.9 %add_convert_fusion = bf16[128,2048]{1,0:T(8,128)(2,1)} fusion(f32[128,2048]{1,0:T(8,128)S(1)} %output.2, bf16[128,2048]{1,0:T(8,128)(2,1)S(1)} %collective-permute-done), kind=kLoop, calls=%fused_computation | loop fusion | flops 786432 | bytes 2097152 | tf_op jit(solution)/shard_map/convert_element_type | solution.py:231
Async XLA Ops:
  0.0 60.0 %copy-start.7 = (f32[128]{0:T(128)S(1)}, f32[128]{0:T(128)}, u32[]{:S(2)}) copy-start(f32[128]{0:T(128)} %param.12) | copy-start | bytes 1540
  0.8 1.0 %copy-start = (bf16[256,1024]{1,0:T(8,128)(2,1)S(1)}, bf16[256,1024]{1,0:T(8,128)(2,1)}, u32[]{:S(2)}) copy-start(bf16[256,1024]{1,0:T(8,128)(2,1)} %retention.3) | copy-start | bytes 1572868
  1.9 1.0 %copy-start.2 = (bf16[256,1024]{1,0:T(8,128)(2,1)S(1)}, bf16[256,1024]{1,0:T(8,128)(2,1)}, u32[]{:S(2)}) copy-start(bf16[256,1024]{1,0:T(8,128)(2,1)} %source.3) | copy-start | bytes 1572868
  2.9 0.7 copy-start.5
  7.5 33.9 %all-to-all-start = ((bf16[64,24,128]{2,1,0:T(8,128)(2,1)}), bf16[64,24,128]{2,1,0:T(8,128)(2,1)S(1)}, u32[]{:S(2)}, u32[]{:S(2)}) async-start(bf16[64,24,128]{2,1,0:T(8,128)(2,1)} %state.1), calls=%async_computation | async-start | bytes 786432 | tf_op jit(solution)/shard_map/all_to_all | solution.py:184
  42.5 17.5 %all-to-all-start.1 = ((bf16[64,16,128]{2,1,0:T(8,128)(2,1)}), bf16[64,16,128]{2,1,0:T(8,128)(2,1)S(1)}, u32[]{:S(2)}, u32[]{:S(2)}) async-start(bf16[64,16,128]{2,1,0:T(8,128)(2,1)} %scan.1), calls=%async_computation.1 | async-start | bytes 524288 | tf_op jit(solution)/shard_map/all_to_all | solution.py:211
  49.0 1.0 %copy-start.1 = (bf16[256,1024]{1,0:T(8,128)(2,1)S(1)}, bf16[256,1024]{1,0:T(8,128)(2,1)}, u32[]{:S(2)}) copy-start(bf16[256,1024]{1,0:T(8,128)(2,1)} %retention.3) | copy-start | bytes 1572868
  50.1 1.0 %copy-start.3 = (bf16[256,1024]{1,0:T(8,128)(2,1)S(1)}, bf16[256,1024]{1,0:T(8,128)(2,1)}, u32[]{:S(2)}) copy-start(bf16[256,1024]{1,0:T(8,128)(2,1)} %source.3) | copy-start | bytes 1572868
  51.1 1.0 %copy-start.4 = (bf16[256,1024]{1,0:T(8,128)(2,1)S(1)}, bf16[256,1024]{1,0:T(8,128)(2,1)}, u32[]{:S(2)}) copy-start(bf16[256,1024]{1,0:T(8,128)(2,1)} %probe.1) | copy-start | bytes 1572868
  52.1 0.7 copy-start.6
  63.2 10.6 %collective-permute-start = (bf16[128,2048]{1,0:T(8,128)(2,1)S(1)}, bf16[128,2048]{1,0:T(8,128)(2,1)S(1)}, u32[]{:S(2)}, u32[]{:S(2)}) collective-permute-start(bf16[128,2048]{1,0:T(8,128)(2,1)S(1)} %output.3), channel_id=1, source_target_pairs={{0,1},{1,0},{2,3},{3,2},{4,5},{5,4},{6,7},{7,6},{8,9},{9,8},{10,11... | collective-permute-start | bytes 1572872 | tf_op jit(solution)/shard_map/ppermute | solution.py:229

commit v2 on v1

v2 whole, which is shorter than its diff:
```python
import functools

import jax
import jax.numpy as jnp
from jax import lax
from jax.experimental import pallas as pl
from jax.experimental.pallas import tpu as pltpu
from jax.sharding import Mesh
from jax.sharding import PartitionSpec as P

SPAN = 128
HEAD = 128
SP = ("sp_0", "sp_1")
GRP_SP = ("grp", "sp_0", "sp_1")
GRP_SP_TP = ("grp", "sp_0", "sp_1", "tp")
F32 = jnp.float32
BF16 = jnp.bfloat16


def dot(a, b, contract):
    return lax.dot_general(a, b, (contract, ((), ())), preferred_element_type=F32)


def two_parts(x):
    high = x.astype(BF16)
    return high, (x - high.astype(F32)).astype(BF16)


def summed_rows(selection, x):
    return sum(dot(selection, part, ((1,), (0,))) for part in two_parts(x))


def keyed_and_log_decay(retention, slack, extra):
    keyed = slack * jax.nn.sigmoid(-retention.astype(F32))
    return keyed, jnp.log1p(-keyed) + extra


def rows_and_columns(shape):
    return lax.broadcasted_iota(jnp.int32, shape, 0), lax.broadcasted_iota(jnp.int32, shape, 1)


def state_kernel(
    slabs, retention, source, far_extra, far_slack, message, r_in, v_in, extra, slack, sems, small
):
    tokens, channels = retention.shape
    wide = 2 * HEAD
    pairs = channels // wide
    first = [
        pltpu.make_async_copy(a, b, small.at[i])
        for i, (a, b) in enumerate(((far_extra, extra), (far_slack, slack)))
    ]
    for copy in first:
        copy.start()

    def copies(source_ref, target, row):
        return [
            pltpu.make_async_copy(
                source_ref.at[:, p * wide : (p + 1) * wide], target.at[p], sems.at[row, p]
            )
            for p in range(pairs)
        ]

    r_copies, v_copies = (copies(retention, r_in, 0), copies(source, v_in, 1))
    for p in range(pairs):
        r_copies[p].start()
        v_copies[p].start()
    r, c = rows_and_columns((tokens, tokens))
    later = (c > r).astype(BF16)
    rows = HEAD // slabs
    for copy in first:
        copy.wait()
    by_token = extra[...].T
    for p in range(pairs):
        r_copies[p].wait()
        added = jnp.concatenate(
            [
                jnp.broadcast_to(by_token[:, h : h + 1], (tokens, HEAD))
                for h in (2 * p, 2 * p + 1)
            ],
            axis=1,
        )
        keyed, log_decay = keyed_and_log_decay(
            r_in[p], slack[:, p * wide : (p + 1) * wide], added
        )
        ahead = summed_rows(later, log_decay)
        sent = (keyed * jnp.exp(ahead)).astype(BF16)
        total = ahead[:1] + log_decay[:1]
        parts = jnp.concatenate(two_parts(total) + (jnp.zeros((6, wide), BF16),), axis=0)
        v_copies[p].wait()
        for k in range(2):
            lanes = slice(k * HEAD, (k + 1) * HEAD)
            h = 2 * p + k
            state = dot(sent[:, lanes], v_in[p, :, lanes], ((0,), (0,)))
            message[h * slabs : (h + 1) * slabs, :rows, :] = state.astype(BF16).reshape(
                slabs, rows, HEAD
            )
            message[h * slabs : (h + 1) * slabs, rows:, :] = jnp.broadcast_to(
                parts[None, :, lanes], (slabs, 8, HEAD)
            )


def scan_kernel(slabs, message, entering, by_channel):
    positions, rows, _ = entering.shape
    slab = lax.rem(lax.axis_index(SP), slabs)
    parts = message[:, rows:, :].astype(F32)
    by_channel[...] = jnp.exp(parts[:, 0] + parts[:, 1]).T
    mine = by_channel[pl.ds(pl.multiple_of(slab * rows, rows), rows), :]
    state = jnp.zeros((rows, HEAD), F32)
    for i in range(positions):
        entering[i] = state.astype(BF16)
        if i + 1 < positions:
            state = mine[:, i : i + 1] * state + message[i, :rows, :].astype(F32)


def local_kernel(probe, retention, source, extra, slack, inside, reading):
    tokens, channels = retention.shape
    r, c = rows_and_columns((SPAN, SPAN))
    upto = c <= r
    upto_ones = upto.astype(BF16)
    by_token = extra[...].T
    for h in range(channels // HEAD):
        lanes = slice(h * HEAD, (h + 1) * HEAD)
        before, decayed = None, None
        for b in range(tokens // SPAN):
            span = slice(b * SPAN, (b + 1) * SPAN)
            keyed, log_decay = keyed_and_log_decay(
                retention[span, lanes], slack[:, lanes], by_token[span, h : h + 1]
            )
            values = source[span, lanes]
            query = jax.nn.silu(probe[span, lanes].astype(F32))
            running = summed_rows(upto_ones, log_decay)
            last = running[SPAN - 1 :]
            raised = query * jnp.exp(running)
            lifted = raised.astype(BF16)
            lowered = (keyed * jnp.exp(-running)).astype(BF16)
            scores = dot(lifted, lowered, ((1,), (1,)))
            weights = jnp.where(upto, scores, 0.0).astype(BF16)
            out = dot(weights, values, ((1,), (0,)))
            if before is not None:
                out = out + dot(lifted, before.astype(BF16), ((1,), (0,)))
                reading[span, lanes] = (query * jnp.exp(running + decayed)).astype(BF16)
            else:
                reading[span, lanes] = lifted
            inside[span, lanes] = out
            if (b + 1) * SPAN < tokens:
                sent = (keyed * jnp.exp(last - running)).astype(BF16)
                added = dot(sent, values, ((0,), (0,)))
                if before is None:
                    before, decayed = added, last
                else:
                    before = jnp.exp(last).reshape(HEAD, 1) * before + added
                    decayed = decayed + last


def output_kernel(away, far, inside, reading, entering, gain, out, normed, matrix, sems):
    tokens, width = out.shape
    pieces = matrix.shape[0]
    wide = width // pieces
    copies = [
        pltpu.make_async_copy(far.at[:, i * wide : (i + 1) * wide], matrix.at[i], sems.at[i])
        for i in range(pieces)
    ]
    for copy in copies:
        copy.start()
    mine = lax.axis_index("tp")
    half = 1 - mine if away else mine
    rows = pl.ds(pl.multiple_of(half * tokens, tokens), tokens)
    for h in range(entering.shape[0]):
        lanes = slice(h * HEAD, (h + 1) * HEAD)
        mixer = inside[rows, lanes] + dot(reading[rows, lanes], entering[h], ((1,), (0,)))
        scale = lax.rsqrt(jnp.mean(mixer * mixer, axis=-1, keepdims=True) + 1e-06)
        normed[:, lanes] = (mixer * scale * gain[...]).astype(BF16)
    for i, copy in enumerate(copies):
        copy.wait()
        out[:, i * wide : (i + 1) * wide] = dot(normed[...], matrix[i], ((1,), (0,))).astype(
            out.dtype
        )


VMEM = 67043328
IN_VMEM = pl.BlockSpec(memory_space=pltpu.VMEM)
IN_HBM = pl.BlockSpec(memory_space=pltpu.HBM)


def call(kernel, name, far, near, outs, flops, scratch=(), left=24 << 20):
    inputs = (*far, *near)
    moved = sum(a.size * a.dtype.itemsize for a in (*inputs, *outs))
    results = pl.pallas_call(
        kernel,
        name=name,
        out_shape=outs,
        in_specs=[IN_HBM] * len(far) + [IN_VMEM] * len(near),
        out_specs=[IN_VMEM] * len(outs),
        scratch_shapes=scratch,
        compiler_params=pltpu.CompilerParams(vmem_limit_bytes=VMEM - left),
        cost_estimate=pl.CostEstimate(flops=flops, bytes_accessed=moved, transcendentals=0),
    )(*inputs)
    return results if len(outs) > 1 else results[0]


def body(
    probe_preactivation,
    retention_preactivation,
    source_entries,
    extra_log_retention,
    retention_slack,
    group_normalizer_gain,
    readout_mapping_matrix,
):
    tokens, channels = probe_preactivation.shape
    heads = channels // HEAD
    positions = lax.axis_size(SP)
    slabs = positions // heads
    rows = HEAD // slabs
    width = readout_mapping_matrix.shape[1]
    slack = retention_slack.reshape(1, channels)
    gain = group_normalizer_gain.reshape(1, HEAD)
    extra = extra_log_retention.T
    flops = 2 * tokens * channels * HEAD
    pairs = channels // (2 * HEAD)

    message = call(
        functools.partial(state_kernel, slabs),
        "state",
        (retention_preactivation, source_entries, extra, slack),
        (),
        [jax.ShapeDtypeStruct((positions, rows + 8, HEAD), BF16)],
        4 * flops,
        [pltpu.VMEM((pairs, tokens, 2 * HEAD), BF16)] * 2
        + [pltpu.VMEM(extra.shape, F32), pltpu.VMEM(slack.shape, F32)]
        + [pltpu.SemaphoreType.DMA((2, pairs)), pltpu.SemaphoreType.DMA((2,))],
        21 << 19,
    )
    arrived = lax.all_to_all(message, SP, split_axis=0, concat_axis=0, tiled=True)
    inside, reading = call(
        local_kernel,
        "local",
        (),
        (probe_preactivation, retention_preactivation, source_entries, extra, slack),
        [
            jax.ShapeDtypeStruct((tokens, channels), F32),
            jax.ShapeDtypeStruct((tokens, channels), BF16),
        ],
        6 * flops,
    )
    scanned = call(
        functools.partial(scan_kernel, slabs),
        "scan",
        (),
        (arrived,),
        [jax.ShapeDtypeStruct((positions, rows, HEAD), BF16)],
        flops,
        [pltpu.VMEM((HEAD, positions), F32)],
    )
    entering = lax.all_to_all(scanned, SP, split_axis=0, concat_axis=0, tiled=True)
    entering = entering.reshape(heads, HEAD, HEAD)
    half = tokens // lax.axis_size("tp")

    pieces = 4

    def projected(away, dtype):
        return call(
            functools.partial(output_kernel, away),
            "away" if away else "kept",
            (readout_mapping_matrix,),
            (inside, reading, entering, gain),
            [jax.ShapeDtypeStruct((half, width), dtype)],
            half * channels * width * 2,
            [
                pltpu.VMEM((half, channels), BF16),
                pltpu.VMEM((pieces, channels, width // pieces), BF16),
                pltpu.SemaphoreType.DMA((pieces,)),
            ],
            14 << 20,
        )

    received = lax.ppermute(projected(True, BF16), "tp", [(0, 1), (1, 0)])
    return (projected(False, F32) + received.astype(F32)).astype(BF16)


def solution(mesh):
    finer = Mesh(
        mesh.devices.reshape(mesh.shape["grp"], 8, 8, mesh.shape["tp"]),
        ("grp", "sp_0", "sp_1", "tp"),
    )
    in_specs = (
        P(GRP_SP, "tp"),
        P(GRP_SP, "tp"),
        P(GRP_SP, "tp"),
        P(GRP_SP, "tp"),
        P("tp"),
        P(),
        P("tp", None),
    )
    out_specs = P(GRP_SP_TP, None)
    return jax.shard_map(body, mesh=finer, in_specs=in_specs, out_specs=out_specs, check_vma=False)
```

time: 75.4 us -> 71.1 us (0.943)
  blocking collectives: 0 us -> 33.7 us
  starting transfers between devices: 35.7 us -> 13.3 us
  waiting for transfers between devices: 15 us -> 2.82 us
  Pallas kernels: 15.6 us -> 13.8 us
  local copies, waits for them, and re-layouts: 7.41 us -> 5.9 us
    all_to_all x0 -> x1, blocking collectives: none -> 33.7 us  [body(): lax.all_to_all(message, SP, split_axis=0, concat_axis=0, tiled=True)]
    all_to_all x1 -> x0, starting transfers between devices: 21.8 us -> none  [body(): lax.all_to_all(message, SP, split_axis=0, concat_axis=0, tiled=True)]
    all_to_all x1 -> x0, waiting for transfers between devices: 12.1 us -> none  [body(): lax.all_to_all(message, SP, split_axis=0, concat_axis=0, tiled=True)]
    pallas_call x5, Pallas kernels: 15.6 us -> 13.8 us  [call(): pl.pallas_call(kernel, name=name, out_shape=outs, in_specs=[IN_HBM] * len...]
    unnamed x17 -> x16, local copies, waits for them, and re-layouts: 7.41 us -> 5.9 us
  transfers between devices with their start and end apart: 3 -> 2, of which waited for: 2 -> 1; matrix products, arithmetic and copies ran while one was open for 0% -> 0% of each run, Pallas kernels for 10% -> 9%
where the time goes in v2:
time: 71.1 us; the launch traced here: 70.6 us
  blocking collectives  33.7 us (47%)
  Pallas kernels  13.8 us (19%)
  starting transfers between devices  13.3 us (19%)
  local copies, waits for them, and re-layouts  5.9 us (8%)
  waiting for transfers between devices  2.82 us (4%)
  other arithmetic  0.92 us (1%)
    all_to_all x1, blocking collectives, body(): lax.all_to_all(message, SP, split_axis=0, concat_axis=0, tiled=True)  33.7 us
    pallas_call x5, Pallas kernels, call(): pl.pallas_call(kernel, name=name, out_shape=outs, in_specs=[IN_HBM] * len...  13.8 us
    ppermute x1, starting transfers between devices, body(): received = lax.ppermute(projected(True, BF16), 'tp', [(0, 1), (1, 0)])  6.85 us
    all_to_all x1, starting transfers between devices, body(): lax.all_to_all(scanned, SP, split_axis=0, concat_axis=0, tiled=True)  6.48 us
    unnamed x16, local copies, waits for them, and re-layouts  5.9 us
    all_to_all x1, waiting for transfers between devices, body(): lax.all_to_all(scanned, SP, split_axis=0, concat_axis=0, tiled=True)  2.82 us
  transfers between devices with their start and end apart: 2, of which 1 were waited for; matrix products, arithmetic and copies ran while one was open for 0% of the time, Pallas kernels for 9%

profile of v2, /device:TPU:513, one launch (start us, length us, event | category | flops | bytes accessed | tf_op | source)
XLA Modules:
  0.0 70.6 jit_solution(282498098257981347)
XLA Ops:
  0.0 0.0 copy-start.7
  0.0 0.0 copy-start.3
  0.0 0.7 %copy-done.3 = f32[256,8]{0,1:T(8,128)S(1)} copy-done((f32[256,8]{0,1:T(8,128)S(1)}, f32[256,8]{0,1:T(8,128)}, u32[]{:S(2)}) %copy-start.3) | copy-done | bytes 8216
  0.7 0.0 copy-start.5
  0.7 0.7 copy-done.5
  1.4 3.7 %state.1 = bf16[64,24,128]{2,1,0:T(8,128)(2,1)S(1)} custom-call(bf16[256,1024]{1,0:T(8,128)(2,1)} %retention.3, bf16[256,1024]{1,0:T(8,128)(2,1)} %source.3, f32[8,256]{1,0:T(8,128)S(1)} %bitcast.6, f32[1,1024]{1,0:T(1,128)S(1)} %bitcast.8), custom_call_target="tpu_custom_call" | custom-call | flops 268435456 | bytes 1454080 | tf_op jit(solution)/shard_map/state/pallas_call | solution.py:188
  5.1 33.7 %all_to_all.10.message = bf16[64,24,128]{2,1,0:T(8,128)(2,1)S(1)} all-to-all(bf16[64,24,128]{2,1,0:T(8,128)(2,1)S(1)} %state.1), channel_id=1, replica_groups=mesh['grp'=2,'sp_0'=8,'sp_1'=8,'tp'=2] {'sp_0','sp_1'}, dimensions={0} | all-to-all | bytes 786432 | tf_op jit(solution)/shard_map/all_to_all | solution.py:234
  38.8 1.1 %scan.1 = bf16[64,16,128]{2,1,0:T(8,128)(2,1)} custom-call(bf16[64,24,128]{2,1,0:T(8,128)(2,1)S(1)} %all_to_all.10.message), custom_call_target="tpu_custom_call" | custom-call | flops 67108864 | bytes 655360 | tf_op jit(solution)/shard_map/scan/pallas_call | solution.py:188
  40.0 6.5 %all-to-all-start.1 = ((bf16[64,16,128]{2,1,0:T(8,128)(2,1)}), bf16[64,16,128]{2,1,0:T(8,128)(2,1)S(1)}, u32[]{:S(2)}, u32[]{:S(2)}) async-start(bf16[64,16,128]{2,1,0:T(8,128)(2,1)} %scan.1), calls=%async_computation.1 | async-start | bytes 524288 | tf_op jit(solution)/shard_map/all_to_all | solution.py:255
  46.4 0.0 copy-start
  46.5 1.0 %copy-done = bf16[256,1024]{1,0:T(8,128)(2,1)S(1)} copy-done((bf16[256,1024]{1,0:T(8,128)(2,1)S(1)}, bf16[256,1024]{1,0:T(8,128)(2,1)}, u32[]{:S(2)}) %copy-start) | copy-done | bytes 524312
  47.5 0.0 copy-start.1
  47.5 1.0 %copy-done.1 = bf16[256,1024]{1,0:T(8,128)(2,1)S(1)} copy-done((bf16[256,1024]{1,0:T(8,128)(2,1)S(1)}, bf16[256,1024]{1,0:T(8,128)(2,1)}, u32[]{:S(2)}) %copy-start.1) | copy-done | bytes 524312
  48.5 0.0 copy-start.2
  48.5 1.0 %copy-done.2 = bf16[256,1024]{1,0:T(8,128)(2,1)S(1)} copy-done((bf16[256,1024]{1,0:T(8,128)(2,1)S(1)}, bf16[256,1024]{1,0:T(8,128)(2,1)}, u32[]{:S(2)}) %copy-start.2) | copy-done | bytes 524312
  49.6 0.0 copy-start.4
  49.6 0.7 copy-done.4
  50.3 0.0 copy-start.6
  50.3 0.7 copy-done.6
  51.0 3.7 %local.1 = (f32[256,1024]{1,0:T(8,128)S(1)}, bf16[256,1024]{1,0:T(8,128)(2,1)S(1)}) custom-call(bf16[256,1024]{1,0:T(8,128)(2,1)S(1)} %copy-done.2, bf16[256,1024]{1,0:T(8,128)(2,1)S(1)} %copy-done, bf16[256,1024]{1,0:T(8,128)(2,1)S(1)} %copy-done.1, f32[8,256]{1,0:T(8,128)S(1)} %bitcast.7, f32[1,1024]{1,0:T(1,128)S(1)} %bitcast.9), custom_call_target="tpu_custom_call" | custom-call | flops 402653184 | bytes 3158016 | tf_op jit(solution)/shard_map/local/pallas_call | solution.py:188
  54.7 2.8 %all-to-all-done.1 = bf16[64,16,128]{2,1,0:T(8,128)(2,1)S(1)} async-done(((bf16[64,16,128]{2,1,0:T(8,128)(2,1)}), bf16[64,16,128]{2,1,0:T(8,128)(2,1)S(1)}, u32[]{:S(2)}, u32[]{:S(2)}) %all-to-all-start.1) | async-done | bytes 262176 | tf_op jit(solution)/shard_map/all_to_all | solution.py:255
  57.5 0.0 copy-done.7
  57.5 2.6 %away.1 = bf16[128,2048]{1,0:T(8,128)(2,1)S(1)} custom-call(bf16[1024,2048]{1,0:T(8,128)(2,1)} %far.3, f32[256,1024]{1,0:T(8,128)S(1)} %get-tuple-element.7.inside, bf16[256,1024]{1,0:T(8,128)(2,1)S(1)} %get-tuple-element.8.reading, bf16[8,128,128]{2,1,0:T(8,128)(2,1)S(1)} %bitcast.4, f32[1,128]{1,0:T(1,128)S(1)} %bitcast.10), custom_call_target="tpu_custom_call" | custom-call | flops 536870912 | bytes 6554112 | tf_op jit(solution)/shard_map/away/pallas_call | solution.py:188
  60.1 6.8 %collective-permute-start = (bf16[128,2048]{1,0:T(8,128)(2,1)S(1)}, bf16[128,2048]{1,0:T(8,128)(2,1)S(1)}, u32[]{:S(2)}, u32[]{:S(2)}) collective-permute-start(bf16[128,2048]{1,0:T(8,128)(2,1)S(1)} %away.1), channel_id=1, source_target_pairs={{0,1},{1,0},{2,3},{3,2},{4,5},{5,4},{6,7},{7,6},{8,9},{9,8},{10,11... | collective-permute-start | bytes 1572872 | tf_op jit(solution)/shard_map/ppermute | solution.py:277
  67.0 2.6 %kept.1 = f32[128,2048]{1,0:T(8,128)S(1)} custom-call(bf16[1024,2048]{1,0:T(8,128)(2,1)} %far.3, f32[256,1024]{1,0:T(8,128)S(1)} %get-tuple-element.7.inside, bf16[256,1024]{1,0:T(8,128)(2,1)S(1)} %get-tuple-element.8.reading, bf16[8,128,128]{2,1,0:T(8,128)(2,1)S(1)} %bitcast.5, f32[1,128]{1,0:T(1,128)S(1)} %bitcast.11), custom_call_target="tpu_custom_call" | custom-call | flops 536870912 | bytes 7078400 | tf_op jit(solution)/shard_map/kept/pallas_call | solution.py:188
  69.6 0.0 collective-permute-done
  69.6 0.9 %add_convert_fusion = bf16[128,2048]{1,0:T(8,128)(2,1)} fusion(f32[128,2048]{1,0:T(8,128)S(1)} %kept.1, bf16[128,2048]{1,0:T(8,128)(2,1)S(1)} %collective-permute-done), kind=kLoop, calls=%fused_computation | loop fusion | flops 786432 | bytes 2097152 | tf_op jit(solution)/shard_map/convert_element_type | solution.py:278
Async XLA Ops:
  0.0 57.5 %copy-start.7 = (f32[128]{0:T(128)S(1)}, f32[128]{0:T(128)}, u32[]{:S(2)}) copy-start(f32[128]{0:T(128)} %param.12) | copy-start | bytes 1540
  0.0 0.7 %copy-start.3 = (f32[256,8]{0,1:T(8,128)S(1)}, f32[256,8]{0,1:T(8,128)}, u32[]{:S(2)}) copy-start(f32[256,8]{0,1:T(8,128)} %param.10) | copy-start | bytes 24580
  0.7 0.7 copy-start.5
  40.0 17.5 %all-to-all-start.1 = ((bf16[64,16,128]{2,1,0:T(8,128)(2,1)}), bf16[64,16,128]{2,1,0:T(8,128)(2,1)S(1)}, u32[]{:S(2)}, u32[]{:S(2)}) async-start(bf16[64,16,128]{2,1,0:T(8,128)(2,1)} %scan.1), calls=%async_computation.1 | async-start | bytes 524288 | tf_op jit(solution)/shard_map/all_to_all | solution.py:255
  46.4 1.0 %copy-start = (bf16[256,1024]{1,0:T(8,128)(2,1)S(1)}, bf16[256,1024]{1,0:T(8,128)(2,1)}, u32[]{:S(2)}) copy-start(bf16[256,1024]{1,0:T(8,128)(2,1)} %retention.3) | copy-start | bytes 1572868
  47.5 1.0 %copy-start.1 = (bf16[256,1024]{1,0:T(8,128)(2,1)S(1)}, bf16[256,1024]{1,0:T(8,128)(2,1)}, u32[]{:S(2)}) copy-start(bf16[256,1024]{1,0:T(8,128)(2,1)} %source.3) | copy-start | bytes 1572868
  48.5 1.0 %copy-start.2 = (bf16[256,1024]{1,0:T(8,128)(2,1)S(1)}, bf16[256,1024]{1,0:T(8,128)(2,1)}, u32[]{:S(2)}) copy-start(bf16[256,1024]{1,0:T(8,128)(2,1)} %probe.1) | copy-start | bytes 1572868
  49.6 0.7 copy-start.4
  50.3 0.7 copy-start.6
  60.1 9.5 %collective-permute-start = (bf16[128,2048]{1,0:T(8,128)(2,1)S(1)}, bf16[128,2048]{1,0:T(8,128)(2,1)S(1)}, u32[]{:S(2)}, u32[]{:S(2)}) collective-permute-start(bf16[128,2048]{1,0:T(8,128)(2,1)S(1)} %away.1), channel_id=1, source_target_pairs={{0,1},{1,0},{2,3},{3,2},{4,5},{5,4},{6,7},{7,6},{8,9},{9,8},{10,11... | collective-permute-start | bytes 1572872 | tf_op jit(solution)/shard_map/ppermute | solution.py:277

commit v3 on v2

--- a/solution.py
+++ b/solution.py
@@ -13,6 +13,7 @@
 SP = ("sp_0", "sp_1")
 GRP_SP = ("grp", "sp_0", "sp_1")
 GRP_SP_TP = ("grp", "sp_0", "sp_1", "tp")
+SWAP = ((0, 1), (1, 0))
 F32 = jnp.float32
 BF16 = jnp.bfloat16
 
@@ -152,29 +153,44 @@
                     decayed = decayed + last
 
 
-def output_kernel(away, far, inside, reading, entering, gain, out, normed, matrix, sems):
-    tokens, width = out.shape
+def norm_kernel(inside, reading, entering, gain, mine, other):
+    tokens = mine.shape[0]
+    index = lax.axis_index("tp")
+    for half, out in ((1 - index, other), (index, mine)):
+        rows = pl.ds(pl.multiple_of(half * tokens, tokens), tokens)
+        for h in range(entering.shape[0]):
+            lanes = slice(h * HEAD, (h + 1) * HEAD)
+            mixer = inside[rows, lanes] + dot(reading[rows, lanes], entering[h], ((1,), (0,)))
+            scale = lax.rsqrt(jnp.mean(mixer * mixer, axis=-1, keepdims=True) + 1e-06)
+            out[:, lanes] = (mixer * scale * gain[...]).astype(BF16)
+
+
+def own_kernel(far, mine, out, matrix, sems):
     pieces = matrix.shape[0]
-    wide = width // pieces
+    wide = out.shape[1] // pieces
     copies = [
         pltpu.make_async_copy(far.at[:, i * wide : (i + 1) * wide], matrix.at[i], sems.at[i])
         for i in range(pieces)
     ]
     for copy in copies:
         copy.start()
-    mine = lax.axis_index("tp")
-    half = 1 - mine if away else mine
-    rows = pl.ds(pl.multiple_of(half * tokens, tokens), tokens)
-    for h in range(entering.shape[0]):
-        lanes = slice(h * HEAD, (h + 1) * HEAD)
-        mixer = inside[rows, lanes] + dot(reading[rows, lanes], entering[h], ((1,), (0,)))
-        scale = lax.rsqrt(jnp.mean(mixer * mixer, axis=-1, keepdims=True) + 1e-06)
-        normed[:, lanes] = (mixer * scale * gain[...]).astype(BF16)
     for i, copy in enumerate(copies):
         copy.wait()
-        out[:, i * wide : (i + 1) * wide] = dot(normed[...], matrix[i], ((1,), (0,))).astype(
-            out.dtype
-        )
+        out[:, i * wide : (i + 1) * wide] = dot(mine[...], matrix[i], ((1,), (0,)))
+
+
+def final_kernel(own, received, matrix, far, out, sems):
+    pieces = out.shape[0]
+    wide = own.shape[1] // pieces
+    copies = []
+    for i in range(pieces):
+        columns = slice(i * wide, (i + 1) * wide)
+        added = dot(received[...], matrix[:, columns], ((1,), (0,)))
+        out[i] = (own[:, columns] + added).astype(BF16)
+        copies.append(pltpu.make_async_copy(out.at[i], far.at[:, columns], sems.at[i]))
+        copies[-1].start()
+    for copy in copies:
+        copy.wait()
 
 
 VMEM = 67043328
@@ -182,7 +198,7 @@
 IN_HBM = pl.BlockSpec(memory_space=pltpu.HBM)
 
 
-def call(kernel, name, far, near, outs, flops, scratch=(), left=24 << 20):
+def call(kernel, name, far, near, outs, flops, scratch=(), left=24 << 20, out_spec=IN_VMEM):
     inputs = (*far, *near)
     moved = sum(a.size * a.dtype.itemsize for a in (*inputs, *outs))
     results = pl.pallas_call(
@@ -190,7 +206,7 @@
         name=name,
         out_shape=outs,
         in_specs=[IN_HBM] * len(far) + [IN_VMEM] * len(near),
-        out_specs=[IN_VMEM] * len(outs),
+        out_specs=[out_spec] * len(outs),
         scratch_shapes=scratch,
         compiler_params=pltpu.CompilerParams(vmem_limit_bytes=VMEM - left),
         cost_estimate=pl.CostEstimate(flops=flops, bytes_accessed=moved, transcendentals=0),
@@ -243,6 +259,10 @@
         ],
         6 * flops,
     )
+    arrived, inside, reading, matrix = lax.optimization_barrier(
+        (arrived, inside, reading, readout_mapping_matrix)
+    )
+    matrix = lax.ppermute(matrix, "tp", SWAP)
     scanned = call(
         functools.partial(scan_kernel, slabs),
         "scan",
@@ -256,26 +276,40 @@
     entering = entering.reshape(heads, HEAD, HEAD)
     half = tokens // lax.axis_size("tp")
 
+    projection = half * channels * width * 2
+    mine, other = call(
+        norm_kernel,
+        "norm",
+        (),
+        (inside, reading, entering, gain),
+        [jax.ShapeDtypeStruct((half, channels), BF16)] * 2,
+        flops,
+    )
+    received = lax.ppermute(other, "tp", SWAP)
     pieces = 4
-
-    def projected(away, dtype):
-        return call(
-            functools.partial(output_kernel, away),
-            "away" if away else "kept",
-            (readout_mapping_matrix,),
-            (inside, reading, entering, gain),
-            [jax.ShapeDtypeStruct((half, width), dtype)],
-            half * channels * width * 2,
-            [
-                pltpu.VMEM((half, channels), BF16),
-                pltpu.VMEM((pieces, channels, width // pieces), BF16),
-                pltpu.SemaphoreType.DMA((pieces,)),
-            ],
-            14 << 20,
-        )
-
-    received = lax.ppermute(projected(True, BF16), "tp", [(0, 1), (1, 0)])
-    return (projected(False, F32) + received.astype(F32)).astype(BF16)
+    own = call(
+        own_kernel,
+        "own",
+        (readout_mapping_matrix,),
+        (mine,),
+        [jax.ShapeDtypeStruct((half, width), F32)],
+        projection,
+        [
+            pltpu.VMEM((pieces, channels, width // pieces), BF16),
+            pltpu.SemaphoreType.DMA((pieces,)),
+        ],
+        17 << 20,
+    )
+    return call(
+        final_kernel,
+        "final",
+        (),
+        (own, received, matrix),
+        [jax.ShapeDtypeStruct((half, width), BF16)],
+        projection,
+        [pltpu.VMEM((pieces, half, width // pieces), BF16), pltpu.SemaphoreType.DMA((pieces,))],
+        out_spec=IN_HBM,
+    )
 
 
 def solution(mesh):

time: 71.1 us -> 76 us (1.069)
  starting transfers between devices: 13.3 us -> 30.5 us
  blocking collectives: 33.7 us -> 20.5 us
  local copies, waits for them, and re-layouts: 5.9 us -> 8.09 us
  Pallas kernels: 13.8 us -> 12.5 us
  waiting for transfers between devices: 2.82 us -> 3.85 us
  other arithmetic: 0.92 us -> 0 us
    all_to_all x1, starting transfers between devices: 6.48 us -> 21.8 us  [body(): lax.all_to_all(message, SP, split_axis=0, concat_axis=0, tiled=True)]
    all_to_all x1, blocking collectives: 33.7 us -> 20.5 us  [body(): lax.all_to_all(scanned, SP, split_axis=0, concat_axis=0, tiled=True)]
    unnamed x16 -> x18, local copies, waits for them, and re-layouts: 5.9 us -> 8.09 us
    ppermute x1 -> x2, starting transfers between devices: 6.85 us -> 8.68 us  [the longest x1 6.17 us: body(): matrix = lax.ppermute(matrix, 'tp', SWAP)]
    pallas_call x5 -> x6, Pallas kernels: 13.8 us -> 12.5 us  [call(): pl.pallas_call(kernel, name=name, out_shape=outs, in_specs=[IN_HBM] * len...]
    all_to_all x1, waiting for transfers between devices: 2.82 us -> 3.84 us  [body(): lax.all_to_all(message, SP, split_axis=0, concat_axis=0, tiled=True)]
    convert_element_type x1 -> x0, other arithmetic: 0.92 us -> none  [body(): return (projected(False, F32) + received.astype(F32)).astype(BF16)]
  transfers between devices with their start and end apart: 2 -> 3, of which waited for: 1 -> 1; matrix products, arithmetic and copies ran while one was open for 0% -> 0% of each run, Pallas kernels for 9% -> 9%
where the time goes in v3:
time: 76 us; the launch traced here: 75.5 us
  starting transfers between devices  30.5 us (40%)
  blocking collectives  20.5 us (27%)
  Pallas kernels  12.5 us (16%)
  local copies, waits for them, and re-layouts  8.09 us (11%)
  waiting for transfers between devices  3.85 us (5%)
    all_to_all x1, starting transfers between devices, body(): lax.all_to_all(message, SP, split_axis=0, concat_axis=0, tiled=True)  21.8 us
    all_to_all x1, blocking collectives, body(): lax.all_to_all(scanned, SP, split_axis=0, concat_axis=0, tiled=True)  20.5 us
    pallas_call x6, Pallas kernels, call(): pl.pallas_call(kernel, name=name, out_shape=outs, in_specs=[IN_HBM] * len...  12.5 us
    unnamed x18, local copies, waits for them, and re-layouts  8.09 us
    ppermute x1, starting transfers between devices, body(): matrix = lax.ppermute(matrix, 'tp', SWAP)  6.17 us
    all_to_all x1, waiting for transfers between devices, body(): lax.all_to_all(message, SP, split_axis=0, concat_axis=0, tiled=True)  3.84 us
    ppermute x1, starting transfers between devices, body(): received = lax.ppermute(other, 'tp', SWAP)  2.51 us
  transfers between devices with their start and end apart: 3, of which 1 were waited for; matrix products, arithmetic and copies ran while one was open for 0% of the time, Pallas kernels for 9%

profile of v3, /device:TPU:513, one launch (start us, length us, event | category | flops | bytes accessed | tf_op | source)
XLA Modules:
  0.0 75.5 jit_solution(2881389185744915828)
XLA Ops:
  0.0 0.0 copy-start.8
  0.0 0.0 copy-start.4
  0.0 0.7 copy-done.4
  0.7 0.0 copy-start.6
  0.7 0.7 copy-done.6
  1.4 4.4 %state.1 = bf16[64,24,128]{2,1,0:T(8,128)(2,1)} custom-call(bf16[256,1024]{1,0:T(8,128)(2,1)} %retention.3, bf16[256,1024]{1,0:T(8,128)(2,1)} %source.3, f32[8,256]{1,0:T(8,128)S(1)} %bitcast.5, f32[1,1024]{1,0:T(1,128)S(1)} %bitcast.7), custom_call_target="tpu_custom_call" | custom-call | flops 268435456 | bytes 1454080 | tf_op jit(solution)/shard_map/state/pallas_call | solution.py:204
  5.9 21.8 %all-to-all-start = ((bf16[64,24,128]{2,1,0:T(8,128)(2,1)}), bf16[64,24,128]{2,1,0:T(8,128)(2,1)S(1)}, u32[]{:S(2)}, u32[]{:S(2)}) async-start(bf16[64,24,128]{2,1,0:T(8,128)(2,1)} %state.1), calls=%async_computation | async-start | bytes 786432 | tf_op jit(solution)/shard_map/all_to_all | solution.py:250
  27.7 0.0 copy-start.1
  27.7 1.0 %copy-done.1 = bf16[256,1024]{1,0:T(8,128)(2,1)S(1)} copy-done((bf16[256,1024]{1,0:T(8,128)(2,1)S(1)}, bf16[256,1024]{1,0:T(8,128)(2,1)}, u32[]{:S(2)}) %copy-start.1) | copy-done | bytes 524312
  28.7 0.0 copy-start.2
  28.7 1.0 %copy-done.2 = bf16[256,1024]{1,0:T(8,128)(2,1)S(1)} copy-done((bf16[256,1024]{1,0:T(8,128)(2,1)S(1)}, bf16[256,1024]{1,0:T(8,128)(2,1)}, u32[]{:S(2)}) %copy-start.2) | copy-done | bytes 524312
  29.8 0.0 copy-start.3
  29.8 1.0 %copy-done.3 = bf16[256,1024]{1,0:T(8,128)(2,1)S(1)} copy-done((bf16[256,1024]{1,0:T(8,128)(2,1)S(1)}, bf16[256,1024]{1,0:T(8,128)(2,1)}, u32[]{:S(2)}) %copy-start.3) | copy-done | bytes 524312
  30.8 0.0 copy-start.5
  30.8 0.7 copy-done.5
  31.5 0.0 copy-start.7
  31.5 0.7 copy-done.7
  32.2 3.7 %local.1 = (f32[256,1024]{1,0:T(8,128)S(1)}, bf16[256,1024]{1,0:T(8,128)(2,1)S(1)}) custom-call(bf16[256,1024]{1,0:T(8,128)(2,1)S(1)} %copy-done.3, bf16[256,1024]{1,0:T(8,128)(2,1)S(1)} %copy-done.1, bf16[256,1024]{1,0:T(8,128)(2,1)S(1)} %copy-done.2, f32[8,256]{1,0:T(8,128)S(1)} %bitcast.6, f32[1,1024]{1,0:T(1,128)S(1)} %bitcast.8), custom_call_target="tpu_custom_call" | custom-call | flops 402653184 | bytes 3158016 | tf_op jit(solution)/shard_map/local/pallas_call | solution.py:204
  35.9 3.8 %all-to-all-done.message = bf16[64,24,128]{2,1,0:T(8,128)(2,1)S(1)} async-done(((bf16[64,24,128]{2,1,0:T(8,128)(2,1)}), bf16[64,24,128]{2,1,0:T(8,128)(2,1)S(1)}, u32[]{:S(2)}, u32[]{:S(2)}) %all-to-all-start) | async-done | bytes 393248 | tf_op jit(solution)/shard_map/all_to_all | solution.py:250
  39.8 6.2 %collective-permute-start.1 = (bf16[1024,2048]{1,0:T(8,128)(2,1)}, bf16[1024,2048]{1,0:T(8,128)(2,1)S(1)}, u32[]{:S(2)}, u32[]{:S(2)}) collective-permute-start(bf16[1024,2048]{1,0:T(8,128)(2,1)} %far.1), channel_id=1, source_target_pairs={{0,1},{1,0},{2,3},{3,2},{4,5},{5,4},{6,7},{7,6},{8,9},{9,8},{10,11... | collective-permute-start | bytes 12582920 | tf_op jit(solution)/shard_map/ppermute | solution.py:265
  45.9 0.4 scan.1
  46.4 20.5 %all_to_all.10 = bf16[64,16,128]{2,1,0:T(8,128)(2,1)S(1)} all-to-all(bf16[64,16,128]{2,1,0:T(8,128)(2,1)S(1)} %scan.1), channel_id=1, replica_groups=mesh['grp'=2,'sp_0'=8,'sp_1'=8,'tp'=2] {'sp_0','sp_1'}, dimensions={0} | all-to-all | bytes 524288 | tf_op jit(solution)/shard_map/all_to_all | solution.py:275
  66.9 0.0 copy-done.8
  66.9 0.5 norm.1
  67.4 2.5 %collective-permute-start = (bf16[128,1024]{1,0:T(8,128)(2,1)S(1)}, bf16[128,1024]{1,0:T(8,128)(2,1)S(1)}, u32[]{:S(2)}, u32[]{:S(2)}) collective-permute-start(bf16[128,1024]{1,0:T(8,128)(2,1)S(1)} %get-tuple-element.19), channel_id=1, source_target_pairs={{0,1},{1,0},{2,3},{3,2},{4,5},{5,4},{6,7},{7,6},{8,9},{9,8},{10,11... | collective-permute-start | bytes 786440 | tf_op jit(solution)/shard_map/ppermute | solution.py:288
  69.9 0.0 copy-start
  69.9 2.2 %copy-done = bf16[1024,2048]{1,0:T(8,128)(2,1)S(1)} copy-done((bf16[1024,2048]{1,0:T(8,128)(2,1)S(1)}, bf16[1024,2048]{1,0:T(8,128)(2,1)}, u32[]{:S(2)}) %copy-start) | copy-done | bytes 4194328
  72.1 2.0 %own.1 = f32[128,2048]{1,0:T(8,128)S(1)} custom-call(bf16[1024,2048]{1,0:T(8,128)(2,1)S(1)} %copy-done, bf16[128,1024]{1,0:T(8,128)(2,1)S(1)} %get-tuple-element.18.mine), custom_call_target="tpu_custom_call" | custom-call | flops 536870912 | bytes 5505024 | tf_op jit(solution)/shard_map/own/pallas_call | solution.py:204
  74.0 0.0 collective-permute-done.received
  74.1 0.0 collective-permute-done.1.matrix
  74.1 1.4 %final.1 = bf16[128,2048]{1,0:T(8,128)(2,1)} custom-call(f32[128,2048]{1,0:T(8,128)S(1)} %own.1, bf16[128,1024]{1,0:T(8,128)(2,1)S(1)} %collective-permute-done.received, bf16[1024,2048]{1,0:T(8,128)(2,1)S(1)} %collective-permute-done.1.matrix), custom_call_target="tpu_custom_call" | custom-call | flops 536870912 | bytes 6029312 | tf_op jit(solution)/shard_map/final/pallas_call | solution.py:204
Async XLA Ops:
  0.0 66.9 %copy-start.8 = (f32[128]{0:T(128)S(1)}, f32[128]{0:T(128)}, u32[]{:S(2)}) copy-start(f32[128]{0:T(128)} %param.12) | copy-start | bytes 1540
  0.0 0.7 copy-start.4
  0.7 0.7 copy-start.6
  5.9 33.9 %all-to-all-start = ((bf16[64,24,128]{2,1,0:T(8,128)(2,1)}), bf16[64,24,128]{2,1,0:T(8,128)(2,1)S(1)}, u32[]{:S(2)}, u32[]{:S(2)}) async-start(bf16[64,24,128]{2,1,0:T(8,128)(2,1)} %state.1), calls=%async_computation | async-start | bytes 786432 | tf_op jit(solution)/shard_map/all_to_all | solution.py:250
  27.7 1.0 %copy-start.1 = (bf16[256,1024]{1,0:T(8,128)(2,1)S(1)}, bf16[256,1024]{1,0:T(8,128)(2,1)}, u32[]{:S(2)}) copy-start(bf16[256,1024]{1,0:T(8,128)(2,1)} %retention.3) | copy-start | bytes 1572868
  28.7 1.0 %copy-start.2 = (bf16[256,1024]{1,0:T(8,128)(2,1)S(1)}, bf16[256,1024]{1,0:T(8,128)(2,1)}, u32[]{:S(2)}) copy-start(bf16[256,1024]{1,0:T(8,128)(2,1)} %source.3) | copy-start | bytes 1572868
  29.8 1.0 %copy-start.3 = (bf16[256,1024]{1,0:T(8,128)(2,1)S(1)}, bf16[256,1024]{1,0:T(8,128)(2,1)}, u32[]{:S(2)}) copy-start(bf16[256,1024]{1,0:T(8,128)(2,1)} %probe.1) | copy-start | bytes 1572868
  30.8 0.7 copy-start.5
  31.5 0.7 copy-start.7
  39.8 34.3 %collective-permute-start.1 = (bf16[1024,2048]{1,0:T(8,128)(2,1)}, bf16[1024,2048]{1,0:T(8,128)(2,1)S(1)}, u32[]{:S(2)}, u32[]{:S(2)}) collective-permute-start(bf16[1024,2048]{1,0:T(8,128)(2,1)} %far.1), channel_id=1, source_target_pairs={{0,1},{1,0},{2,3},{3,2},{4,5},{5,4},{6,7},{7,6},{8,9},{9,8},{10,11... | collective-permute-start | bytes 12582920 | tf_op jit(solution)/shard_map/ppermute | solution.py:265
  67.4 6.7 %collective-permute-start = (bf16[128,1024]{1,0:T(8,128)(2,1)S(1)}, bf16[128,1024]{1,0:T(8,128)(2,1)S(1)}, u32[]{:S(2)}, u32[]{:S(2)}) collective-permute-start(bf16[128,1024]{1,0:T(8,128)(2,1)S(1)} %get-tuple-element.19), channel_id=1, source_target_pairs={{0,1},{1,0},{2,3},{3,2},{4,5},{5,4},{6,7},{7,6},{8,9},{9,8},{10,11... | collective-permute-start | bytes 786440 | tf_op jit(solution)/shard_map/ppermute | solution.py:288
  69.9 2.2 %copy-start = (bf16[1024,2048]{1,0:T(8,128)(2,1)S(1)}, bf16[1024,2048]{1,0:T(8,128)(2,1)}, u32[]{:S(2)}) copy-start(bf16[1024,2048]{1,0:T(8,128)(2,1)} %far.1) | copy-start | bytes 12582916

commit v4 on v3

--- a/solution.py
+++ b/solution.py
@@ -14,6 +14,7 @@
 GRP_SP = ("grp", "sp_0", "sp_1")
 GRP_SP_TP = ("grp", "sp_0", "sp_1", "tp")
 SWAP = ((0, 1), (1, 0))
+STAY = ((0, 0), (1, 1))
 F32 = jnp.float32
 BF16 = jnp.bfloat16
 
@@ -40,39 +41,15 @@
     return lax.broadcasted_iota(jnp.int32, shape, 0), lax.broadcasted_iota(jnp.int32, shape, 1)
 
 
-def state_kernel(
-    slabs, retention, source, far_extra, far_slack, message, r_in, v_in, extra, slack, sems, small
-):
+def state_kernel(slabs, retention, source, extra, slack, message):
     tokens, channels = retention.shape
     wide = 2 * HEAD
-    pairs = channels // wide
-    first = [
-        pltpu.make_async_copy(a, b, small.at[i])
-        for i, (a, b) in enumerate(((far_extra, extra), (far_slack, slack)))
-    ]
-    for copy in first:
-        copy.start()
-
-    def copies(source_ref, target, row):
-        return [
-            pltpu.make_async_copy(
-                source_ref.at[:, p * wide : (p + 1) * wide], target.at[p], sems.at[row, p]
-            )
-            for p in range(pairs)
-        ]
-
-    r_copies, v_copies = (copies(retention, r_in, 0), copies(source, v_in, 1))
-    for p in range(pairs):
-        r_copies[p].start()
-        v_copies[p].start()
     r, c = rows_and_columns((tokens, tokens))
     later = (c > r).astype(BF16)
     rows = HEAD // slabs
-    for copy in first:
-        copy.wait()
     by_token = extra[...].T
-    for p in range(pairs):
-        r_copies[p].wait()
+    for p in range(channels // wide):
+        lanes = slice(p * wide, (p + 1) * wide)
         added = jnp.concatenate(
             [
                 jnp.broadcast_to(by_token[:, h : h + 1], (tokens, HEAD))
@@ -81,22 +58,22 @@
             axis=1,
         )
         keyed, log_decay = keyed_and_log_decay(
-            r_in[p], slack[:, p * wide : (p + 1) * wide], added
+            retention[:, lanes], slack[:, lanes], added
         )
         ahead = summed_rows(later, log_decay)
         sent = (keyed * jnp.exp(ahead)).astype(BF16)
         total = ahead[:1] + log_decay[:1]
         parts = jnp.concatenate(two_parts(total) + (jnp.zeros((6, wide), BF16),), axis=0)
-        v_copies[p].wait()
         for k in range(2):
-            lanes = slice(k * HEAD, (k + 1) * HEAD)
             h = 2 * p + k
-            state = dot(sent[:, lanes], v_in[p, :, lanes], ((0,), (0,)))
+            part = slice(k * HEAD, (k + 1) * HEAD)
+            values = source[:, h * HEAD : (h + 1) * HEAD]
+            state = dot(sent[:, part], values, ((0,), (0,)))
             message[h * slabs : (h + 1) * slabs, :rows, :] = state.astype(BF16).reshape(
                 slabs, rows, HEAD
             )
             message[h * slabs : (h + 1) * slabs, rows:, :] = jnp.broadcast_to(
-                parts[None, :, lanes], (slabs, 8, HEAD)
+                parts[None, :, part], (slabs, 8, HEAD)
             )
 
 
@@ -165,18 +142,8 @@
             out[:, lanes] = (mixer * scale * gain[...]).astype(BF16)
 
 
-def own_kernel(far, mine, out, matrix, sems):
-    pieces = matrix.shape[0]
-    wide = out.shape[1] // pieces
-    copies = [
-        pltpu.make_async_copy(far.at[:, i * wide : (i + 1) * wide], matrix.at[i], sems.at[i])
-        for i in range(pieces)
-    ]
-    for copy in copies:
-        copy.start()
-    for i, copy in enumerate(copies):
-        copy.wait()
-        out[:, i * wide : (i + 1) * wide] = dot(mine[...], matrix[i], ((1,), (0,)))
+def own_kernel(mine, matrix, out):
+    out[...] = dot(mine[...], matrix[...], ((1,), (0,)))
 
 
 def final_kernel(own, received, matrix, far, out, sems):
@@ -233,36 +200,45 @@
     gain = group_normalizer_gain.reshape(1, HEAD)
     extra = extra_log_retention.T
     flops = 2 * tokens * channels * HEAD
-    pairs = channels // (2 * HEAD)
-
+    retention, source, extra, slack, probe = (
+        lax.ppermute(a, "tp", STAY)
+        for a in (
+            retention_preactivation,
+            source_entries,
+            extra,
+            slack,
+            probe_preactivation,
+        )
+    )
+    retention, source, partner_matrix = lax.optimization_barrier(
+        (retention, source, readout_mapping_matrix)
+    )
+    partner_matrix = lax.ppermute(partner_matrix, "tp", SWAP)
     message = call(
         functools.partial(state_kernel, slabs),
         "state",
-        (retention_preactivation, source_entries, extra, slack),
-        (),
+        (),
+        (retention, source, extra, slack),
         [jax.ShapeDtypeStruct((positions, rows + 8, HEAD), BF16)],
         4 * flops,
-        [pltpu.VMEM((pairs, tokens, 2 * HEAD), BF16)] * 2
-        + [pltpu.VMEM(extra.shape, F32), pltpu.VMEM(slack.shape, F32)]
-        + [pltpu.SemaphoreType.DMA((2, pairs)), pltpu.SemaphoreType.DMA((2,))],
-        21 << 19,
     )
     arrived = lax.all_to_all(message, SP, split_axis=0, concat_axis=0, tiled=True)
     inside, reading = call(
         local_kernel,
         "local",
         (),
-        (probe_preactivation, retention_preactivation, source_entries, extra, slack),
+        (probe, retention, source, extra, slack),
         [
             jax.ShapeDtypeStruct((tokens, channels), F32),
             jax.ShapeDtypeStruct((tokens, channels), BF16),
         ],
         6 * flops,
     )
-    arrived, inside, reading, matrix = lax.optimization_barrier(
-        (arrived, inside, reading, readout_mapping_matrix)
-    )
-    matrix = lax.ppermute(matrix, "tp", SWAP)
+    arrived, inside, reading, matrix, partner_matrix = lax.optimization_barrier(
+        (arrived, inside, reading, readout_mapping_matrix, partner_matrix)
+    )
+    matrix = lax.ppermute(matrix, "tp", STAY)
+    partner_matrix = lax.ppermute(partner_matrix, "tp", STAY)
     scanned = call(
         functools.partial(scan_kernel, slabs),
         "scan",
@@ -290,21 +266,16 @@
     own = call(
         own_kernel,
         "own",
-        (readout_mapping_matrix,),
-        (mine,),
+        (),
+        (mine, matrix),
         [jax.ShapeDtypeStruct((half, width), F32)],
         projection,
-        [
-            pltpu.VMEM((pieces, channels, width // pieces), BF16),
-            pltpu.SemaphoreType.DMA((pieces,)),
-        ],
-        17 << 20,
     )
     return call(
         final_kernel,
         "final",
         (),
-        (own, received, matrix),
+        (own, received, partner_matrix),
         [jax.ShapeDtypeStruct((half, width), BF16)],
         projection,
         [pltpu.VMEM((pieces, half, width // pieces), BF16), pltpu.SemaphoreType.DMA((pieces,))],

time: 76 us -> 77.6 us (1.021)
  starting transfers between devices: 30.5 us -> 39.4 us
  local copies, waits for them, and re-layouts: 8.09 us -> 0.01 us
  waiting for transfers between devices: 3.85 us -> 10.1 us
  Pallas kernels: 12.5 us -> 9.3 us
  blocking collectives: 20.5 us -> 18.3 us
    ppermute x1 -> x8, starting transfers between devices: 6.17 us -> 29.3 us  [the longest x1 20.4 us: body(): partner_matrix = lax.ppermute(partner_matrix, 'tp', SWAP)]
    all_to_all x1, starting transfers between devices: 21.8 us -> 6.49 us  [body(): lax.all_to_all(message, SP, split_axis=0, concat_axis=0, tiled=True)]
    unnamed x18 -> x2, local copies, waits for them, and re-layouts: 8.09 us -> 0.01 us
    all_to_all x1, waiting for transfers between devices: 3.84 us -> 9.65 us  [body(): lax.all_to_all(message, SP, split_axis=0, concat_axis=0, tiled=True)]
    pallas_call x6, Pallas kernels: 12.5 us -> 9.3 us  [call(): pl.pallas_call(kernel, name=name, out_shape=outs, in_specs=[IN_HBM] * len...]
    all_to_all x1, blocking collectives: 20.5 us -> 18.3 us  [body(): lax.all_to_all(scanned, SP, split_axis=0, concat_axis=0, tiled=True)]
    ppermute x1, starting transfers between devices: 2.51 us -> 3.54 us  [body(): received = lax.ppermute(other, 'tp', SWAP)]
  transfers between devices with their start and end apart: 3 -> 10, of which waited for: 1 -> 2; matrix products, arithmetic and copies ran while one was open for 0% -> 0% of each run, Pallas kernels for 9% -> 10%
where the time goes in v4:
time: 77.6 us; the launch traced here: 77.1 us
  starting transfers between devices  39.4 us (51%)
  blocking collectives  18.3 us (24%)
  waiting for transfers between devices  10.1 us (13%)
  Pallas kernels  9.3 us (12%)
    ppermute x1, starting transfers between devices, body(): partner_matrix = lax.ppermute(partner_matrix, 'tp', SWAP)  20.4 us
    all_to_all x1, blocking collectives, body(): lax.all_to_all(scanned, SP, split_axis=0, concat_axis=0, tiled=True)  18.3 us
    all_to_all x1, waiting for transfers between devices, body(): lax.all_to_all(message, SP, split_axis=0, concat_axis=0, tiled=True)  9.65 us
    pallas_call x6, Pallas kernels, call(): pl.pallas_call(kernel, name=name, out_shape=outs, in_specs=[IN_HBM] * len...  9.3 us
    all_to_all x1, starting transfers between devices, body(): lax.all_to_all(message, SP, split_axis=0, concat_axis=0, tiled=True)  6.49 us
    ppermute x5, starting transfers between devices, body(): lax.ppermute(a, 'tp', STAY)  4.55 us
    ppermute x1, starting transfers between devices, body(): received = lax.ppermute(other, 'tp', SWAP)  3.54 us
    ppermute x1, starting transfers between devices, body(): matrix = lax.ppermute(matrix, 'tp', STAY)  2.19 us
  transfers between devices with their start and end apart: 10, of which 2 were waited for; matrix products, arithmetic and copies ran while one was open for 0% of the time, Pallas kernels for 10%

profile of v4, /device:TPU:513, one launch (start us, length us, event | category | flops | bytes accessed | tf_op | source)
XLA Modules:
  0.0 77.1 jit_solution(7308254678838380106)
XLA Ops:
  0.0 0.0 copy-start
  0.0 1.1 %collective-permute-start = (bf16[256,1024]{1,0:T(8,128)(2,1)}, bf16[256,1024]{1,0:T(8,128)(2,1)S(1)}, u32[]{:S(2)}, u32[]{:S(2)}) collective-permute-start(bf16[256,1024]{1,0:T(8,128)(2,1)} %param.8), channel_id=1, source_target_pairs={{0,0},{1,1},{2,2},{3,3},{4,4},{5,5},{6,6},{7,7},{8,8},{9,9},{10,10... | collective-permute-start | bytes 1572872 | tf_op jit(solution)/shard_map/ppermute | solution.py:204
  1.1 1.0 %collective-permute-start.1 = (bf16[256,1024]{1,0:T(8,128)(2,1)}, bf16[256,1024]{1,0:T(8,128)(2,1)S(1)}, u32[]{:S(2)}, u32[]{:S(2)}) collective-permute-start(bf16[256,1024]{1,0:T(8,128)(2,1)} %param.9), channel_id=1, source_target_pairs={{0,0},{1,1},{2,2},{3,3},{4,4},{5,5},{6,6},{7,7},{8,8},{9,9},{10,10... | collective-permute-start | bytes 1572872 | tf_op jit(solution)/shard_map/ppermute | solution.py:204
  2.1 0.0 collective-permute-done.retention
  2.1 0.0 collective-permute-done.1.source
  2.1 20.4 %collective-permute-start.5 = (bf16[1024,2048]{1,0:T(8,128)(2,1)}, bf16[1024,2048]{1,0:T(8,128)(2,1)}, u32[]{:S(2)}, u32[]{:S(2)}) collective-permute-start(bf16[1024,2048]{1,0:T(8,128)(2,1)} %param.13), channel_id=1, source_target_pairs={{0,1},{1,0},{2,3},{3,2},{4,5},{5,4},{6,7},{7,6},{8,9},{9,8},{10,11... | collective-permute-start | bytes 12582920 | tf_op jit(solution)/shard_map/ppermute | solution.py:216
  22.5 0.7 collective-permute-start.2
  23.2 0.7 collective-permute-start.3
  23.9 0.0 collective-permute-done.3.slack
  23.9 0.0 collective-permute-done.2.extra
  23.9 2.5 %state.1 = bf16[64,24,128]{2,1,0:T(8,128)(2,1)} custom-call(bf16[256,1024]{1,0:T(8,128)(2,1)S(1)} %collective-permute-done.retention, bf16[256,1024]{1,0:T(8,128)(2,1)S(1)} %collective-permute-done.1.source, f32[8,256]{1,0:T(8,128)S(1)} %collective-permute-done.2.extra, f32[1,1024]{1,0:T(1,128)S(1)} %collective-permute-done.3.slack), custom_call_target="tpu_custom_call" | custom-call | flops 268435456 | bytes 1454080 | tf_op jit(solution)/shard_map/state/pallas_call | solution.py:171
  26.4 6.5 %all-to-all-start = ((bf16[64,24,128]{2,1,0:T(8,128)(2,1)}), bf16[64,24,128]{2,1,0:T(8,128)(2,1)S(1)}, u32[]{:S(2)}, u32[]{:S(2)}) async-start(bf16[64,24,128]{2,1,0:T(8,128)(2,1)} %state.1), calls=%async_computation | async-start | bytes 786432 | tf_op jit(solution)/shard_map/all_to_all | solution.py:225
  32.9 1.1 %collective-permute-start.4 = (bf16[256,1024]{1,0:T(8,128)(2,1)}, bf16[256,1024]{1,0:T(8,128)(2,1)S(1)}, u32[]{:S(2)}, u32[]{:S(2)}) collective-permute-start(bf16[256,1024]{1,0:T(8,128)(2,1)} %param.7), channel_id=1, source_target_pairs={{0,0},{1,1},{2,2},{3,3},{4,4},{5,5},{6,6},{7,7},{8,8},{9,9},{10,10... | collective-permute-start | bytes 1572872 | tf_op jit(solution)/shard_map/ppermute | solution.py:204
  33.9 0.0 collective-permute-done.4.probe
  33.9 3.7 %local.1 = (f32[256,1024]{1,0:T(8,128)S(1)}, bf16[256,1024]{1,0:T(8,128)(2,1)S(1)}) custom-call(bf16[256,1024]{1,0:T(8,128)(2,1)S(1)} %collective-permute-done.4.probe, bf16[256,1024]{1,0:T(8,128)(2,1)S(1)} %collective-permute-done.retention, bf16[256,1024]{1,0:T(8,128)(2,1)S(1)} %collective-permute-done.1.source, ...), custom_call_target="tpu_custom_call" | custom-call | flops 402653184 | bytes 3158016 | tf_op jit(solution)/shard_map/local/pallas_call | solution.py:171
  37.7 9.6 %all-to-all-done.message = bf16[64,24,128]{2,1,0:T(8,128)(2,1)S(1)} async-done(((bf16[64,24,128]{2,1,0:T(8,128)(2,1)}), bf16[64,24,128]{2,1,0:T(8,128)(2,1)S(1)}, u32[]{:S(2)}, u32[]{:S(2)}) %all-to-all-start) | async-done | bytes 393248 | tf_op jit(solution)/shard_map/all_to_all | solution.py:225
  47.3 0.0 collective-permute-done.5
  47.3 2.2 %collective-permute-start.6 = (bf16[1024,2048]{1,0:T(8,128)(2,1)}, bf16[1024,2048]{1,0:T(8,128)(2,1)S(1)}, u32[]{:S(2)}, u32[]{:S(2)}) collective-permute-start(bf16[1024,2048]{1,0:T(8,128)(2,1)} %param.13), channel_id=1, source_target_pairs={{0,0},{1,1},{2,2},{3,3},{4,4},{5,5},{6,6},{7,7},{8,8},{9,9},{10,10... | collective-permute-start | bytes 12582920 | tf_op jit(solution)/shard_map/ppermute | solution.py:240
  49.5 2.2 %collective-permute-start.8 = (bf16[1024,2048]{1,0:T(8,128)(2,1)}, bf16[1024,2048]{1,0:T(8,128)(2,1)S(1)}, u32[]{:S(2)}, u32[]{:S(2)}) collective-permute-start(bf16[1024,2048]{1,0:T(8,128)(2,1)} %collective-permute-done.5), channel_id=1, source_target_pairs={{0,0},{1,1},{2,2},{3,3},{4,4},{5,5},{6,6},{7,7},{8,8},{9,9},{10,10... | collective-permute-start | bytes 12582920 | tf_op jit(solution)/shard_map/ppermute | solution.py:241
  51.7 0.4 scan.1
  52.2 18.3 %all_to_all.10 = bf16[64,16,128]{2,1,0:T(8,128)(2,1)S(1)} all-to-all(bf16[64,16,128]{2,1,0:T(8,128)(2,1)S(1)} %scan.1), channel_id=1, replica_groups=mesh['grp'=2,'sp_0'=8,'sp_1'=8,'tp'=2] {'sp_0','sp_1'}, dimensions={0} | all-to-all | bytes 524288 | tf_op jit(solution)/shard_map/all_to_all | solution.py:251
  70.5 0.0 copy-done
  70.5 0.5 norm.1
  71.0 3.5 %collective-permute-start.7 = (bf16[128,1024]{1,0:T(8,128)(2,1)S(1)}, bf16[128,1024]{1,0:T(8,128)(2,1)S(1)}, u32[]{:S(2)}, u32[]{:S(2)}) collective-permute-start(bf16[128,1024]{1,0:T(8,128)(2,1)S(1)} %get-tuple-element.27), channel_id=1, source_target_pairs={{0,1},{1,0},{2,3},{3,2},{4,5},{5,4},{6,7},{7,6},{8,9},{9,8},{10,11... | collective-permute-start | bytes 786440 | tf_op jit(solution)/shard_map/ppermute | solution.py:264
  74.5 0.0 collective-permute-done.6.matrix
  74.5 0.7 own.1
  75.3 0.4 collective-permute-done.7.received
  75.7 0.0 collective-permute-done.8.matrix
  75.7 1.4 %final.1 = bf16[128,2048]{1,0:T(8,128)(2,1)} custom-call(f32[128,2048]{1,0:T(8,128)S(1)} %own.1, bf16[128,1024]{1,0:T(8,128)(2,1)S(1)} %collective-permute-done.7.received, bf16[1024,2048]{1,0:T(8,128)(2,1)S(1)} %collective-permute-done.8.matrix), custom_call_target="tpu_custom_call" | custom-call | flops 536870912 | bytes 6029312 | tf_op jit(solution)/shard_map/final/pallas_call | solution.py:171
Async XLA Ops:
  0.0 70.5 %copy-start = (f32[128]{0:T(128)S(1)}, f32[128]{0:T(128)}, u32[]{:S(2)}) copy-start(f32[128]{0:T(128)} %param.12) | copy-start | bytes 1540
  0.0 2.1 %collective-permute-start = (bf16[256,1024]{1,0:T(8,128)(2,1)}, bf16[256,1024]{1,0:T(8,128)(2,1)S(1)}, u32[]{:S(2)}, u32[]{:S(2)}) collective-permute-start(bf16[256,1024]{1,0:T(8,128)(2,1)} %param.8), channel_id=1, source_target_pairs={{0,0},{1,1},{2,2},{3,3},{4,4},{5,5},{6,6},{7,7},{8,8},{9,9},{10,10... | collective-permute-start | bytes 1572872 | tf_op jit(solution)/shard_map/ppermute | solution.py:204
  1.1 1.0 %collective-permute-start.1 = (bf16[256,1024]{1,0:T(8,128)(2,1)}, bf16[256,1024]{1,0:T(8,128)(2,1)S(1)}, u32[]{:S(2)}, u32[]{:S(2)}) collective-permute-start(bf16[256,1024]{1,0:T(8,128)(2,1)} %param.9), channel_id=1, source_target_pairs={{0,0},{1,1},{2,2},{3,3},{4,4},{5,5},{6,6},{7,7},{8,8},{9,9},{10,10... | collective-permute-start | bytes 1572872 | tf_op jit(solution)/shard_map/ppermute | solution.py:204
  2.1 45.2 %collective-permute-start.5 = (bf16[1024,2048]{1,0:T(8,128)(2,1)}, bf16[1024,2048]{1,0:T(8,128)(2,1)}, u32[]{:S(2)}, u32[]{:S(2)}) collective-permute-start(bf16[1024,2048]{1,0:T(8,128)(2,1)} %param.13), channel_id=1, source_target_pairs={{0,1},{1,0},{2,3},{3,2},{4,5},{5,4},{6,7},{7,6},{8,9},{9,8},{10,11... | collective-permute-start | bytes 12582920 | tf_op jit(solution)/shard_map/ppermute | solution.py:216
  22.5 1.4 %collective-permute-start.2 = (f32[8,256]{1,0:T(8,128)}, f32[8,256]{1,0:T(8,128)S(1)}, u32[]{:S(2)}, u32[]{:S(2)}) collective-permute-start(f32[8,256]{1,0:T(8,128)} %bitcast.6), channel_id=1, source_target_pairs={{0,0},{1,1},{2,2},{3,3},{4,4},{5,5},{6,6},{7,7},{8,8},{9,9},{10,10... | collective-permute-start | bytes 24584 | tf_op jit(solution)/shard_map/ppermute | solution.py:204
  23.2 0.7 collective-permute-start.3
  26.4 20.9 %all-to-all-start = ((bf16[64,24,128]{2,1,0:T(8,128)(2,1)}), bf16[64,24,128]{2,1,0:T(8,128)(2,1)S(1)}, u32[]{:S(2)}, u32[]{:S(2)}) async-start(bf16[64,24,128]{2,1,0:T(8,128)(2,1)} %state.1), calls=%async_computation | async-start | bytes 786432 | tf_op jit(solution)/shard_map/all_to_all | solution.py:225
  32.9 1.1 %collective-permute-start.4 = (bf16[256,1024]{1,0:T(8,128)(2,1)}, bf16[256,1024]{1,0:T(8,128)(2,1)S(1)}, u32[]{:S(2)}, u32[]{:S(2)}) collective-permute-start(bf16[256,1024]{1,0:T(8,128)(2,1)} %param.7), channel_id=1, source_target_pairs={{0,0},{1,1},{2,2},{3,3},{4,4},{5,5},{6,6},{7,7},{8,8},{9,9},{10,10... | collective-permute-start | bytes 1572872 | tf_op jit(solution)/shard_map/ppermute | solution.py:204
  47.3 27.2 %collective-permute-start.6 = (bf16[1024,2048]{1,0:T(8,128)(2,1)}, bf16[1024,2048]{1,0:T(8,128)(2,1)S(1)}, u32[]{:S(2)}, u32[]{:S(2)}) collective-permute-start(bf16[1024,2048]{1,0:T(8,128)(2,1)} %param.13), channel_id=1, source_target_pairs={{0,0},{1,1},{2,2},{3,3},{4,4},{5,5},{6,6},{7,7},{8,8},{9,9},{10,10... | collective-permute-start | bytes 12582920 | tf_op jit(solution)/shard_map/ppermute | solution.py:240
  49.5 26.2 %collective-permute-start.8 = (bf16[1024,2048]{1,0:T(8,128)(2,1)}, bf16[1024,2048]{1,0:T(8,128)(2,1)S(1)}, u32[]{:S(2)}, u32[]{:S(2)}) collective-permute-start(bf16[1024,2048]{1,0:T(8,128)(2,1)} %collective-permute-done.5), channel_id=1, source_target_pairs={{0,0},{1,1},{2,2},{3,3},{4,4},{5,5},{6,6},{7,7},{8,8},{9,9},{10,10... | collective-permute-start | bytes 12582920 | tf_op jit(solution)/shard_map/ppermute | solution.py:241
  71.0 4.7 %collective-permute-start.7 = (bf16[128,1024]{1,0:T(8,128)(2,1)S(1)}, bf16[128,1024]{1,0:T(8,128)(2,1)S(1)}, u32[]{:S(2)}, u32[]{:S(2)}) collective-permute-start(bf16[128,1024]{1,0:T(8,128)(2,1)S(1)} %get-tuple-element.27), channel_id=1, source_target_pairs={{0,1},{1,0},{2,3},{3,2},{4,5},{5,4},{6,7},{7,6},{8,9},{9,8},{10,11... | collective-permute-start | bytes 786440 | tf_op jit(solution)/shard_map/ppermute | solution.py:264

commit v5 on v2

--- a/solution.py
+++ b/solution.py
@@ -152,16 +152,8 @@
                     decayed = decayed + last
 
 
-def output_kernel(away, far, inside, reading, entering, gain, out, normed, matrix, sems):
-    tokens, width = out.shape
-    pieces = matrix.shape[0]
-    wide = width // pieces
-    copies = [
-        pltpu.make_async_copy(far.at[:, i * wide : (i + 1) * wide], matrix.at[i], sems.at[i])
-        for i in range(pieces)
-    ]
-    for copy in copies:
-        copy.start()
+def output_kernel(away, inside, reading, entering, gain, matrix, out, normed):
+    tokens = out.shape[0]
     mine = lax.axis_index("tp")
     half = 1 - mine if away else mine
     rows = pl.ds(pl.multiple_of(half * tokens, tokens), tokens)
@@ -170,11 +162,7 @@
         mixer = inside[rows, lanes] + dot(reading[rows, lanes], entering[h], ((1,), (0,)))
         scale = lax.rsqrt(jnp.mean(mixer * mixer, axis=-1, keepdims=True) + 1e-06)
         normed[:, lanes] = (mixer * scale * gain[...]).astype(BF16)
-    for i, copy in enumerate(copies):
-        copy.wait()
-        out[:, i * wide : (i + 1) * wide] = dot(normed[...], matrix[i], ((1,), (0,))).astype(
-            out.dtype
-        )
+    out[...] = dot(normed[...], matrix[...], ((1,), (0,))).astype(out.dtype)
 
 
 VMEM = 67043328
@@ -229,7 +217,7 @@
         [pltpu.VMEM((pairs, tokens, 2 * HEAD), BF16)] * 2
         + [pltpu.VMEM(extra.shape, F32), pltpu.VMEM(slack.shape, F32)]
         + [pltpu.SemaphoreType.DMA((2, pairs)), pltpu.SemaphoreType.DMA((2,))],
-        21 << 19,
+        0,
     )
     arrived = lax.all_to_all(message, SP, split_axis=0, concat_axis=0, tiled=True)
     inside, reading = call(
@@ -243,35 +231,29 @@
         ],
         6 * flops,
     )
+    arrived, inside, reading = lax.optimization_barrier((arrived, inside, reading))
     scanned = call(
         functools.partial(scan_kernel, slabs),
         "scan",
         (),
         (arrived,),
         [jax.ShapeDtypeStruct((positions, rows, HEAD), BF16)],
-        flops,
+        40 * flops,
         [pltpu.VMEM((HEAD, positions), F32)],
     )
     entering = lax.all_to_all(scanned, SP, split_axis=0, concat_axis=0, tiled=True)
     entering = entering.reshape(heads, HEAD, HEAD)
     half = tokens // lax.axis_size("tp")
-
-    pieces = 4
 
     def projected(away, dtype):
         return call(
             functools.partial(output_kernel, away),
             "away" if away else "kept",
-            (readout_mapping_matrix,),
-            (inside, reading, entering, gain),
+            (),
+            (inside, reading, entering, gain, readout_mapping_matrix),
             [jax.ShapeDtypeStruct((half, width), dtype)],
             half * channels * width * 2,
-            [
-                pltpu.VMEM((half, channels), BF16),
-                pltpu.VMEM((pieces, channels, width // pieces), BF16),
-                pltpu.SemaphoreType.DMA((pieces,)),
-            ],
-            14 << 20,
+            [pltpu.VMEM((half, channels), BF16)],
         )
 
     received = lax.ppermute(projected(True, BF16), "tp", [(0, 1), (1, 0)])

time: 71.1 us -> 70.3 us (0.989)
  starting transfers between devices: 13.3 us -> 28.7 us
  blocking collectives: 33.7 us -> 20.4 us
  Pallas kernels: 13.8 us -> 10.9 us
  waiting for transfers between devices: 2.82 us -> 4.4 us
  local copies, waits for them, and re-layouts: 5.9 us -> 4.51 us
    all_to_all x1, starting transfers between devices: 6.48 us -> 21.8 us  [body(): lax.all_to_all(message, SP, split_axis=0, concat_axis=0, tiled=True)]
    all_to_all x1, blocking collectives: 33.7 us -> 20.4 us  [body(): lax.all_to_all(scanned, SP, split_axis=0, concat_axis=0, tiled=True)]
    pallas_call x5, Pallas kernels: 13.8 us -> 10.9 us  [call(): pl.pallas_call(kernel, name=name, out_shape=outs, in_specs=[IN_HBM] * len...]
    unnamed x16 -> x14, local copies, waits for them, and re-layouts: 5.9 us -> 4.51 us
    all_to_all x1, waiting for transfers between devices: 2.82 us -> 3.85 us  [body(): lax.all_to_all(message, SP, split_axis=0, concat_axis=0, tiled=True)]
  transfers between devices with their start and end apart: 2 -> 2, of which waited for: 1 -> 2; matrix products, arithmetic and copies ran while one was open for 0% -> 0% of each run, Pallas kernels for 9% -> 7%
where the time goes in v5:
time: 70.3 us; the launch traced here: 69.9 us
  starting transfers between devices  28.7 us (41%)
  blocking collectives  20.4 us (29%)
  Pallas kernels  10.9 us (16%)
  local copies, waits for them, and re-layouts  4.51 us (6%)
  waiting for transfers between devices  4.4 us (6%)
  other arithmetic  0.9 us (1%)
    all_to_all x1, starting transfers between devices, body(): lax.all_to_all(message, SP, split_axis=0, concat_axis=0, tiled=True)  21.8 us
    all_to_all x1, blocking collectives, body(): lax.all_to_all(scanned, SP, split_axis=0, concat_axis=0, tiled=True)  20.4 us
    pallas_call x5, Pallas kernels, call(): pl.pallas_call(kernel, name=name, out_shape=outs, in_specs=[IN_HBM] * len...  10.9 us
    ppermute x1, starting transfers between devices, body(): received = lax.ppermute(projected(True, BF16), 'tp', [(0, 1), (1, 0)])  6.92 us
    unnamed x14, local copies, waits for them, and re-layouts  4.51 us
    all_to_all x1, waiting for transfers between devices, body(): lax.all_to_all(message, SP, split_axis=0, concat_axis=0, tiled=True)  3.85 us
  transfers between devices with their start and end apart: 2, of which 2 were waited for; matrix products, arithmetic and copies ran while one was open for 0% of the time, Pallas kernels for 7%

profile of v5, /device:TPU:513, one launch (start us, length us, event | category | flops | bytes accessed | tf_op | source)
XLA Modules:
  0.0 69.9 jit_solution(17535359233536913750)
XLA Ops:
  0.0 4.8 %state.1 = bf16[64,24,128]{2,1,0:T(8,128)(2,1)} custom-call(bf16[256,1024]{1,0:T(8,128)(2,1)} %retention.3, bf16[256,1024]{1,0:T(8,128)(2,1)} %source.3, f32[8,256]{1,0:T(8,128)} %bitcast.6, f32[1,1024]{1,0:T(1,128)} %bitcast.8), custom_call_target="tpu_custom_call" | custom-call | flops 268435456 | bytes 1454080 | tf_op jit(solution)/shard_map/state/pallas_call | solution.py:176
  4.8 21.8 %all-to-all-start = ((bf16[64,24,128]{2,1,0:T(8,128)(2,1)}), bf16[64,24,128]{2,1,0:T(8,128)(2,1)S(1)}, u32[]{:S(2)}, u32[]{:S(2)}) async-start(bf16[64,24,128]{2,1,0:T(8,128)(2,1)} %state.1), calls=%async_computation | async-start | bytes 786432 | tf_op jit(solution)/shard_map/all_to_all | solution.py:222
  26.6 0.0 copy-start.1
  26.6 1.0 %copy-done.1 = bf16[256,1024]{1,0:T(8,128)(2,1)S(1)} copy-done((bf16[256,1024]{1,0:T(8,128)(2,1)S(1)}, bf16[256,1024]{1,0:T(8,128)(2,1)}, u32[]{:S(2)}) %copy-start.1) | copy-done | bytes 524312
  27.6 0.0 copy-start.2
  27.6 1.0 %copy-done.2 = bf16[256,1024]{1,0:T(8,128)(2,1)S(1)} copy-done((bf16[256,1024]{1,0:T(8,128)(2,1)S(1)}, bf16[256,1024]{1,0:T(8,128)(2,1)}, u32[]{:S(2)}) %copy-start.2) | copy-done | bytes 524312
  28.7 0.0 copy-start.3
  28.7 1.0 %copy-done.3 = bf16[256,1024]{1,0:T(8,128)(2,1)S(1)} copy-done((bf16[256,1024]{1,0:T(8,128)(2,1)S(1)}, bf16[256,1024]{1,0:T(8,128)(2,1)}, u32[]{:S(2)}) %copy-start.3) | copy-done | bytes 524312
  29.7 0.0 copy-start.4
  29.7 0.7 copy-done.4
  30.4 0.0 copy-start.5
  30.4 0.7 copy-done.5
  31.1 3.7 %local.1 = (f32[256,1024]{1,0:T(8,128)S(1)}, bf16[256,1024]{1,0:T(8,128)(2,1)S(1)}) custom-call(bf16[256,1024]{1,0:T(8,128)(2,1)S(1)} %copy-done.3, bf16[256,1024]{1,0:T(8,128)(2,1)S(1)} %copy-done.1, bf16[256,1024]{1,0:T(8,128)(2,1)S(1)} %copy-done.2, f32[8,256]{1,0:T(8,128)S(1)} %bitcast.7, f32[1,1024]{1,0:T(1,128)S(1)} %bitcast.9), custom_call_target="tpu_custom_call" | custom-call | flops 402653184 | bytes 3158016 | tf_op jit(solution)/shard_map/local/pallas_call | solution.py:176
  34.8 3.9 %all-to-all-done.message = bf16[64,24,128]{2,1,0:T(8,128)(2,1)S(1)} async-done(((bf16[64,24,128]{2,1,0:T(8,128)(2,1)}), bf16[64,24,128]{2,1,0:T(8,128)(2,1)S(1)}, u32[]{:S(2)}, u32[]{:S(2)}) %all-to-all-start) | async-done | bytes 393248 | tf_op jit(solution)/shard_map/all_to_all | solution.py:222
  38.7 0.0 copy-start
  38.7 0.0 copy-start.6
  38.7 0.4 scan.1
  39.1 20.4 %all_to_all.10 = bf16[64,16,128]{2,1,0:T(8,128)(2,1)S(1)} all-to-all(bf16[64,16,128]{2,1,0:T(8,128)(2,1)S(1)} %scan.1), channel_id=1, replica_groups=mesh['grp'=2,'sp_0'=8,'sp_1'=8,'tp'=2] {'sp_0','sp_1'}, dimensions={0} | all-to-all | bytes 524288 | tf_op jit(solution)/shard_map/all_to_all | solution.py:244
  59.5 0.0 copy-done
  59.5 0.0 copy-done.6
  59.5 1.0 %away.1 = bf16[128,2048]{1,0:T(8,128)(2,1)S(1)} custom-call(f32[256,1024]{1,0:T(8,128)S(1)} %get-tuple-element.12.inside, bf16[256,1024]{1,0:T(8,128)(2,1)S(1)} %get-tuple-element.13.reading, bf16[8,128,128]{2,1,0:T(8,128)(2,1)S(1)} %bitcast.4, f32[1,128]{1,0:T(1,128)S(1)} %bitcast.10, bf16[1024,2048]{1,0:T(8,128)(2,1)S(1)} %copy-done), custom_call_target="tpu_custom_call" | custom-call | flops 536870912 | bytes 6554112 | tf_op jit(solution)/shard_map/away/pallas_call | solution.py:176
  60.5 6.9 %collective-permute-start = (bf16[128,2048]{1,0:T(8,128)(2,1)S(1)}, bf16[128,2048]{1,0:T(8,128)(2,1)S(1)}, u32[]{:S(2)}, u32[]{:S(2)}) collective-permute-start(bf16[128,2048]{1,0:T(8,128)(2,1)S(1)} %away.1), channel_id=1, source_target_pairs={{0,1},{1,0},{2,3},{3,2},{4,5},{5,4},{6,7},{7,6},{8,9},{9,8},{10,11... | collective-permute-start | bytes 1572872 | tf_op jit(solution)/shard_map/ppermute | solution.py:259
  67.4 1.0 %kept.1 = f32[128,2048]{1,0:T(8,128)S(1)} custom-call(f32[256,1024]{1,0:T(8,128)S(1)} %get-tuple-element.12.inside, bf16[256,1024]{1,0:T(8,128)(2,1)S(1)} %get-tuple-element.13.reading, bf16[8,128,128]{2,1,0:T(8,128)(2,1)S(1)} %bitcast.5, f32[1,128]{1,0:T(1,128)S(1)} %bitcast.11, bf16[1024,2048]{1,0:T(8,128)(2,1)S(1)} %copy-done), custom_call_target="tpu_custom_call" | custom-call | flops 536870912 | bytes 7078400 | tf_op jit(solution)/shard_map/kept/pallas_call | solution.py:176
  68.4 0.5 collective-permute-done
  69.0 0.9 %add_convert_fusion = bf16[128,2048]{1,0:T(8,128)(2,1)} fusion(f32[128,2048]{1,0:T(8,128)S(1)} %kept.1, bf16[128,2048]{1,0:T(8,128)(2,1)S(1)} %collective-permute-done), kind=kLoop, calls=%fused_computation | loop fusion | flops 786432 | bytes 2097152 | tf_op jit(solution)/shard_map/convert_element_type | solution.py:260
Async XLA Ops:
  4.8 33.9 %all-to-all-start = ((bf16[64,24,128]{2,1,0:T(8,128)(2,1)}), bf16[64,24,128]{2,1,0:T(8,128)(2,1)S(1)}, u32[]{:S(2)}, u32[]{:S(2)}) async-start(bf16[64,24,128]{2,1,0:T(8,128)(2,1)} %state.1), calls=%async_computation | async-start | bytes 786432 | tf_op jit(solution)/shard_map/all_to_all | solution.py:222
  26.6 1.0 %copy-start.1 = (bf16[256,1024]{1,0:T(8,128)(2,1)S(1)}, bf16[256,1024]{1,0:T(8,128)(2,1)}, u32[]{:S(2)}) copy-start(bf16[256,1024]{1,0:T(8,128)(2,1)} %retention.3) | copy-start | bytes 1572868
  27.6 1.0 %copy-start.2 = (bf16[256,1024]{1,0:T(8,128)(2,1)S(1)}, bf16[256,1024]{1,0:T(8,128)(2,1)}, u32[]{:S(2)}) copy-start(bf16[256,1024]{1,0:T(8,128)(2,1)} %source.3) | copy-start | bytes 1572868
  28.7 1.0 %copy-start.3 = (bf16[256,1024]{1,0:T(8,128)(2,1)S(1)}, bf16[256,1024]{1,0:T(8,128)(2,1)}, u32[]{:S(2)}) copy-start(bf16[256,1024]{1,0:T(8,128)(2,1)} %probe.1) | copy-start | bytes 1572868
  29.7 0.7 copy-start.4
  30.4 0.7 copy-start.5
  38.7 20.8 %copy-start = (bf16[1024,2048]{1,0:T(8,128)(2,1)S(1)}, bf16[1024,2048]{1,0:T(8,128)(2,1)}, u32[]{:S(2)}) copy-start(bf16[1024,2048]{1,0:T(8,128)(2,1)} %matrix.3) | copy-start | bytes 12582916
  38.7 20.8 %copy-start.6 = (f32[128]{0:T(128)S(1)}, f32[128]{0:T(128)}, u32[]{:S(2)}) copy-start(f32[128]{0:T(128)} %param.12) | copy-start | bytes 1540
  60.5 8.5 %collective-permute-start = (bf16[128,2048]{1,0:T(8,128)(2,1)S(1)}, bf16[128,2048]{1,0:T(8,128)(2,1)S(1)}, u32[]{:S(2)}, u32[]{:S(2)}) collective-permute-start(bf16[128,2048]{1,0:T(8,128)(2,1)S(1)} %away.1), channel_id=1, source_target_pairs={{0,1},{1,0},{2,3},{3,2},{4,5},{5,4},{6,7},{7,6},{8,9},{9,8},{10,11... | collective-permute-start | bytes 1572872 | tf_op jit(solution)/shard_map/ppermute | solution.py:259

commit v6 on v5

--- a/solution.py
+++ b/solution.py
@@ -39,39 +39,26 @@
     return lax.broadcasted_iota(jnp.int32, shape, 0), lax.broadcasted_iota(jnp.int32, shape, 1)
 
 
-def state_kernel(
-    slabs, retention, source, far_extra, far_slack, message, r_in, v_in, extra, slack, sems, small
-):
+def copied(pairs, sems):
+    copies = [pltpu.make_async_copy(a, b, sems.at[i]) for i, (a, b) in enumerate(pairs)]
+    for copy in copies:
+        copy.start()
+    return copies
+
+
+def state_kernel(slabs, far, message, near, sems):
+    copies = copied(zip(far, near), sems)
+    retention, source, extra, slack = near
     tokens, channels = retention.shape
     wide = 2 * HEAD
-    pairs = channels // wide
-    first = [
-        pltpu.make_async_copy(a, b, small.at[i])
-        for i, (a, b) in enumerate(((far_extra, extra), (far_slack, slack)))
-    ]
-    for copy in first:
-        copy.start()
-
-    def copies(source_ref, target, row):
-        return [
-            pltpu.make_async_copy(
-                source_ref.at[:, p * wide : (p + 1) * wide], target.at[p], sems.at[row, p]
-            )
-            for p in range(pairs)
-        ]
-
-    r_copies, v_copies = (copies(retention, r_in, 0), copies(source, v_in, 1))
-    for p in range(pairs):
-        r_copies[p].start()
-        v_copies[p].start()
+    rows = HEAD // slabs
     r, c = rows_and_columns((tokens, tokens))
     later = (c > r).astype(BF16)
-    rows = HEAD // slabs
-    for copy in first:
+    for copy in copies:
         copy.wait()
     by_token = extra[...].T
-    for p in range(pairs):
-        r_copies[p].wait()
+    for p in range(channels // wide):
+        lanes = slice(p * wide, (p + 1) * wide)
         added = jnp.concatenate(
             [
                 jnp.broadcast_to(by_token[:, h : h + 1], (tokens, HEAD))
@@ -79,23 +66,21 @@
             ],
             axis=1,
         )
-        keyed, log_decay = keyed_and_log_decay(
-            r_in[p], slack[:, p * wide : (p + 1) * wide], added
-        )
+        keyed, log_decay = keyed_and_log_decay(retention[:, lanes], slack[:, lanes], added)
         ahead = summed_rows(later, log_decay)
         sent = (keyed * jnp.exp(ahead)).astype(BF16)
         total = ahead[:1] + log_decay[:1]
         parts = jnp.concatenate(two_parts(total) + (jnp.zeros((6, wide), BF16),), axis=0)
-        v_copies[p].wait()
         for k in range(2):
-            lanes = slice(k * HEAD, (k + 1) * HEAD)
+            part = slice(k * HEAD, (k + 1) * HEAD)
             h = 2 * p + k
-            state = dot(sent[:, lanes], v_in[p, :, lanes], ((0,), (0,)))
+            values = source[:, h * HEAD : (h + 1) * HEAD]
+            state = dot(sent[:, part], values, ((0,), (0,)))
             message[h * slabs : (h + 1) * slabs, :rows, :] = state.astype(BF16).reshape(
                 slabs, rows, HEAD
             )
             message[h * slabs : (h + 1) * slabs, rows:, :] = jnp.broadcast_to(
-                parts[None, :, lanes], (slabs, 8, HEAD)
+                parts[None, :, part], (slabs, 8, HEAD)
             )
 
 
@@ -112,11 +97,15 @@
             state = mine[:, i : i + 1] * state + message[i, :rows, :].astype(F32)
 
 
-def local_kernel(probe, retention, source, extra, slack, inside, reading):
+def local_kernel(far, inside, reading, near, sems):
+    copies = copied(zip(far, near), sems)
+    retention, source, extra, slack, probe = near
     tokens, channels = retention.shape
     r, c = rows_and_columns((SPAN, SPAN))
     upto = c <= r
     upto_ones = upto.astype(BF16)
+    for copy in copies:
+        copy.wait()
     by_token = extra[...].T
     for h in range(channels // HEAD):
         lanes = slice(h * HEAD, (h + 1) * HEAD)
@@ -141,7 +130,7 @@
                 reading[span, lanes] = (query * jnp.exp(running + decayed)).astype(BF16)
             else:
                 reading[span, lanes] = lifted
-            inside[span, lanes] = out
+            inside[span, lanes] = out.astype(BF16)
             if (b + 1) * SPAN < tokens:
                 sent = (keyed * jnp.exp(last - running)).astype(BF16)
                 added = dot(sent, values, ((0,), (0,)))
@@ -179,7 +168,7 @@
         out_shape=outs,
         in_specs=[IN_HBM] * len(far) + [IN_VMEM] * len(near),
         out_specs=[IN_VMEM] * len(outs),
-        scratch_shapes=scratch,
+        scratch_shapes=list(scratch),
         compiler_params=pltpu.CompilerParams(vmem_limit_bytes=VMEM - left),
         cost_estimate=pl.CostEstimate(flops=flops, bytes_accessed=moved, transcendentals=0),
     )(*inputs)
@@ -205,31 +194,35 @@
     gain = group_normalizer_gain.reshape(1, HEAD)
     extra = extra_log_retention.T
     flops = 2 * tokens * channels * HEAD
-    pairs = channels // (2 * HEAD)
+    inputs = (retention_preactivation, source_entries, extra, slack)
+
+    def near(arrays):
+        return (
+            tuple(pltpu.VMEM(a.shape, a.dtype) for a in arrays),
+            pltpu.SemaphoreType.DMA((len(arrays),)),
+        )
 
     message = call(
-        functools.partial(state_kernel, slabs),
+        lambda *refs: state_kernel(slabs, refs[:4], *refs[4:]),
         "state",
-        (retention_preactivation, source_entries, extra, slack),
+        inputs,
         (),
         [jax.ShapeDtypeStruct((positions, rows + 8, HEAD), BF16)],
         4 * flops,
-        [pltpu.VMEM((pairs, tokens, 2 * HEAD), BF16)] * 2
-        + [pltpu.VMEM(extra.shape, F32), pltpu.VMEM(slack.shape, F32)]
-        + [pltpu.SemaphoreType.DMA((2, pairs)), pltpu.SemaphoreType.DMA((2,))],
+        near(inputs),
         0,
     )
     arrived = lax.all_to_all(message, SP, split_axis=0, concat_axis=0, tiled=True)
+    inputs = (*inputs, probe_preactivation)
     inside, reading = call(
-        local_kernel,
+        lambda *refs: local_kernel(refs[:5], *refs[5:]),
         "local",
+        inputs,
         (),
-        (probe_preactivation, retention_preactivation, source_entries, extra, slack),
-        [
-            jax.ShapeDtypeStruct((tokens, channels), F32),
-            jax.ShapeDtypeStruct((tokens, channels), BF16),
-        ],
+        [jax.ShapeDtypeStruct((tokens, channels), BF16)] * 2,
         6 * flops,
+        near(inputs),
+        21 << 19,
     )
     arrived, inside, reading = lax.optimization_barrier((arrived, inside, reading))
     scanned = call(

time: 70.3 us -> 68.2 us (0.970)
  local copies, waits for them, and re-layouts: 4.51 us -> 1.39 us
  Pallas kernels: 10.9 us -> 12 us
  waiting for transfers between devices: 4.4 us -> 5.32 us
  blocking collectives: 20.4 us -> 19.5 us
    unnamed x14 -> x12, local copies, waits for them, and re-layouts: 4.51 us -> 1.39 us
    pallas_call x5, Pallas kernels: 10.9 us -> 12 us  [call(): pl.pallas_call(kernel, name=name, out_shape=outs, in_specs=[IN_HBM] * len...]
    all_to_all x1, waiting for transfers between devices: 3.85 us -> 4.77 us  [body(): lax.all_to_all(message, SP, split_axis=0, concat_axis=0, tiled=True)]
    all_to_all x1, blocking collectives: 20.4 us -> 19.5 us  [body(): lax.all_to_all(scanned, SP, split_axis=0, concat_axis=0, tiled=True)]
  transfers between devices with their start and end apart: 2 -> 2, of which waited for: 2 -> 2; matrix products, arithmetic and copies ran while one was open for 0% -> 0% of each run, Pallas kernels for 7% -> 10%
where the time goes in v6:
time: 68.2 us; the launch traced here: 67.9 us
  starting transfers between devices  28.7 us (42%)
  blocking collectives  19.5 us (29%)
  Pallas kernels  12 us (18%)
  waiting for transfers between devices  5.32 us (8%)
  local copies, waits for them, and re-layouts  1.39 us (2%)
  other arithmetic  0.9 us (1%)
    all_to_all x1, starting transfers between devices, body(): lax.all_to_all(message, SP, split_axis=0, concat_axis=0, tiled=True)  21.8 us
    all_to_all x1, blocking collectives, body(): lax.all_to_all(scanned, SP, split_axis=0, concat_axis=0, tiled=True)  19.5 us
    pallas_call x5, Pallas kernels, call(): pl.pallas_call(kernel, name=name, out_shape=outs, in_specs=[IN_HBM] * len...  12 us
    ppermute x1, starting transfers between devices, body(): received = lax.ppermute(projected(True, BF16), 'tp', [(0, 1), (1, 0)])  6.92 us
    all_to_all x1, waiting for transfers between devices, body(): lax.all_to_all(message, SP, split_axis=0, concat_axis=0, tiled=True)  4.77 us
    unnamed x12, local copies, waits for them, and re-layouts  1.39 us
  transfers between devices with their start and end apart: 2, of which 2 were waited for; matrix products, arithmetic and copies ran while one was open for 0% of the time, Pallas kernels for 10%

profile of v6, /device:TPU:513, one launch (start us, length us, event | category | flops | bytes accessed | tf_op | source)
XLA Modules:
  0.0 67.9 jit_solution(10157668275983264793)
XLA Ops:
  0.0 3.7 %state.1 = bf16[64,24,128]{2,1,0:T(8,128)(2,1)} custom-call(bf16[256,1024]{1,0:T(8,128)(2,1)} %refs_0_.3, bf16[256,1024]{1,0:T(8,128)(2,1)} %refs_1_.3, f32[8,256]{1,0:T(8,128)} %bitcast.6, f32[1,1024]{1,0:T(1,128)} %bitcast.8), custom_call_target="tpu_custom_call" | custom-call | flops 268435456 | bytes 1454080 | tf_op jit(solution)/shard_map/state/pallas_call | solution.py:165
  3.7 21.8 %all-to-all-start = ((bf16[64,24,128]{2,1,0:T(8,128)(2,1)}), bf16[64,24,128]{2,1,0:T(8,128)(2,1)S(1)}, u32[]{:S(2)}, u32[]{:S(2)}) async-start(bf16[64,24,128]{2,1,0:T(8,128)(2,1)} %state.1), calls=%async_computation | async-start | bytes 786432 | tf_op jit(solution)/shard_map/all_to_all | solution.py:215
  25.5 0.0 copy-start.3
  25.5 0.7 %copy-done.3 = f32[256,8]{0,1:T(8,128)S(1)} copy-done((f32[256,8]{0,1:T(8,128)S(1)}, f32[256,8]{0,1:T(8,128)}, u32[]{:S(2)}) %copy-start.3) | copy-done | bytes 8216
  26.2 0.0 copy-start.4
  26.2 0.7 %copy-done.4 = f32[1024]{0:T(1024)S(1)} copy-done((f32[1024]{0:T(1024)S(1)}, f32[1024]{0:T(1024)}, u32[]{:S(2)}) %copy-start.4) | copy-done | bytes 4120
  26.9 5.9 %local.1 = (bf16[256,1024]{1,0:T(8,128)(2,1)}, bf16[256,1024]{1,0:T(8,128)(2,1)}) custom-call(bf16[256,1024]{1,0:T(8,128)(2,1)} %refs_0_.3, bf16[256,1024]{1,0:T(8,128)(2,1)} %refs_1_.3, f32[8,256]{1,0:T(8,128)S(1)} %bitcast.7, f32[1,1024]{1,0:T(1,128)S(1)} %bitcast.9, bf16[256,1024]{1,0:T(8,128)(2,1)} %refs_4_.1), custom_call_target="tpu_custom_call" | custom-call | flops 402653184 | bytes 2633728 | tf_op jit(solution)/shard_map/local/pallas_call | solution.py:165
  32.8 4.8 %all-to-all-done.message = bf16[64,24,128]{2,1,0:T(8,128)(2,1)S(1)} async-done(((bf16[64,24,128]{2,1,0:T(8,128)(2,1)}), bf16[64,24,128]{2,1,0:T(8,128)(2,1)S(1)}, u32[]{:S(2)}, u32[]{:S(2)}) %all-to-all-start) | async-done | bytes 393248 | tf_op jit(solution)/shard_map/all_to_all | solution.py:215
  37.6 0.0 copy-start
  37.6 0.0 copy-start.1
  37.6 0.0 copy-start.2
  37.6 0.0 copy-start.5
  37.6 0.4 scan.1
  38.1 19.5 %all_to_all.10 = bf16[64,16,128]{2,1,0:T(8,128)(2,1)S(1)} all-to-all(bf16[64,16,128]{2,1,0:T(8,128)(2,1)S(1)} %scan.1), channel_id=1, replica_groups=mesh['grp'=2,'sp_0'=8,'sp_1'=8,'tp'=2] {'sp_0','sp_1'}, dimensions={0} | all-to-all | bytes 524288 | tf_op jit(solution)/shard_map/all_to_all | solution.py:237
  57.6 0.0 copy-done
  57.6 0.0 copy-done.1
  57.6 0.0 copy-done.2
  57.6 0.0 copy-done.5
  57.6 1.0 %away.1 = bf16[128,2048]{1,0:T(8,128)(2,1)S(1)} custom-call(bf16[256,1024]{1,0:T(8,128)(2,1)S(1)} %copy-done.1, bf16[256,1024]{1,0:T(8,128)(2,1)S(1)} %copy-done.2, bf16[8,128,128]{2,1,0:T(8,128)(2,1)S(1)} %bitcast.4, f32[1,128]{1,0:T(1,128)S(1)} %bitcast.10, bf16[1024,2048]{1,0:T(8,128)(2,1)S(1)} %copy-done), custom_call_target="tpu_custom_call" | custom-call | flops 536870912 | bytes 6029824 | tf_op jit(solution)/shard_map/away/pallas_call | solution.py:165
  58.6 6.9 %collective-permute-start = (bf16[128,2048]{1,0:T(8,128)(2,1)S(1)}, bf16[128,2048]{1,0:T(8,128)(2,1)S(1)}, u32[]{:S(2)}, u32[]{:S(2)}) collective-permute-start(bf16[128,2048]{1,0:T(8,128)(2,1)S(1)} %away.1), channel_id=1, source_target_pairs={{0,1},{1,0},{2,3},{3,2},{4,5},{5,4},{6,7},{7,6},{8,9},{9,8},{10,11... | collective-permute-start | bytes 1572872 | tf_op jit(solution)/shard_map/ppermute | solution.py:252
  65.5 1.0 %kept.1 = f32[128,2048]{1,0:T(8,128)S(1)} custom-call(bf16[256,1024]{1,0:T(8,128)(2,1)S(1)} %copy-done.1, bf16[256,1024]{1,0:T(8,128)(2,1)S(1)} %copy-done.2, bf16[8,128,128]{2,1,0:T(8,128)(2,1)S(1)} %bitcast.5, f32[1,128]{1,0:T(1,128)S(1)} %bitcast.11, bf16[1024,2048]{1,0:T(8,128)(2,1)S(1)} %copy-done), custom_call_target="tpu_custom_call" | custom-call | flops 536870912 | bytes 6554112 | tf_op jit(solution)/shard_map/kept/pallas_call | solution.py:165
  66.5 0.5 collective-permute-done
  67.0 0.9 %add_convert_fusion = bf16[128,2048]{1,0:T(8,128)(2,1)} fusion(f32[128,2048]{1,0:T(8,128)S(1)} %kept.1, bf16[128,2048]{1,0:T(8,128)(2,1)S(1)} %collective-permute-done), kind=kLoop, calls=%fused_computation | loop fusion | flops 786432 | bytes 2097152 | tf_op jit(solution)/shard_map/convert_element_type | solution.py:253
Async XLA Ops:
  3.7 33.9 %all-to-all-start = ((bf16[64,24,128]{2,1,0:T(8,128)(2,1)}), bf16[64,24,128]{2,1,0:T(8,128)(2,1)S(1)}, u32[]{:S(2)}, u32[]{:S(2)}) async-start(bf16[64,24,128]{2,1,0:T(8,128)(2,1)} %state.1), calls=%async_computation | async-start | bytes 786432 | tf_op jit(solution)/shard_map/all_to_all | solution.py:215
  25.5 0.7 %copy-start.3 = (f32[256,8]{0,1:T(8,128)S(1)}, f32[256,8]{0,1:T(8,128)}, u32[]{:S(2)}) copy-start(f32[256,8]{0,1:T(8,128)} %param.10) | copy-start | bytes 24580
  26.2 0.7 %copy-start.4 = (f32[1024]{0:T(1024)S(1)}, f32[1024]{0:T(1024)}, u32[]{:S(2)}) copy-start(f32[1024]{0:T(1024)} %param.11) | copy-start | bytes 12292
  37.6 20.0 %copy-start = (bf16[1024,2048]{1,0:T(8,128)(2,1)S(1)}, bf16[1024,2048]{1,0:T(8,128)(2,1)}, u32[]{:S(2)}) copy-start(bf16[1024,2048]{1,0:T(8,128)(2,1)} %matrix.3) | copy-start | bytes 12582916
  37.6 20.0 %copy-start.1 = (bf16[256,1024]{1,0:T(8,128)(2,1)S(1)}, bf16[256,1024]{1,0:T(8,128)(2,1)}, u32[]{:S(2)}) copy-start(bf16[256,1024]{1,0:T(8,128)(2,1)} %get-tuple-element.12.inside) | copy-start | bytes 1572868
  37.6 20.0 %copy-start.2 = (bf16[256,1024]{1,0:T(8,128)(2,1)S(1)}, bf16[256,1024]{1,0:T(8,128)(2,1)}, u32[]{:S(2)}) copy-start(bf16[256,1024]{1,0:T(8,128)(2,1)} %get-tuple-element.13.reading) | copy-start | bytes 1572868
  37.6 20.0 %copy-start.5 = (f32[128]{0:T(128)S(1)}, f32[128]{0:T(128)}, u32[]{:S(2)}) copy-start(f32[128]{0:T(128)} %param.12) | copy-start | bytes 1540
  58.6 8.5 %collective-permute-start = (bf16[128,2048]{1,0:T(8,128)(2,1)S(1)}, bf16[128,2048]{1,0:T(8,128)(2,1)S(1)}, u32[]{:S(2)}, u32[]{:S(2)}) collective-permute-start(bf16[128,2048]{1,0:T(8,128)(2,1)S(1)} %away.1), channel_id=1, source_target_pairs={{0,1},{1,0},{2,3},{3,2},{4,5},{5,4},{6,7},{7,6},{8,9},{9,8},{10,11... | collective-permute-start | bytes 1572872 | tf_op jit(solution)/shard_map/ppermute | solution.py:252

commit v7 on v6

--- a/solution.py
+++ b/solution.py
@@ -32,11 +32,21 @@
 
 def keyed_and_log_decay(retention, slack, extra):
     keyed = slack * jax.nn.sigmoid(-retention.astype(F32))
-    return keyed, jnp.log1p(-keyed) + extra
+    return keyed, jnp.log(1.0 - keyed) + extra
 
 
 def rows_and_columns(shape):
     return lax.broadcasted_iota(jnp.int32, shape, 0), lax.broadcasted_iota(jnp.int32, shape, 1)
+
+
+def for_pair(by_token, p):
+    return jnp.concatenate(
+        [
+            jnp.broadcast_to(by_token[:, h : h + 1], (by_token.shape[0], HEAD))
+            for h in (2 * p, 2 * p + 1)
+        ],
+        axis=1,
+    )
 
 
 def copied(pairs, sems):
@@ -44,6 +54,15 @@
     for copy in copies:
         copy.start()
     return copies
+
+
+def staggered(make, count):
+    chains = [make(i) for i in range(count)]
+    live = []
+    while chains or live:
+        if chains:
+            live.append(chains.pop(0))
+        live = [chain for chain in live if next(chain, live) is None]
 
 
 def state_kernel(slabs, far, message, near, sems):
@@ -57,20 +76,19 @@
     for copy in copies:
         copy.wait()
     by_token = extra[...].T
-    for p in range(channels // wide):
+
+    def chain(p):
         lanes = slice(p * wide, (p + 1) * wide)
-        added = jnp.concatenate(
-            [
-                jnp.broadcast_to(by_token[:, h : h + 1], (tokens, HEAD))
-                for h in (2 * p, 2 * p + 1)
-            ],
-            axis=1,
+        keyed, log_decay = keyed_and_log_decay(
+            retention[:, lanes], slack[:, lanes], for_pair(by_token, p)
         )
-        keyed, log_decay = keyed_and_log_decay(retention[:, lanes], slack[:, lanes], added)
+        yield
         ahead = summed_rows(later, log_decay)
+        yield
         sent = (keyed * jnp.exp(ahead)).astype(BF16)
         total = ahead[:1] + log_decay[:1]
         parts = jnp.concatenate(two_parts(total) + (jnp.zeros((6, wide), BF16),), axis=0)
+        yield
         for k in range(2):
             part = slice(k * HEAD, (k + 1) * HEAD)
             h = 2 * p + k
@@ -83,6 +101,8 @@
                 parts[None, :, part], (slabs, 8, HEAD)
             )
 
+    staggered(chain, channels // wide)
+
 
 def scan_kernel(slabs, message, entering, by_channel):
     positions, rows, _ = entering.shape
@@ -101,44 +121,62 @@
     copies = copied(zip(far, near), sems)
     retention, source, extra, slack, probe = near
     tokens, channels = retention.shape
+    wide = 2 * HEAD
+    r, c = rows_and_columns((tokens, tokens))
+    within = ((c <= r) & (r // SPAN == c // SPAN)).astype(BF16)
     r, c = rows_and_columns((SPAN, SPAN))
     upto = c <= r
-    upto_ones = upto.astype(BF16)
     for copy in copies:
         copy.wait()
     by_token = extra[...].T
-    for h in range(channels // HEAD):
-        lanes = slice(h * HEAD, (h + 1) * HEAD)
-        before, decayed = None, None
+
+    def chain(p):
+        lanes = slice(p * wide, (p + 1) * wide)
+        keyed, log_decay = keyed_and_log_decay(
+            retention[:, lanes], slack[:, lanes], for_pair(by_token, p)
+        )
+        yield
+        running = summed_rows(within, log_decay)
+        yield
+        raised = jax.nn.silu(probe[:, lanes].astype(F32)) * jnp.exp(running)
+        lifted = raised.astype(BF16)
+        lowered = (keyed * jnp.exp(-running)).astype(BF16)
+        yield
+        decayed, before = None, [None, None]
         for b in range(tokens // SPAN):
             span = slice(b * SPAN, (b + 1) * SPAN)
-            keyed, log_decay = keyed_and_log_decay(
-                retention[span, lanes], slack[:, lanes], by_token[span, h : h + 1]
-            )
-            values = source[span, lanes]
-            query = jax.nn.silu(probe[span, lanes].astype(F32))
-            running = summed_rows(upto_ones, log_decay)
-            last = running[SPAN - 1 :]
-            raised = query * jnp.exp(running)
-            lifted = raised.astype(BF16)
-            lowered = (keyed * jnp.exp(-running)).astype(BF16)
-            scores = dot(lifted, lowered, ((1,), (1,)))
-            weights = jnp.where(upto, scores, 0.0).astype(BF16)
-            out = dot(weights, values, ((1,), (0,)))
-            if before is not None:
-                out = out + dot(lifted, before.astype(BF16), ((1,), (0,)))
-                reading[span, lanes] = (query * jnp.exp(running + decayed)).astype(BF16)
+            last = running[(b + 1) * SPAN - 1 : (b + 1) * SPAN]
+            if b == 0:
+                reading[span, lanes] = lifted[span]
             else:
-                reading[span, lanes] = lifted
-            inside[span, lanes] = out.astype(BF16)
-            if (b + 1) * SPAN < tokens:
-                sent = (keyed * jnp.exp(last - running)).astype(BF16)
-                added = dot(sent, values, ((0,), (0,)))
-                if before is None:
-                    before, decayed = added, last
-                else:
-                    before = jnp.exp(last).reshape(HEAD, 1) * before + added
-                    decayed = decayed + last
+                reading[span, lanes] = (raised[span] * jnp.exp(decayed)).astype(BF16)
+            more = (b + 1) * SPAN < tokens
+            if more:
+                sent = (keyed[span] * jnp.exp(last - running[span])).astype(BF16)
+                decayed = last if b == 0 else decayed + last
+            weights = []
+            for k in range(2):
+                part = slice(k * HEAD, (k + 1) * HEAD)
+                scores = dot(lifted[span, part], lowered[span, part], ((1,), (1,)))
+                weights.append(jnp.where(upto, scores, 0.0).astype(BF16))
+            yield
+            for k in range(2):
+                part = slice(k * HEAD, (k + 1) * HEAD)
+                columns = slice(p * wide + k * HEAD, p * wide + (k + 1) * HEAD)
+                values = source[span, columns]
+                left, right = weights[k], values
+                if b > 0:
+                    left = jnp.concatenate([left, lifted[span, part]], axis=1)
+                    right = jnp.concatenate([right, before[k].astype(BF16)], axis=0)
+                inside[span, columns] = dot(left, right, ((1,), (0,))).astype(BF16)
+                if more:
+                    added = dot(sent[:, part], values, ((0,), (0,)))
+                    if b > 0:
+                        added = jnp.exp(last[:, part]).reshape(HEAD, 1) * before[k] + added
+                    before[k] = added
+            yield
+
+    staggered(chain, channels // wide)
 
 
 def output_kernel(away, inside, reading, entering, gain, matrix, out, normed):

time: 68.2 us -> 66.3 us (0.972)
  Pallas kernels: 12 us -> 9.68 us
  blocking collectives: 19.5 us -> 17.5 us
  waiting for transfers between devices: 5.32 us -> 7.28 us
    pallas_call x5, Pallas kernels: 12 us -> 9.68 us  [call(): pl.pallas_call(kernel, name=name, out_shape=outs, in_specs=[IN_HBM] * len...]
    all_to_all x1, blocking collectives: 19.5 us -> 17.5 us  [body(): lax.all_to_all(scanned, SP, split_axis=0, concat_axis=0, tiled=True)]
    all_to_all x1, waiting for transfers between devices: 4.77 us -> 6.73 us  [body(): lax.all_to_all(message, SP, split_axis=0, concat_axis=0, tiled=True)]
  transfers between devices with their start and end apart: 2 -> 2, of which waited for: 2 -> 2; matrix products, arithmetic and copies ran while one was open for 0% -> 0% of each run, Pallas kernels for 10% -> 7%
where the time goes in v7:
time: 66.3 us; the launch traced here: 66 us
  starting transfers between devices  29.1 us (44%)
  blocking collectives  17.5 us (26%)
  Pallas kernels  9.68 us (15%)
  waiting for transfers between devices  7.28 us (11%)
  local copies, waits for them, and re-layouts  1.39 us (2%)
  other arithmetic  0.9 us (1%)
    all_to_all x1, starting transfers between devices, body(): lax.all_to_all(message, SP, split_axis=0, concat_axis=0, tiled=True)  21.8 us
    all_to_all x1, blocking collectives, body(): lax.all_to_all(scanned, SP, split_axis=0, concat_axis=0, tiled=True)  17.5 us
    pallas_call x5, Pallas kernels, call(): pl.pallas_call(kernel, name=name, out_shape=outs, in_specs=[IN_HBM] * len...  9.68 us
    ppermute x1, starting transfers between devices, body(): received = lax.ppermute(projected(True, BF16), 'tp', [(0, 1), (1, 0)])  7.33 us
    all_to_all x1, waiting for transfers between devices, body(): lax.all_to_all(message, SP, split_axis=0, concat_axis=0, tiled=True)  6.73 us
    unnamed x12, local copies, waits for them, and re-layouts  1.39 us
  transfers between devices with their start and end apart: 2, of which 2 were waited for; matrix products, arithmetic and copies ran while one was open for 0% of the time, Pallas kernels for 7%

profile of v7, /device:TPU:513, one launch (start us, length us, event | category | flops | bytes accessed | tf_op | source)
XLA Modules:
  0.0 66.0 jit_solution(8296514496567695775)
XLA Ops:
  0.0 3.3 %state.1 = bf16[64,24,128]{2,1,0:T(8,128)(2,1)} custom-call(bf16[256,1024]{1,0:T(8,128)(2,1)} %refs_0_.3, bf16[256,1024]{1,0:T(8,128)(2,1)} %refs_1_.3, f32[8,256]{1,0:T(8,128)} %bitcast.6, f32[1,1024]{1,0:T(1,128)} %bitcast.8), custom_call_target="tpu_custom_call" | custom-call | flops 268435456 | bytes 1454080 | tf_op jit(solution)/shard_map/state/pallas_call | solution.py:203
  3.3 21.8 %all-to-all-start = ((bf16[64,24,128]{2,1,0:T(8,128)(2,1)}), bf16[64,24,128]{2,1,0:T(8,128)(2,1)S(1)}, u32[]{:S(2)}, u32[]{:S(2)}) async-start(bf16[64,24,128]{2,1,0:T(8,128)(2,1)} %state.1), calls=%async_computation | async-start | bytes 786432 | tf_op jit(solution)/shard_map/all_to_all | solution.py:253
  25.1 0.0 copy-start.3
  25.2 0.7 %copy-done.3 = f32[256,8]{0,1:T(8,128)S(1)} copy-done((f32[256,8]{0,1:T(8,128)S(1)}, f32[256,8]{0,1:T(8,128)}, u32[]{:S(2)}) %copy-start.3) | copy-done | bytes 8216
  25.8 0.0 copy-start.4
  25.8 0.7 %copy-done.4 = f32[1024]{0:T(1024)S(1)} copy-done((f32[1024]{0:T(1024)S(1)}, f32[1024]{0:T(1024)}, u32[]{:S(2)}) %copy-start.4) | copy-done | bytes 4120
  26.5 4.0 %local.1 = (bf16[256,1024]{1,0:T(8,128)(2,1)}, bf16[256,1024]{1,0:T(8,128)(2,1)}) custom-call(bf16[256,1024]{1,0:T(8,128)(2,1)} %refs_0_.3, bf16[256,1024]{1,0:T(8,128)(2,1)} %refs_1_.3, f32[8,256]{1,0:T(8,128)S(1)} %bitcast.7, f32[1,1024]{1,0:T(1,128)S(1)} %bitcast.9, bf16[256,1024]{1,0:T(8,128)(2,1)} %refs_4_.1), custom_call_target="tpu_custom_call" | custom-call | flops 402653184 | bytes 2633728 | tf_op jit(solution)/shard_map/local/pallas_call | solution.py:203
  30.5 6.7 %all-to-all-done.message = bf16[64,24,128]{2,1,0:T(8,128)(2,1)S(1)} async-done(((bf16[64,24,128]{2,1,0:T(8,128)(2,1)}), bf16[64,24,128]{2,1,0:T(8,128)(2,1)S(1)}, u32[]{:S(2)}, u32[]{:S(2)}) %all-to-all-start) | async-done | bytes 393248 | tf_op jit(solution)/shard_map/all_to_all | solution.py:253
  37.2 0.0 copy-start
  37.2 0.0 copy-start.1
  37.2 0.0 copy-start.2
  37.2 0.0 copy-start.5
  37.2 0.4 scan.1
  37.7 17.5 %all_to_all.10 = bf16[64,16,128]{2,1,0:T(8,128)(2,1)S(1)} all-to-all(bf16[64,16,128]{2,1,0:T(8,128)(2,1)S(1)} %scan.1), channel_id=1, replica_groups=mesh['grp'=2,'sp_0'=8,'sp_1'=8,'tp'=2] {'sp_0','sp_1'}, dimensions={0} | all-to-all | bytes 524288 | tf_op jit(solution)/shard_map/all_to_all | solution.py:275
  55.2 0.0 copy-done
  55.2 0.0 copy-done.1
  55.2 0.0 copy-done.2
  55.2 0.0 copy-done.5
  55.2 1.0 %away.1 = bf16[128,2048]{1,0:T(8,128)(2,1)S(1)} custom-call(bf16[256,1024]{1,0:T(8,128)(2,1)S(1)} %copy-done.1, bf16[256,1024]{1,0:T(8,128)(2,1)S(1)} %copy-done.2, bf16[8,128,128]{2,1,0:T(8,128)(2,1)S(1)} %bitcast.4, f32[1,128]{1,0:T(1,128)S(1)} %bitcast.10, bf16[1024,2048]{1,0:T(8,128)(2,1)S(1)} %copy-done), custom_call_target="tpu_custom_call" | custom-call | flops 536870912 | bytes 6029824 | tf_op jit(solution)/shard_map/away/pallas_call | solution.py:203
  56.2 7.3 %collective-permute-start = (bf16[128,2048]{1,0:T(8,128)(2,1)S(1)}, bf16[128,2048]{1,0:T(8,128)(2,1)S(1)}, u32[]{:S(2)}, u32[]{:S(2)}) collective-permute-start(bf16[128,2048]{1,0:T(8,128)(2,1)S(1)} %away.1), channel_id=1, source_target_pairs={{0,1},{1,0},{2,3},{3,2},{4,5},{5,4},{6,7},{7,6},{8,9},{9,8},{10,11... | collective-permute-start | bytes 1572872 | tf_op jit(solution)/shard_map/ppermute | solution.py:290
  63.6 1.0 %kept.1 = f32[128,2048]{1,0:T(8,128)S(1)} custom-call(bf16[256,1024]{1,0:T(8,128)(2,1)S(1)} %copy-done.1, bf16[256,1024]{1,0:T(8,128)(2,1)S(1)} %copy-done.2, bf16[8,128,128]{2,1,0:T(8,128)(2,1)S(1)} %bitcast.5, f32[1,128]{1,0:T(1,128)S(1)} %bitcast.11, bf16[1024,2048]{1,0:T(8,128)(2,1)S(1)} %copy-done), custom_call_target="tpu_custom_call" | custom-call | flops 536870912 | bytes 6554112 | tf_op jit(solution)/shard_map/kept/pallas_call | solution.py:203
  64.6 0.6 collective-permute-done
  65.1 0.9 %add_convert_fusion = bf16[128,2048]{1,0:T(8,128)(2,1)} fusion(f32[128,2048]{1,0:T(8,128)S(1)} %kept.1, bf16[128,2048]{1,0:T(8,128)(2,1)S(1)} %collective-permute-done), kind=kLoop, calls=%fused_computation | loop fusion | flops 786432 | bytes 2097152 | tf_op jit(solution)/shard_map/convert_element_type | solution.py:291
Async XLA Ops:
  3.3 33.9 %all-to-all-start = ((bf16[64,24,128]{2,1,0:T(8,128)(2,1)}), bf16[64,24,128]{2,1,0:T(8,128)(2,1)S(1)}, u32[]{:S(2)}, u32[]{:S(2)}) async-start(bf16[64,24,128]{2,1,0:T(8,128)(2,1)} %state.1), calls=%async_computation | async-start | bytes 786432 | tf_op jit(solution)/shard_map/all_to_all | solution.py:253
  25.1 0.7 %copy-start.3 = (f32[256,8]{0,1:T(8,128)S(1)}, f32[256,8]{0,1:T(8,128)}, u32[]{:S(2)}) copy-start(f32[256,8]{0,1:T(8,128)} %param.10) | copy-start | bytes 24580
  25.8 0.7 %copy-start.4 = (f32[1024]{0:T(1024)S(1)}, f32[1024]{0:T(1024)}, u32[]{:S(2)}) copy-start(f32[1024]{0:T(1024)} %param.11) | copy-start | bytes 12292
  37.2 18.0 %copy-start = (bf16[1024,2048]{1,0:T(8,128)(2,1)S(1)}, bf16[1024,2048]{1,0:T(8,128)(2,1)}, u32[]{:S(2)}) copy-start(bf16[1024,2048]{1,0:T(8,128)(2,1)} %matrix.3) | copy-start | bytes 12582916
  37.2 18.0 %copy-start.1 = (bf16[256,1024]{1,0:T(8,128)(2,1)S(1)}, bf16[256,1024]{1,0:T(8,128)(2,1)}, u32[]{:S(2)}) copy-start(bf16[256,1024]{1,0:T(8,128)(2,1)} %get-tuple-element.12.inside) | copy-start | bytes 1572868
  37.2 18.0 %copy-start.2 = (bf16[256,1024]{1,0:T(8,128)(2,1)S(1)}, bf16[256,1024]{1,0:T(8,128)(2,1)}, u32[]{:S(2)}) copy-start(bf16[256,1024]{1,0:T(8,128)(2,1)} %get-tuple-element.13.reading) | copy-start | bytes 1572868
  37.2 18.0 %copy-start.5 = (f32[128]{0:T(128)S(1)}, f32[128]{0:T(128)}, u32[]{:S(2)}) copy-start(f32[128]{0:T(128)} %param.12) | copy-start | bytes 1540
  56.2 8.9 %collective-permute-start = (bf16[128,2048]{1,0:T(8,128)(2,1)S(1)}, bf16[128,2048]{1,0:T(8,128)(2,1)S(1)}, u32[]{:S(2)}, u32[]{:S(2)}) collective-permute-start(bf16[128,2048]{1,0:T(8,128)(2,1)S(1)} %away.1), channel_id=1, source_target_pairs={{0,1},{1,0},{2,3},{3,2},{4,5},{5,4},{6,7},{7,6},{8,9},{9,8},{10,11... | collective-permute-start | bytes 1572872 | tf_op jit(solution)/shard_map/ppermute | solution.py:290

commit v8 on v7

--- a/solution.py
+++ b/solution.py
@@ -67,13 +67,13 @@
 
 def state_kernel(slabs, far, message, near, sems):
     copies = copied(zip(far, near), sems)
-    retention, source, extra, slack = near
+    retention, extra, slack, source = near
     tokens, channels = retention.shape
     wide = 2 * HEAD
     rows = HEAD // slabs
     r, c = rows_and_columns((tokens, tokens))
     later = (c > r).astype(BF16)
-    for copy in copies:
+    for copy in copies[:-1]:
         copy.wait()
     by_token = extra[...].T
 
@@ -89,6 +89,8 @@
         total = ahead[:1] + log_decay[:1]
         parts = jnp.concatenate(two_parts(total) + (jnp.zeros((6, wide), BF16),), axis=0)
         yield
+        if p == 0:
+            copies[-1].wait()
         for k in range(2):
             part = slice(k * HEAD, (k + 1) * HEAD)
             h = 2 * p + k
@@ -119,7 +121,7 @@
 
 def local_kernel(far, inside, reading, near, sems):
     copies = copied(zip(far, near), sems)
-    retention, source, extra, slack, probe = near
+    retention, extra, slack, source, probe = near
     tokens, channels = retention.shape
     wide = 2 * HEAD
     r, c = rows_and_columns((tokens, tokens))
@@ -192,12 +194,24 @@
     out[...] = dot(normed[...], matrix[...], ((1,), (0,))).astype(out.dtype)
 
 
+def final_kernel(kept, received, far, out, sems):
+    pieces, rows, _ = out.shape
+    copies = []
+    for i in range(pieces):
+        span = slice(i * rows, (i + 1) * rows)
+        out[i] = (kept[span] + received[span].astype(F32)).astype(BF16)
+        copies.append(pltpu.make_async_copy(out.at[i], far.at[span], sems.at[i]))
+        copies[-1].start()
+    for copy in copies:
+        copy.wait()
+
+
 VMEM = 67043328
 IN_VMEM = pl.BlockSpec(memory_space=pltpu.VMEM)
 IN_HBM = pl.BlockSpec(memory_space=pltpu.HBM)
 
 
-def call(kernel, name, far, near, outs, flops, scratch=(), left=24 << 20):
+def call(kernel, name, far, near, outs, flops, scratch=(), left=24 << 20, out_spec=IN_VMEM):
     inputs = (*far, *near)
     moved = sum(a.size * a.dtype.itemsize for a in (*inputs, *outs))
     results = pl.pallas_call(
@@ -205,7 +219,7 @@
         name=name,
         out_shape=outs,
         in_specs=[IN_HBM] * len(far) + [IN_VMEM] * len(near),
-        out_specs=[IN_VMEM] * len(outs),
+        out_specs=[out_spec] * len(outs),
         scratch_shapes=list(scratch),
         compiler_params=pltpu.CompilerParams(vmem_limit_bytes=VMEM - left),
         cost_estimate=pl.CostEstimate(flops=flops, bytes_accessed=moved, transcendentals=0),
@@ -232,7 +246,7 @@
     gain = group_normalizer_gain.reshape(1, HEAD)
     extra = extra_log_retention.T
     flops = 2 * tokens * channels * HEAD
-    inputs = (retention_preactivation, source_entries, extra, slack)
+    inputs = (retention_preactivation, extra, slack, source_entries)
 
     def near(arrays):
         return (
@@ -260,7 +274,7 @@
         [jax.ShapeDtypeStruct((tokens, channels), BF16)] * 2,
         6 * flops,
         near(inputs),
-        21 << 19,
+        10300000,
     )
     arrived, inside, reading = lax.optimization_barrier((arrived, inside, reading))
     scanned = call(
@@ -288,7 +302,17 @@
         )
 
     received = lax.ppermute(projected(True, BF16), "tp", [(0, 1), (1, 0)])
-    return (projected(False, F32) + received.astype(F32)).astype(BF16)
+    pieces = 4
+    return call(
+        final_kernel,
+        "final",
+        (),
+        (projected(False, F32), received),
+        [jax.ShapeDtypeStruct((half, width), BF16)],
+        half * width,
+        [pltpu.VMEM((pieces, half // pieces, width), BF16), pltpu.SemaphoreType.DMA((pieces,))],
+        out_spec=IN_HBM,
+    )
 
 
 def solution(mesh):

time: 66.3 us -> 66.1 us (level)
  local copies, waits for them, and re-layouts: 1.39 us -> 0.01 us
  waiting for transfers between devices: 7.28 us -> 8.62 us
  other arithmetic: 0.9 us -> 0 us
  Pallas kernels: 9.68 us -> 10.5 us
    unnamed x12 -> x8, local copies, waits for them, and re-layouts: 1.39 us -> 0.01 us
    all_to_all x1, waiting for transfers between devices: 6.73 us -> 8.07 us  [body(): lax.all_to_all(message, SP, split_axis=0, concat_axis=0, tiled=True)]
    convert_element_type x1 -> x0, other arithmetic: 0.9 us -> none  [body(): return (projected(False, F32) + received.astype(F32)).astype(BF16)]
    pallas_call x5 -> x6, Pallas kernels: 9.68 us -> 10.5 us  [call(): pl.pallas_call(kernel, name=name, out_shape=outs, in_specs=[IN_HBM] * len...]
  transfers between devices with their start and end apart: 2 -> 2, of which waited for: 2 -> 2; matrix products, arithmetic and copies ran while one was open for 0% -> 0% of each run, Pallas kernels for 7% -> 8%
where the time goes in v8:
time: 66.1 us; the launch traced here: 65.9 us
  starting transfers between devices  29.3 us (44%)
  blocking collectives  17.4 us (26%)
  Pallas kernels  10.5 us (16%)
  waiting for transfers between devices  8.62 us (13%)
    all_to_all x1, starting transfers between devices, body(): lax.all_to_all(message, SP, split_axis=0, concat_axis=0, tiled=True)  21.8 us
    all_to_all x1, blocking collectives, body(): lax.all_to_all(scanned, SP, split_axis=0, concat_axis=0, tiled=True)  17.4 us
    pallas_call x6, Pallas kernels, call(): pl.pallas_call(kernel, name=name, out_shape=outs, in_specs=[IN_HBM] * len...  10.5 us
    all_to_all x1, waiting for transfers between devices, body(): lax.all_to_all(message, SP, split_axis=0, concat_axis=0, tiled=True)  8.07 us
    ppermute x1, starting transfers between devices, body(): received = lax.ppermute(projected(True, BF16), 'tp', [(0, 1), (1, 0)])  7.46 us
  transfers between devices with their start and end apart: 2, of which 2 were waited for; matrix products, arithmetic and copies ran while one was open for 0% of the time, Pallas kernels for 8%

profile of v8, /device:TPU:513, one launch (start us, length us, event | category | flops | bytes accessed | tf_op | source)
XLA Modules:
  0.0 65.9 jit_solution(2836183959889534384)
XLA Ops:
  0.0 3.3 %state.1 = bf16[64,24,128]{2,1,0:T(8,128)(2,1)} custom-call(bf16[256,1024]{1,0:T(8,128)(2,1)} %refs_0_.3, f32[8,256]{1,0:T(8,128)} %bitcast.8, f32[1,1024]{1,0:T(1,128)} %bitcast.10, bf16[256,1024]{1,0:T(8,128)(2,1)} %refs_3_.3), custom_call_target="tpu_custom_call" | custom-call | flops 268435456 | bytes 1454080 | tf_op jit(solution)/shard_map/state/pallas_call | solution.py:217
  3.3 21.8 %all-to-all-start = ((bf16[64,24,128]{2,1,0:T(8,128)(2,1)}), bf16[64,24,128]{2,1,0:T(8,128)(2,1)S(1)}, u32[]{:S(2)}, u32[]{:S(2)}) async-start(bf16[64,24,128]{2,1,0:T(8,128)(2,1)} %state.1), calls=%async_computation | async-start | bytes 786432 | tf_op jit(solution)/shard_map/all_to_all | solution.py:267
  25.1 4.0 %local.1 = (bf16[256,1024]{1,0:T(8,128)(2,1)}, bf16[256,1024]{1,0:T(8,128)(2,1)}) custom-call(bf16[256,1024]{1,0:T(8,128)(2,1)} %refs_0_.3, f32[8,256]{1,0:T(8,128)} %bitcast.9, f32[1,1024]{1,0:T(1,128)} %bitcast.11, bf16[256,1024]{1,0:T(8,128)(2,1)} %refs_3_.3, bf16[256,1024]{1,0:T(8,128)(2,1)} %refs_4_.1), custom_call_target="tpu_custom_call" | custom-call | flops 402653184 | bytes 2633728 | tf_op jit(solution)/shard_map/local/pallas_call | solution.py:217
  29.1 8.1 %all-to-all-done.message = bf16[64,24,128]{2,1,0:T(8,128)(2,1)S(1)} async-done(((bf16[64,24,128]{2,1,0:T(8,128)(2,1)}), bf16[64,24,128]{2,1,0:T(8,128)(2,1)S(1)}, u32[]{:S(2)}, u32[]{:S(2)}) %all-to-all-start) | async-done | bytes 393248 | tf_op jit(solution)/shard_map/all_to_all | solution.py:267
  37.2 0.0 copy-start
  37.2 0.0 copy-start.1
  37.2 0.0 copy-start.2
  37.2 0.0 copy-start.3
  37.2 0.4 scan.1
  37.6 17.4 %all_to_all.10 = bf16[64,16,128]{2,1,0:T(8,128)(2,1)S(1)} all-to-all(bf16[64,16,128]{2,1,0:T(8,128)(2,1)S(1)} %scan.1), channel_id=1, replica_groups=mesh['grp'=2,'sp_0'=8,'sp_1'=8,'tp'=2] {'sp_0','sp_1'}, dimensions={0} | all-to-all | bytes 524288 | tf_op jit(solution)/shard_map/all_to_all | solution.py:289
  55.0 0.0 copy-done
  55.0 0.0 copy-done.1
  55.0 0.0 copy-done.2
  55.0 0.0 copy-done.3
  55.0 1.0 %away.1 = bf16[128,2048]{1,0:T(8,128)(2,1)S(1)} custom-call(bf16[256,1024]{1,0:T(8,128)(2,1)S(1)} %copy-done.1, bf16[256,1024]{1,0:T(8,128)(2,1)S(1)} %copy-done.2, bf16[8,128,128]{2,1,0:T(8,128)(2,1)S(1)} %bitcast.4, f32[1,128]{1,0:T(1,128)S(1)} %bitcast.6, bf16[1024,2048]{1,0:T(8,128)(2,1)S(1)} %copy-done), custom_call_target="tpu_custom_call" | custom-call | flops 536870912 | bytes 6029824 | tf_op jit(solution)/shard_map/away/pallas_call | solution.py:217
  56.0 7.5 %collective-permute-start = (bf16[128,2048]{1,0:T(8,128)(2,1)S(1)}, bf16[128,2048]{1,0:T(8,128)(2,1)S(1)}, u32[]{:S(2)}, u32[]{:S(2)}) collective-permute-start(bf16[128,2048]{1,0:T(8,128)(2,1)S(1)} %away.1), channel_id=1, source_target_pairs={{0,1},{1,0},{2,3},{3,2},{4,5},{5,4},{6,7},{7,6},{8,9},{9,8},{10,11... | collective-permute-start | bytes 1572872 | tf_op jit(solution)/shard_map/ppermute | solution.py:304
  63.5 1.0 %kept.1 = f32[128,2048]{1,0:T(8,128)S(1)} custom-call(bf16[256,1024]{1,0:T(8,128)(2,1)S(1)} %copy-done.1, bf16[256,1024]{1,0:T(8,128)(2,1)S(1)} %copy-done.2, bf16[8,128,128]{2,1,0:T(8,128)(2,1)S(1)} %bitcast.5, f32[1,128]{1,0:T(1,128)S(1)} %bitcast.7, bf16[1024,2048]{1,0:T(8,128)(2,1)S(1)} %copy-done), custom_call_target="tpu_custom_call" | custom-call | flops 536870912 | bytes 6554112 | tf_op jit(solution)/shard_map/kept/pallas_call | solution.py:217
  64.5 0.5 collective-permute-done.received
  65.0 0.8 %final.1 = bf16[128,2048]{1,0:T(8,128)(2,1)} custom-call(f32[128,2048]{1,0:T(8,128)S(1)} %kept.1, bf16[128,2048]{1,0:T(8,128)(2,1)S(1)} %collective-permute-done.received), custom_call_target="tpu_custom_call" | custom-call | flops 262144 | bytes 2097152 | tf_op jit(solution)/shard_map/final/pallas_call | solution.py:217
Async XLA Ops:
  3.3 33.9 %all-to-all-start = ((bf16[64,24,128]{2,1,0:T(8,128)(2,1)}), bf16[64,24,128]{2,1,0:T(8,128)(2,1)S(1)}, u32[]{:S(2)}, u32[]{:S(2)}) async-start(bf16[64,24,128]{2,1,0:T(8,128)(2,1)} %state.1), calls=%async_computation | async-start | bytes 786432 | tf_op jit(solution)/shard_map/all_to_all | solution.py:267
  37.2 17.9 %copy-start = (bf16[1024,2048]{1,0:T(8,128)(2,1)S(1)}, bf16[1024,2048]{1,0:T(8,128)(2,1)}, u32[]{:S(2)}) copy-start(bf16[1024,2048]{1,0:T(8,128)(2,1)} %matrix.3) | copy-start | bytes 12582916
  37.2 17.9 %copy-start.1 = (bf16[256,1024]{1,0:T(8,128)(2,1)S(1)}, bf16[256,1024]{1,0:T(8,128)(2,1)}, u32[]{:S(2)}) copy-start(bf16[256,1024]{1,0:T(8,128)(2,1)} %get-tuple-element.12.inside) | copy-start | bytes 1572868
  37.2 17.9 %copy-start.2 = (bf16[256,1024]{1,0:T(8,128)(2,1)S(1)}, bf16[256,1024]{1,0:T(8,128)(2,1)}, u32[]{:S(2)}) copy-start(bf16[256,1024]{1,0:T(8,128)(2,1)} %get-tuple-element.13.reading) | copy-start | bytes 1572868
  37.2 17.9 %copy-start.3 = (f32[128]{0:T(128)S(1)}, f32[128]{0:T(128)}, u32[]{:S(2)}) copy-start(f32[128]{0:T(128)} %param.12) | copy-start | bytes 1540
  56.0 9.0 %collective-permute-start = (bf16[128,2048]{1,0:T(8,128)(2,1)S(1)}, bf16[128,2048]{1,0:T(8,128)(2,1)S(1)}, u32[]{:S(2)}, u32[]{:S(2)}) collective-permute-start(bf16[128,2048]{1,0:T(8,128)(2,1)S(1)} %away.1), channel_id=1, source_target_pairs={{0,1},{1,0},{2,3},{3,2},{4,5},{5,4},{6,7},{7,6},{8,9},{9,8},{10,11... | collective-permute-start | bytes 1572872 | tf_op jit(solution)/shard_map/ppermute | solution.py:304

commit v9 on v8

--- a/solution.py
+++ b/solution.py
@@ -87,7 +87,7 @@
         yield
         sent = (keyed * jnp.exp(ahead)).astype(BF16)
         total = ahead[:1] + log_decay[:1]
-        parts = jnp.concatenate(two_parts(total) + (jnp.zeros((6, wide), BF16),), axis=0)
+        parts = jnp.concatenate(two_parts(total), axis=0)
         yield
         if p == 0:
             copies[-1].wait()
@@ -96,11 +96,11 @@
             h = 2 * p + k
             values = source[:, h * HEAD : (h + 1) * HEAD]
             state = dot(sent[:, part], values, ((0,), (0,)))
-            message[h * slabs : (h + 1) * slabs, :rows, :] = state.astype(BF16).reshape(
-                slabs, rows, HEAD
+            message[h * slabs : (h + 1) * slabs, : rows // 2] = state.astype(BF16).reshape(
+                slabs, rows // 2, 2, HEAD
             )
-            message[h * slabs : (h + 1) * slabs, rows:, :] = jnp.broadcast_to(
-                parts[None, :, part], (slabs, 8, HEAD)
+            message[h * slabs : (h + 1) * slabs, rows // 2] = jnp.broadcast_to(
+                parts[None, :, part], (slabs, 2, HEAD)
             )
 
     staggered(chain, channels // wide)
@@ -109,14 +109,14 @@
 def scan_kernel(slabs, message, entering, by_channel):
     positions, rows, _ = entering.shape
     slab = lax.rem(lax.axis_index(SP), slabs)
-    parts = message[:, rows:, :].astype(F32)
+    parts = message[:, rows // 2].astype(F32)
     by_channel[...] = jnp.exp(parts[:, 0] + parts[:, 1]).T
     mine = by_channel[pl.ds(pl.multiple_of(slab * rows, rows), rows), :]
     state = jnp.zeros((rows, HEAD), F32)
     for i in range(positions):
         entering[i] = state.astype(BF16)
         if i + 1 < positions:
-            state = mine[:, i : i + 1] * state + message[i, :rows, :].astype(F32)
+            state = mine[:, i : i + 1] * state + message[i, : rows // 2].astype(F32).reshape(rows, HEAD)
 
 
 def local_kernel(far, inside, reading, near, sems):
@@ -259,7 +259,7 @@
         "state",
         inputs,
         (),
-        [jax.ShapeDtypeStruct((positions, rows + 8, HEAD), BF16)],
+        [jax.ShapeDtypeStruct((positions, rows // 2 + 1, 2, HEAD), BF16)],
         4 * flops,
         near(inputs),
         0,

time: 66.1 us -> 65.1 us (0.985)
  waiting for transfers between devices: 8.62 us -> 7.93 us
    all_to_all x1, waiting for transfers between devices: 8.07 us -> 7.38 us  [body(): lax.all_to_all(message, SP, split_axis=0, concat_axis=0, tiled=True)]
where the time goes in v9:
time: 65.1 us; the launch traced here: 64.8 us
  starting transfers between devices  29.3 us (45%)
  blocking collectives  17 us (26%)
  Pallas kernels  10.5 us (16%)
  waiting for transfers between devices  7.93 us (12%)
    all_to_all x1, starting transfers between devices, body(): lax.all_to_all(message, SP, split_axis=0, concat_axis=0, tiled=True)  21.8 us
    all_to_all x1, blocking collectives, body(): lax.all_to_all(scanned, SP, split_axis=0, concat_axis=0, tiled=True)  17 us
    pallas_call x6, Pallas kernels, call(): pl.pallas_call(kernel, name=name, out_shape=outs, in_specs=[IN_HBM] * len...  10.5 us
    ppermute x1, starting transfers between devices, body(): received = lax.ppermute(projected(True, BF16), 'tp', [(0, 1), (1, 0)])  7.5 us
    all_to_all x1, waiting for transfers between devices, body(): lax.all_to_all(message, SP, split_axis=0, concat_axis=0, tiled=True)  7.38 us
  transfers between devices with their start and end apart: 2, of which 2 were waited for; matrix products, arithmetic and copies ran while one was open for 0% of the time, Pallas kernels for 8%

profile of v9, /device:TPU:513, one launch (start us, length us, event | category | flops | bytes accessed | tf_op | source)
XLA Modules:
  0.0 64.8 jit_solution(1292097848725597038)
XLA Ops:
  0.0 3.2 %state.1 = bf16[64,9,2,128]{3,2,1,0:T(2,128)(2,1)} custom-call(bf16[256,1024]{1,0:T(8,128)(2,1)} %refs_0_.3, f32[8,256]{1,0:T(8,128)} %bitcast.8, f32[1,1024]{1,0:T(1,128)} %bitcast.10, bf16[256,1024]{1,0:T(8,128)(2,1)} %refs_3_.3), custom_call_target="tpu_custom_call" | custom-call | flops 268435456 | bytes 1355776 | tf_op jit(solution)/shard_map/state/pallas_call | solution.py:217
  3.2 21.8 %all-to-all-start = ((bf16[64,9,2,128]{3,2,1,0:T(2,128)(2,1)}), bf16[64,9,2,128]{3,2,1,0:T(2,128)(2,1)S(1)}, u32[]{:S(2)}, u32[]{:S(2)}) async-start(bf16[64,9,2,128]{3,2,1,0:T(2,128)(2,1)} %state.1), calls=%async_computation | async-start | bytes 589824 | tf_op jit(solution)/shard_map/all_to_all | solution.py:267
  25.1 4.0 %local.1 = (bf16[256,1024]{1,0:T(8,128)(2,1)}, bf16[256,1024]{1,0:T(8,128)(2,1)}) custom-call(bf16[256,1024]{1,0:T(8,128)(2,1)} %refs_0_.3, f32[8,256]{1,0:T(8,128)} %bitcast.9, f32[1,1024]{1,0:T(1,128)} %bitcast.11, bf16[256,1024]{1,0:T(8,128)(2,1)} %refs_3_.3, bf16[256,1024]{1,0:T(8,128)(2,1)} %refs_4_.1), custom_call_target="tpu_custom_call" | custom-call | flops 402653184 | bytes 2633728 | tf_op jit(solution)/shard_map/local/pallas_call | solution.py:217
  29.1 7.4 %all-to-all-done.message = bf16[64,9,2,128]{3,2,1,0:T(2,128)(2,1)S(1)} async-done(((bf16[64,9,2,128]{3,2,1,0:T(2,128)(2,1)}), bf16[64,9,2,128]{3,2,1,0:T(2,128)(2,1)S(1)}, u32[]{:S(2)}, u32[]{:S(2)}) %all-to-all-start) | async-done | bytes 294944 | tf_op jit(solution)/shard_map/all_to_all | solution.py:267
  36.5 0.0 copy-start
  36.5 0.0 copy-start.1
  36.5 0.0 copy-start.2
  36.5 0.0 copy-start.3
  36.5 0.5 scan.1
  36.9 17.0 %all_to_all.10 = bf16[64,16,128]{2,1,0:T(8,128)(2,1)S(1)} all-to-all(bf16[64,16,128]{2,1,0:T(8,128)(2,1)S(1)} %scan.1), channel_id=1, replica_groups=mesh['grp'=2,'sp_0'=8,'sp_1'=8,'tp'=2] {'sp_0','sp_1'}, dimensions={0} | all-to-all | bytes 524288 | tf_op jit(solution)/shard_map/all_to_all | solution.py:289
  53.9 0.0 copy-done
  53.9 0.0 copy-done.1
  53.9 0.0 copy-done.2
  53.9 0.0 copy-done.3
  53.9 1.0 %away.1 = bf16[128,2048]{1,0:T(8,128)(2,1)S(1)} custom-call(bf16[256,1024]{1,0:T(8,128)(2,1)S(1)} %copy-done.1, bf16[256,1024]{1,0:T(8,128)(2,1)S(1)} %copy-done.2, bf16[8,128,128]{2,1,0:T(8,128)(2,1)S(1)} %bitcast.4, f32[1,128]{1,0:T(1,128)S(1)} %bitcast.6, bf16[1024,2048]{1,0:T(8,128)(2,1)S(1)} %copy-done), custom_call_target="tpu_custom_call" | custom-call | flops 536870912 | bytes 6029824 | tf_op jit(solution)/shard_map/away/pallas_call | solution.py:217
  54.9 7.5 %collective-permute-start = (bf16[128,2048]{1,0:T(8,128)(2,1)S(1)}, bf16[128,2048]{1,0:T(8,128)(2,1)S(1)}, u32[]{:S(2)}, u32[]{:S(2)}) collective-permute-start(bf16[128,2048]{1,0:T(8,128)(2,1)S(1)} %away.1), channel_id=1, source_target_pairs={{0,1},{1,0},{2,3},{3,2},{4,5},{5,4},{6,7},{7,6},{8,9},{9,8},{10,11... | collective-permute-start | bytes 1572872 | tf_op jit(solution)/shard_map/ppermute | solution.py:304
  62.4 1.0 %kept.1 = f32[128,2048]{1,0:T(8,128)S(1)} custom-call(bf16[256,1024]{1,0:T(8,128)(2,1)S(1)} %copy-done.1, bf16[256,1024]{1,0:T(8,128)(2,1)S(1)} %copy-done.2, bf16[8,128,128]{2,1,0:T(8,128)(2,1)S(1)} %bitcast.5, f32[1,128]{1,0:T(1,128)S(1)} %bitcast.7, bf16[1024,2048]{1,0:T(8,128)(2,1)S(1)} %copy-done), custom_call_target="tpu_custom_call" | custom-call | flops 536870912 | bytes 6554112 | tf_op jit(solution)/shard_map/kept/pallas_call | solution.py:217
  63.4 0.6 collective-permute-done.received
  64.0 0.8 %final.1 = bf16[128,2048]{1,0:T(8,128)(2,1)} custom-call(f32[128,2048]{1,0:T(8,128)S(1)} %kept.1, bf16[128,2048]{1,0:T(8,128)(2,1)S(1)} %collective-permute-done.received), custom_call_target="tpu_custom_call" | custom-call | flops 262144 | bytes 2097152 | tf_op jit(solution)/shard_map/final/pallas_call | solution.py:217
Async XLA Ops:
  3.2 33.2 %all-to-all-start = ((bf16[64,9,2,128]{3,2,1,0:T(2,128)(2,1)}), bf16[64,9,2,128]{3,2,1,0:T(2,128)(2,1)S(1)}, u32[]{:S(2)}, u32[]{:S(2)}) async-start(bf16[64,9,2,128]{3,2,1,0:T(2,128)(2,1)} %state.1), calls=%async_computation | async-start | bytes 589824 | tf_op jit(solution)/shard_map/all_to_all | solution.py:267
  36.5 17.5 %copy-start = (bf16[1024,2048]{1,0:T(8,128)(2,1)S(1)}, bf16[1024,2048]{1,0:T(8,128)(2,1)}, u32[]{:S(2)}) copy-start(bf16[1024,2048]{1,0:T(8,128)(2,1)} %matrix.3) | copy-start | bytes 12582916
  36.5 17.5 %copy-start.1 = (bf16[256,1024]{1,0:T(8,128)(2,1)S(1)}, bf16[256,1024]{1,0:T(8,128)(2,1)}, u32[]{:S(2)}) copy-start(bf16[256,1024]{1,0:T(8,128)(2,1)} %get-tuple-element.12.inside) | copy-start | bytes 1572868
  36.5 17.5 %copy-start.2 = (bf16[256,1024]{1,0:T(8,128)(2,1)S(1)}, bf16[256,1024]{1,0:T(8,128)(2,1)}, u32[]{:S(2)}) copy-start(bf16[256,1024]{1,0:T(8,128)(2,1)} %get-tuple-element.13.reading) | copy-start | bytes 1572868
  36.5 17.5 %copy-start.3 = (f32[128]{0:T(128)S(1)}, f32[128]{0:T(128)}, u32[]{:S(2)}) copy-start(f32[128]{0:T(128)} %param.12) | copy-start | bytes 1540
  54.9 9.0 %collective-permute-start = (bf16[128,2048]{1,0:T(8,128)(2,1)S(1)}, bf16[128,2048]{1,0:T(8,128)(2,1)S(1)}, u32[]{:S(2)}, u32[]{:S(2)}) collective-permute-start(bf16[128,2048]{1,0:T(8,128)(2,1)S(1)} %away.1), channel_id=1, source_target_pairs={{0,1},{1,0},{2,3},{3,2},{4,5},{5,4},{6,7},{7,6},{8,9},{9,8},{10,11... | collective-permute-start | bytes 1572872 | tf_op jit(solution)/shard_map/ppermute | solution.py:304

commit v10 on v9

--- a/solution.py
+++ b/solution.py
@@ -65,8 +65,9 @@
         live = [chain for chain in live if next(chain, live) is None]
 
 
-def state_kernel(slabs, far, message, near, sems):
+def state_kernel(slabs, far, far_message, near, sems, message, out_sems):
     copies = copied(zip(far, near), sems)
+    leaving = []
     retention, extra, slack, source = near
     tokens, channels = retention.shape
     wide = 2 * HEAD
@@ -102,8 +103,16 @@
             message[h * slabs : (h + 1) * slabs, rows // 2] = jnp.broadcast_to(
                 parts[None, :, part], (slabs, 2, HEAD)
             )
+        yield
+        owners = slice(2 * p * slabs, 2 * (p + 1) * slabs)
+        leaving.append(
+            pltpu.make_async_copy(message.at[owners], far_message.at[owners], out_sems.at[p])
+        )
+        leaving[-1].start()
 
     staggered(chain, channels // wide)
+    for copy in leaving:
+        copy.wait()
 
 
 def scan_kernel(slabs, message, entering, by_channel):
@@ -119,8 +128,9 @@
             state = mine[:, i : i + 1] * state + message[i, : rows // 2].astype(F32).reshape(rows, HEAD)
 
 
-def local_kernel(far, inside, reading, near, sems):
+def local_kernel(far, far_inside, far_reading, near, sems, inside, reading, out_sems):
     copies = copied(zip(far, near), sems)
+    leaving = []
     retention, extra, slack, source, probe = near
     tokens, channels = retention.shape
     wide = 2 * HEAD
@@ -177,8 +187,15 @@
                         added = jnp.exp(last[:, part]).reshape(HEAD, 1) * before[k] + added
                     before[k] = added
             yield
+        for i, (a, b) in enumerate(((inside, far_inside), (reading, far_reading))):
+            leaving.append(
+                pltpu.make_async_copy(a.at[:, lanes], b.at[:, lanes], out_sems.at[i, p])
+            )
+            leaving[-1].start()
 
     staggered(chain, channels // wide)
+    for copy in leaving:
+        copy.wait()
 
 
 def output_kernel(away, inside, reading, entering, gain, matrix, out, normed):
@@ -201,7 +218,9 @@
         span = slice(i * rows, (i + 1) * rows)
         out[i] = (kept[span] + received[span].astype(F32)).astype(BF16)
         copies.append(pltpu.make_async_copy(out.at[i], far.at[span], sems.at[i]))
-        copies[-1].start()
+        if i > 0:
+            copies[i - 1].start()
+    copies[-1].start()
     for copy in copies:
         copy.wait()
 
@@ -261,8 +280,13 @@
         (),
         [jax.ShapeDtypeStruct((positions, rows // 2 + 1, 2, HEAD), BF16)],
         4 * flops,
-        near(inputs),
+        (
+            *near(inputs),
+            pltpu.VMEM((positions, rows // 2 + 1, 2, HEAD), BF16),
+            pltpu.SemaphoreType.DMA((channels // (2 * HEAD),)),
+        ),
         0,
+        IN_HBM,
     )
     arrived = lax.all_to_all(message, SP, split_axis=0, concat_axis=0, tiled=True)
     inputs = (*inputs, probe_preactivation)
@@ -273,8 +297,13 @@
         (),
         [jax.ShapeDtypeStruct((tokens, channels), BF16)] * 2,
         6 * flops,
-        near(inputs),
+        (
+            *near(inputs),
+            *[pltpu.VMEM((tokens, channels), BF16)] * 2,
+            pltpu.SemaphoreType.DMA((2, channels // (2 * HEAD))),
+        ),
         10300000,
+        IN_HBM,
     )
     arrived, inside, reading = lax.optimization_barrier((arrived, inside, reading))
     scanned = call(

time: 65.1 us -> 65 us (level)
  no operation moved by 1% of the time
where the time goes in v10:
time: 65 us; the launch traced here: 64.8 us
  starting transfers between devices  29.3 us (45%)
  blocking collectives  17 us (26%)
  Pallas kernels  10.5 us (16%)
  waiting for transfers between devices  7.94 us (12%)
    all_to_all x1, starting transfers between devices, body(): lax.all_to_all(message, SP, split_axis=0, concat_axis=0, tiled=True)  21.8 us
    all_to_all x1, blocking collectives, body(): lax.all_to_all(scanned, SP, split_axis=0, concat_axis=0, tiled=True)  17 us
    pallas_call x6, Pallas kernels, call(): pl.pallas_call(kernel, name=name, out_shape=outs, in_specs=[IN_HBM] * len...  10.5 us
    ppermute x1, starting transfers between devices, body(): received = lax.ppermute(projected(True, BF16), 'tp', [(0, 1), (1, 0)])  7.51 us
    all_to_all x1, waiting for transfers between devices, body(): lax.all_to_all(message, SP, split_axis=0, concat_axis=0, tiled=True)  7.39 us
  transfers between devices with their start and end apart: 2, of which 2 were waited for; matrix products, arithmetic and copies ran while one was open for 0% of the time, Pallas kernels for 8%

profile of v10, /device:TPU:513, one launch (start us, length us, event | category | flops | bytes accessed | tf_op | source)
XLA Modules:
  0.0 64.8 jit_solution(3436957956638643331)
XLA Ops:
  0.0 3.2 %state.1 = bf16[64,9,2,128]{3,2,1,0:T(2,128)(2,1)} custom-call(bf16[256,1024]{1,0:T(8,128)(2,1)} %refs_0_.3, f32[8,256]{1,0:T(8,128)} %bitcast.8, f32[1,1024]{1,0:T(1,128)} %bitcast.10, bf16[256,1024]{1,0:T(8,128)(2,1)} %refs_3_.3), custom_call_target="tpu_custom_call" | custom-call | flops 268435456 | bytes 1355776 | tf_op jit(solution)/shard_map/state/pallas_call | solution.py:236
  3.2 21.8 %all-to-all-start = ((bf16[64,9,2,128]{3,2,1,0:T(2,128)(2,1)}), bf16[64,9,2,128]{3,2,1,0:T(2,128)(2,1)S(1)}, u32[]{:S(2)}, u32[]{:S(2)}) async-start(bf16[64,9,2,128]{3,2,1,0:T(2,128)(2,1)} %state.1), calls=%async_computation | async-start | bytes 589824 | tf_op jit(solution)/shard_map/all_to_all | solution.py:291
  25.0 4.0 %local.1 = (bf16[256,1024]{1,0:T(8,128)(2,1)}, bf16[256,1024]{1,0:T(8,128)(2,1)}) custom-call(bf16[256,1024]{1,0:T(8,128)(2,1)} %refs_0_.3, f32[8,256]{1,0:T(8,128)} %bitcast.9, f32[1,1024]{1,0:T(1,128)} %bitcast.11, bf16[256,1024]{1,0:T(8,128)(2,1)} %refs_3_.3, bf16[256,1024]{1,0:T(8,128)(2,1)} %refs_4_.1), custom_call_target="tpu_custom_call" | custom-call | flops 402653184 | bytes 2633728 | tf_op jit(solution)/shard_map/local/pallas_call | solution.py:236
  29.0 7.4 %all-to-all-done.message = bf16[64,9,2,128]{3,2,1,0:T(2,128)(2,1)S(1)} async-done(((bf16[64,9,2,128]{3,2,1,0:T(2,128)(2,1)}), bf16[64,9,2,128]{3,2,1,0:T(2,128)(2,1)S(1)}, u32[]{:S(2)}, u32[]{:S(2)}) %all-to-all-start) | async-done | bytes 294944 | tf_op jit(solution)/shard_map/all_to_all | solution.py:291
  36.4 0.0 copy-start
  36.4 0.0 copy-start.1
  36.4 0.0 copy-start.2
  36.4 0.0 copy-start.3
  36.4 0.5 scan.1
  36.9 17.0 %all_to_all.10 = bf16[64,16,128]{2,1,0:T(8,128)(2,1)S(1)} all-to-all(bf16[64,16,128]{2,1,0:T(8,128)(2,1)S(1)} %scan.1), channel_id=1, replica_groups=mesh['grp'=2,'sp_0'=8,'sp_1'=8,'tp'=2] {'sp_0','sp_1'}, dimensions={0} | all-to-all | bytes 524288 | tf_op jit(solution)/shard_map/all_to_all | solution.py:318
  53.9 0.0 copy-done
  53.9 0.0 copy-done.1
  53.9 0.0 copy-done.2
  53.9 0.0 copy-done.3
  53.9 1.0 %away.1 = bf16[128,2048]{1,0:T(8,128)(2,1)S(1)} custom-call(bf16[256,1024]{1,0:T(8,128)(2,1)S(1)} %copy-done.1, bf16[256,1024]{1,0:T(8,128)(2,1)S(1)} %copy-done.2, bf16[8,128,128]{2,1,0:T(8,128)(2,1)S(1)} %bitcast.4, f32[1,128]{1,0:T(1,128)S(1)} %bitcast.6, bf16[1024,2048]{1,0:T(8,128)(2,1)S(1)} %copy-done), custom_call_target="tpu_custom_call" | custom-call | flops 536870912 | bytes 6029824 | tf_op jit(solution)/shard_map/away/pallas_call | solution.py:236
  54.9 7.5 %collective-permute-start = (bf16[128,2048]{1,0:T(8,128)(2,1)S(1)}, bf16[128,2048]{1,0:T(8,128)(2,1)S(1)}, u32[]{:S(2)}, u32[]{:S(2)}) collective-permute-start(bf16[128,2048]{1,0:T(8,128)(2,1)S(1)} %away.1), channel_id=1, source_target_pairs={{0,1},{1,0},{2,3},{3,2},{4,5},{5,4},{6,7},{7,6},{8,9},{9,8},{10,11... | collective-permute-start | bytes 1572872 | tf_op jit(solution)/shard_map/ppermute | solution.py:333
  62.4 1.0 %kept.1 = f32[128,2048]{1,0:T(8,128)S(1)} custom-call(bf16[256,1024]{1,0:T(8,128)(2,1)S(1)} %copy-done.1, bf16[256,1024]{1,0:T(8,128)(2,1)S(1)} %copy-done.2, bf16[8,128,128]{2,1,0:T(8,128)(2,1)S(1)} %bitcast.5, f32[1,128]{1,0:T(1,128)S(1)} %bitcast.7, bf16[1024,2048]{1,0:T(8,128)(2,1)S(1)} %copy-done), custom_call_target="tpu_custom_call" | custom-call | flops 536870912 | bytes 6554112 | tf_op jit(solution)/shard_map/kept/pallas_call | solution.py:236
  63.4 0.5 collective-permute-done.received
  63.9 0.9 %final.1 = bf16[128,2048]{1,0:T(8,128)(2,1)} custom-call(f32[128,2048]{1,0:T(8,128)S(1)} %kept.1, bf16[128,2048]{1,0:T(8,128)(2,1)S(1)} %collective-permute-done.received), custom_call_target="tpu_custom_call" | custom-call | flops 262144 | bytes 2097152 | tf_op jit(solution)/shard_map/final/pallas_call | solution.py:236
Async XLA Ops:
  3.2 33.2 %all-to-all-start = ((bf16[64,9,2,128]{3,2,1,0:T(2,128)(2,1)}), bf16[64,9,2,128]{3,2,1,0:T(2,128)(2,1)S(1)}, u32[]{:S(2)}, u32[]{:S(2)}) async-start(bf16[64,9,2,128]{3,2,1,0:T(2,128)(2,1)} %state.1), calls=%async_computation | async-start | bytes 589824 | tf_op jit(solution)/shard_map/all_to_all | solution.py:291
  36.4 17.5 %copy-start = (bf16[1024,2048]{1,0:T(8,128)(2,1)S(1)}, bf16[1024,2048]{1,0:T(8,128)(2,1)}, u32[]{:S(2)}) copy-start(bf16[1024,2048]{1,0:T(8,128)(2,1)} %matrix.3) | copy-start | bytes 12582916
  36.4 17.5 %copy-start.1 = (bf16[256,1024]{1,0:T(8,128)(2,1)S(1)}, bf16[256,1024]{1,0:T(8,128)(2,1)}, u32[]{:S(2)}) copy-start(bf16[256,1024]{1,0:T(8,128)(2,1)} %get-tuple-element.12.inside) | copy-start | bytes 1572868
  36.4 17.5 %copy-start.2 = (bf16[256,1024]{1,0:T(8,128)(2,1)S(1)}, bf16[256,1024]{1,0:T(8,128)(2,1)}, u32[]{:S(2)}) copy-start(bf16[256,1024]{1,0:T(8,128)(2,1)} %get-tuple-element.13.reading) | copy-start | bytes 1572868
  36.4 17.5 %copy-start.3 = (f32[128]{0:T(128)S(1)}, f32[128]{0:T(128)}, u32[]{:S(2)}) copy-start(f32[128]{0:T(128)} %param.12) | copy-start | bytes 1540
  54.9 9.0 %collective-permute-start = (bf16[128,2048]{1,0:T(8,128)(2,1)S(1)}, bf16[128,2048]{1,0:T(8,128)(2,1)S(1)}, u32[]{:S(2)}, u32[]{:S(2)}) collective-permute-start(bf16[128,2048]{1,0:T(8,128)(2,1)S(1)} %away.1), channel_id=1, source_target_pairs={{0,1},{1,0},{2,3},{3,2},{4,5},{5,4},{6,7},{7,6},{8,9},{9,8},{10,11... | collective-permute-start | bytes 1572872 | tf_op jit(solution)/shard_map/ppermute | solution.py:333

commit v11 on v9

--- a/solution.py
+++ b/solution.py
@@ -73,24 +73,33 @@
     rows = HEAD // slabs
     r, c = rows_and_columns((tokens, tokens))
     later = (c > r).astype(BF16)
-    for copy in copies[:-1]:
+    for copy in copies:
         copy.wait()
     by_token = extra[...].T
 
     def chain(p):
         lanes = slice(p * wide, (p + 1) * wide)
-        keyed, log_decay = keyed_and_log_decay(
-            retention[:, lanes], slack[:, lanes], for_pair(by_token, p)
+        added = for_pair(by_token, p)
+        halves = []
+        for q in range(2):
+            span = slice(q * tokens // 2, (q + 1) * tokens // 2)
+            halves.append(
+                keyed_and_log_decay(retention[span, lanes], slack[:, lanes], added[span])
+            )
+            yield
+        log_decay = jnp.concatenate([x[1] for x in halves], axis=0)
+        high, low = two_parts(log_decay)
+        ahead = []
+        for q in range(2):
+            part = later[q * tokens // 2 : (q + 1) * tokens // 2]
+            ahead.append(dot(part, high, ((1,), (0,))) + dot(part, low, ((1,), (0,))))
+            yield
+        sent = jnp.concatenate(
+            [(halves[q][0] * jnp.exp(ahead[q])).astype(BF16) for q in range(2)], axis=0
         )
-        yield
-        ahead = summed_rows(later, log_decay)
-        yield
-        sent = (keyed * jnp.exp(ahead)).astype(BF16)
-        total = ahead[:1] + log_decay[:1]
+        total = ahead[0][:1] + log_decay[:1]
         parts = jnp.concatenate(two_parts(total), axis=0)
         yield
-        if p == 0:
-            copies[-1].wait()
         for k in range(2):
             part = slice(k * HEAD, (k + 1) * HEAD)
             h = 2 * p + k
@@ -109,9 +118,11 @@
 def scan_kernel(slabs, message, entering, by_channel):
     positions, rows, _ = entering.shape
     slab = lax.rem(lax.axis_index(SP), slabs)
-    parts = message[:, rows // 2].astype(F32)
-    by_channel[...] = jnp.exp(parts[:, 0] + parts[:, 1]).T
-    mine = by_channel[pl.ds(pl.multiple_of(slab * rows, rows), rows), :]
+    r, c = rows_and_columns((2 * positions, positions))
+    pairs = (r // 2 == c).astype(BF16)
+    decays = message[:, rows // 2].reshape(2 * positions, HEAD)
+    by_channel[...] = dot(decays, pairs, ((0,), (0,)))
+    mine = jnp.exp(by_channel[pl.ds(pl.multiple_of(slab * rows, rows), rows), :])
     state = jnp.zeros((rows, HEAD), F32)
     for i in range(positions):
         entering[i] = state.astype(BF16)

time: 65.1 us -> 65.1 us (level)
  no operation moved by 1% of the time
where the time goes in v11:
time: 65.1 us; the launch traced here: 64.8 us
  starting transfers between devices  29.3 us (45%)
  blocking collectives  17 us (26%)
  Pallas kernels  10.5 us (16%)
  waiting for transfers between devices  7.93 us (12%)
    all_to_all x1, starting transfers between devices, body(): lax.all_to_all(message, SP, split_axis=0, concat_axis=0, tiled=True)  21.8 us
    all_to_all x1, blocking collectives, body(): lax.all_to_all(scanned, SP, split_axis=0, concat_axis=0, tiled=True)  17 us
    pallas_call x6, Pallas kernels, call(): pl.pallas_call(kernel, name=name, out_shape=outs, in_specs=[IN_HBM] * len...  10.5 us
    ppermute x1, starting transfers between devices, body(): received = lax.ppermute(projected(True, BF16), 'tp', [(0, 1), (1, 0)])  7.5 us
    all_to_all x1, waiting for transfers between devices, body(): lax.all_to_all(message, SP, split_axis=0, concat_axis=0, tiled=True)  7.38 us
  transfers between devices with their start and end apart: 2, of which 2 were waited for; matrix products, arithmetic and copies ran while one was open for 0% of the time, Pallas kernels for 8%

profile of v11, /device:TPU:513, one launch (start us, length us, event | category | flops | bytes accessed | tf_op | source)
XLA Modules:
  0.0 64.8 jit_solution(18058210055663928736)
XLA Ops:
  0.0 3.2 %state.1 = bf16[64,9,2,128]{3,2,1,0:T(2,128)(2,1)} custom-call(bf16[256,1024]{1,0:T(8,128)(2,1)} %refs_0_.3, f32[8,256]{1,0:T(8,128)} %bitcast.8, f32[1,1024]{1,0:T(1,128)} %bitcast.10, bf16[256,1024]{1,0:T(8,128)(2,1)} %refs_3_.3), custom_call_target="tpu_custom_call" | custom-call | flops 268435456 | bytes 1355776 | tf_op jit(solution)/shard_map/state/pallas_call | solution.py:228
  3.2 21.8 %all-to-all-start = ((bf16[64,9,2,128]{3,2,1,0:T(2,128)(2,1)}), bf16[64,9,2,128]{3,2,1,0:T(2,128)(2,1)S(1)}, u32[]{:S(2)}, u32[]{:S(2)}) async-start(bf16[64,9,2,128]{3,2,1,0:T(2,128)(2,1)} %state.1), calls=%async_computation | async-start | bytes 589824 | tf_op jit(solution)/shard_map/all_to_all | solution.py:278
  25.1 4.0 %local.1 = (bf16[256,1024]{1,0:T(8,128)(2,1)}, bf16[256,1024]{1,0:T(8,128)(2,1)}) custom-call(bf16[256,1024]{1,0:T(8,128)(2,1)} %refs_0_.3, f32[8,256]{1,0:T(8,128)} %bitcast.9, f32[1,1024]{1,0:T(1,128)} %bitcast.11, bf16[256,1024]{1,0:T(8,128)(2,1)} %refs_3_.3, bf16[256,1024]{1,0:T(8,128)(2,1)} %refs_4_.1), custom_call_target="tpu_custom_call" | custom-call | flops 402653184 | bytes 2633728 | tf_op jit(solution)/shard_map/local/pallas_call | solution.py:228
  29.1 7.4 %all-to-all-done.message = bf16[64,9,2,128]{3,2,1,0:T(2,128)(2,1)S(1)} async-done(((bf16[64,9,2,128]{3,2,1,0:T(2,128)(2,1)}), bf16[64,9,2,128]{3,2,1,0:T(2,128)(2,1)S(1)}, u32[]{:S(2)}, u32[]{:S(2)}) %all-to-all-start) | async-done | bytes 294944 | tf_op jit(solution)/shard_map/all_to_all | solution.py:278
  36.5 0.0 copy-start
  36.5 0.0 copy-start.1
  36.5 0.0 copy-start.2
  36.5 0.0 copy-start.3
  36.5 0.5 scan.1
  37.0 17.0 %all_to_all.10 = bf16[64,16,128]{2,1,0:T(8,128)(2,1)S(1)} all-to-all(bf16[64,16,128]{2,1,0:T(8,128)(2,1)S(1)} %scan.1), channel_id=1, replica_groups=mesh['grp'=2,'sp_0'=8,'sp_1'=8,'tp'=2] {'sp_0','sp_1'}, dimensions={0} | all-to-all | bytes 524288 | tf_op jit(solution)/shard_map/all_to_all | solution.py:300
  53.9 0.0 copy-done
  54.0 0.0 copy-done.1
  54.0 0.0 copy-done.2
  54.0 0.0 copy-done.3
  54.0 1.0 %away.1 = bf16[128,2048]{1,0:T(8,128)(2,1)S(1)} custom-call(bf16[256,1024]{1,0:T(8,128)(2,1)S(1)} %copy-done.1, bf16[256,1024]{1,0:T(8,128)(2,1)S(1)} %copy-done.2, bf16[8,128,128]{2,1,0:T(8,128)(2,1)S(1)} %bitcast.4, f32[1,128]{1,0:T(1,128)S(1)} %bitcast.6, bf16[1024,2048]{1,0:T(8,128)(2,1)S(1)} %copy-done), custom_call_target="tpu_custom_call" | custom-call | flops 536870912 | bytes 6029824 | tf_op jit(solution)/shard_map/away/pallas_call | solution.py:228
  55.0 7.5 %collective-permute-start = (bf16[128,2048]{1,0:T(8,128)(2,1)S(1)}, bf16[128,2048]{1,0:T(8,128)(2,1)S(1)}, u32[]{:S(2)}, u32[]{:S(2)}) collective-permute-start(bf16[128,2048]{1,0:T(8,128)(2,1)S(1)} %away.1), channel_id=1, source_target_pairs={{0,1},{1,0},{2,3},{3,2},{4,5},{5,4},{6,7},{7,6},{8,9},{9,8},{10,11... | collective-permute-start | bytes 1572872 | tf_op jit(solution)/shard_map/ppermute | solution.py:315
  62.5 1.0 %kept.1 = f32[128,2048]{1,0:T(8,128)S(1)} custom-call(bf16[256,1024]{1,0:T(8,128)(2,1)S(1)} %copy-done.1, bf16[256,1024]{1,0:T(8,128)(2,1)S(1)} %copy-done.2, bf16[8,128,128]{2,1,0:T(8,128)(2,1)S(1)} %bitcast.5, f32[1,128]{1,0:T(1,128)S(1)} %bitcast.7, bf16[1024,2048]{1,0:T(8,128)(2,1)S(1)} %copy-done), custom_call_target="tpu_custom_call" | custom-call | flops 536870912 | bytes 6554112 | tf_op jit(solution)/shard_map/kept/pallas_call | solution.py:228
  63.5 0.5 collective-permute-done.received
  64.0 0.8 %final.1 = bf16[128,2048]{1,0:T(8,128)(2,1)} custom-call(f32[128,2048]{1,0:T(8,128)S(1)} %kept.1, bf16[128,2048]{1,0:T(8,128)(2,1)S(1)} %collective-permute-done.received), custom_call_target="tpu_custom_call" | custom-call | flops 262144 | bytes 2097152 | tf_op jit(solution)/shard_map/final/pallas_call | solution.py:228
Async XLA Ops:
  3.2 33.2 %all-to-all-start = ((bf16[64,9,2,128]{3,2,1,0:T(2,128)(2,1)}), bf16[64,9,2,128]{3,2,1,0:T(2,128)(2,1)S(1)}, u32[]{:S(2)}, u32[]{:S(2)}) async-start(bf16[64,9,2,128]{3,2,1,0:T(2,128)(2,1)} %state.1), calls=%async_computation | async-start | bytes 589824 | tf_op jit(solution)/shard_map/all_to_all | solution.py:278
  36.5 17.5 %copy-start = (bf16[1024,2048]{1,0:T(8,128)(2,1)S(1)}, bf16[1024,2048]{1,0:T(8,128)(2,1)}, u32[]{:S(2)}) copy-start(bf16[1024,2048]{1,0:T(8,128)(2,1)} %matrix.3) | copy-start | bytes 12582916
  36.5 17.5 %copy-start.1 = (bf16[256,1024]{1,0:T(8,128)(2,1)S(1)}, bf16[256,1024]{1,0:T(8,128)(2,1)}, u32[]{:S(2)}) copy-start(bf16[256,1024]{1,0:T(8,128)(2,1)} %get-tuple-element.12.inside) | copy-start | bytes 1572868
  36.5 17.5 %copy-start.2 = (bf16[256,1024]{1,0:T(8,128)(2,1)S(1)}, bf16[256,1024]{1,0:T(8,128)(2,1)}, u32[]{:S(2)}) copy-start(bf16[256,1024]{1,0:T(8,128)(2,1)} %get-tuple-element.13.reading) | copy-start | bytes 1572868
  36.5 17.5 %copy-start.3 = (f32[128]{0:T(128)S(1)}, f32[128]{0:T(128)}, u32[]{:S(2)}) copy-start(f32[128]{0:T(128)} %param.12) | copy-start | bytes 1540
  55.0 9.0 %collective-permute-start = (bf16[128,2048]{1,0:T(8,128)(2,1)S(1)}, bf16[128,2048]{1,0:T(8,128)(2,1)S(1)}, u32[]{:S(2)}, u32[]{:S(2)}) collective-permute-start(bf16[128,2048]{1,0:T(8,128)(2,1)S(1)} %away.1), channel_id=1, source_target_pairs={{0,1},{1,0},{2,3},{3,2},{4,5},{5,4},{6,7},{7,6},{8,9},{9,8},{10,11... | collective-permute-start | bytes 1572872 | tf_op jit(solution)/shard_map/ppermute | solution.py:315

commit v12 on v9

--- a/solution.py
+++ b/solution.py
@@ -49,11 +49,29 @@
     )
 
 
+PIECES = 4
+
+
 def copied(pairs, sems):
-    copies = [pltpu.make_async_copy(a, b, sems.at[i]) for i, (a, b) in enumerate(pairs)]
-    for copy in copies:
-        copy.start()
-    return copies
+    groups = []
+    for i, (source, target) in enumerate(pairs):
+        rows = source.shape[0]
+        pieces = PIECES if rows % (PIECES * 16) == 0 else 1
+        group = []
+        for k in range(pieces):
+            span = pl.ds(k * (rows // pieces), rows // pieces)
+            group.append(
+                pltpu.make_async_copy(source.at[span], target.at[span], sems.at[i, k])
+            )
+            group[-1].start()
+        groups.append(group)
+    return groups
+
+
+def wait_all(groups):
+    for group in groups:
+        for copy in group:
+            copy.wait()
 
 
 def staggered(make, count):
@@ -73,8 +91,7 @@
     rows = HEAD // slabs
     r, c = rows_and_columns((tokens, tokens))
     later = (c > r).astype(BF16)
-    for copy in copies[:-1]:
-        copy.wait()
+    wait_all(copies[:-1])
     by_token = extra[...].T
 
     def chain(p):
@@ -90,7 +107,7 @@
         parts = jnp.concatenate(two_parts(total), axis=0)
         yield
         if p == 0:
-            copies[-1].wait()
+            wait_all(copies[-1:])
         for k in range(2):
             part = slice(k * HEAD, (k + 1) * HEAD)
             h = 2 * p + k
@@ -128,8 +145,7 @@
     within = ((c <= r) & (r // SPAN == c // SPAN)).astype(BF16)
     r, c = rows_and_columns((SPAN, SPAN))
     upto = c <= r
-    for copy in copies:
-        copy.wait()
+    wait_all(copies)
     by_token = extra[...].T
 
     def chain(p):
@@ -251,7 +267,7 @@
     def near(arrays):
         return (
             tuple(pltpu.VMEM(a.shape, a.dtype) for a in arrays),
-            pltpu.SemaphoreType.DMA((len(arrays),)),
+            pltpu.SemaphoreType.DMA((len(arrays), PIECES)),
         )
 
     message = call(

time: 65.1 us -> 65.2 us (level)
  no operation moved by 1% of the time
where the time goes in v12:
time: 65.2 us; the launch traced here: 65 us
  starting transfers between devices  29.2 us (45%)
  blocking collectives  17.1 us (26%)
  Pallas kernels  10.9 us (17%)
  waiting for transfers between devices  7.72 us (12%)
    all_to_all x1, starting transfers between devices, body(): lax.all_to_all(message, SP, split_axis=0, concat_axis=0, tiled=True)  21.8 us
    all_to_all x1, blocking collectives, body(): lax.all_to_all(scanned, SP, split_axis=0, concat_axis=0, tiled=True)  17.1 us
    pallas_call x6, Pallas kernels, call(): pl.pallas_call(kernel, name=name, out_shape=outs, in_specs=[IN_HBM] * len...  10.9 us
    ppermute x1, starting transfers between devices, body(): received = lax.ppermute(projected(True, BF16), 'tp', [(0, 1), (1, 0)])  7.39 us
    all_to_all x1, waiting for transfers between devices, body(): lax.all_to_all(message, SP, split_axis=0, concat_axis=0, tiled=True)  7.17 us
  transfers between devices with their start and end apart: 2, of which 2 were waited for; matrix products, arithmetic and copies ran while one was open for 0% of the time, Pallas kernels for 8%

profile of v12, /device:TPU:513, one launch (start us, length us, event | category | flops | bytes accessed | tf_op | source)
XLA Modules:
  0.0 65.0 jit_solution(7539004170763038081)
XLA Ops:
  0.0 3.4 %state.1 = bf16[64,9,2,128]{3,2,1,0:T(2,128)(2,1)} custom-call(bf16[256,1024]{1,0:T(8,128)(2,1)} %refs_0_.3, f32[8,256]{1,0:T(8,128)} %bitcast.8, f32[1,1024]{1,0:T(1,128)} %bitcast.10, bf16[256,1024]{1,0:T(8,128)(2,1)} %refs_3_.3), custom_call_target="tpu_custom_call" | custom-call | flops 268435456 | bytes 1355776 | tf_op jit(solution)/shard_map/state/pallas_call | solution.py:233
  3.4 21.8 %all-to-all-start = ((bf16[64,9,2,128]{3,2,1,0:T(2,128)(2,1)}), bf16[64,9,2,128]{3,2,1,0:T(2,128)(2,1)S(1)}, u32[]{:S(2)}, u32[]{:S(2)}) async-start(bf16[64,9,2,128]{3,2,1,0:T(2,128)(2,1)} %state.1), calls=%async_computation | async-start | bytes 589824 | tf_op jit(solution)/shard_map/all_to_all | solution.py:283
  25.3 4.2 %local.1 = (bf16[256,1024]{1,0:T(8,128)(2,1)}, bf16[256,1024]{1,0:T(8,128)(2,1)}) custom-call(bf16[256,1024]{1,0:T(8,128)(2,1)} %refs_0_.3, f32[8,256]{1,0:T(8,128)} %bitcast.9, f32[1,1024]{1,0:T(1,128)} %bitcast.11, bf16[256,1024]{1,0:T(8,128)(2,1)} %refs_3_.3, bf16[256,1024]{1,0:T(8,128)(2,1)} %refs_4_.1), custom_call_target="tpu_custom_call" | custom-call | flops 402653184 | bytes 2633728 | tf_op jit(solution)/shard_map/local/pallas_call | solution.py:233
  29.5 7.2 %all-to-all-done.message = bf16[64,9,2,128]{3,2,1,0:T(2,128)(2,1)S(1)} async-done(((bf16[64,9,2,128]{3,2,1,0:T(2,128)(2,1)}), bf16[64,9,2,128]{3,2,1,0:T(2,128)(2,1)S(1)}, u32[]{:S(2)}, u32[]{:S(2)}) %all-to-all-start) | async-done | bytes 294944 | tf_op jit(solution)/shard_map/all_to_all | solution.py:283
  36.6 0.0 copy-start
  36.6 0.0 copy-start.1
  36.7 0.0 copy-start.2
  36.7 0.0 copy-start.3
  36.7 0.5 scan.1
  37.1 17.1 %all_to_all.10 = bf16[64,16,128]{2,1,0:T(8,128)(2,1)S(1)} all-to-all(bf16[64,16,128]{2,1,0:T(8,128)(2,1)S(1)} %scan.1), channel_id=1, replica_groups=mesh['grp'=2,'sp_0'=8,'sp_1'=8,'tp'=2] {'sp_0','sp_1'}, dimensions={0} | all-to-all | bytes 524288 | tf_op jit(solution)/shard_map/all_to_all | solution.py:305
  54.2 0.0 copy-done
  54.2 0.0 copy-done.1
  54.2 0.0 copy-done.2
  54.2 0.0 copy-done.3
  54.2 1.0 %away.1 = bf16[128,2048]{1,0:T(8,128)(2,1)S(1)} custom-call(bf16[256,1024]{1,0:T(8,128)(2,1)S(1)} %copy-done.1, bf16[256,1024]{1,0:T(8,128)(2,1)S(1)} %copy-done.2, bf16[8,128,128]{2,1,0:T(8,128)(2,1)S(1)} %bitcast.4, f32[1,128]{1,0:T(1,128)S(1)} %bitcast.6, bf16[1024,2048]{1,0:T(8,128)(2,1)S(1)} %copy-done), custom_call_target="tpu_custom_call" | custom-call | flops 536870912 | bytes 6029824 | tf_op jit(solution)/shard_map/away/pallas_call | solution.py:233
  55.2 7.4 %collective-permute-start = (bf16[128,2048]{1,0:T(8,128)(2,1)S(1)}, bf16[128,2048]{1,0:T(8,128)(2,1)S(1)}, u32[]{:S(2)}, u32[]{:S(2)}) collective-permute-start(bf16[128,2048]{1,0:T(8,128)(2,1)S(1)} %away.1), channel_id=1, source_target_pairs={{0,1},{1,0},{2,3},{3,2},{4,5},{5,4},{6,7},{7,6},{8,9},{9,8},{10,11... | collective-permute-start | bytes 1572872 | tf_op jit(solution)/shard_map/ppermute | solution.py:320
  62.6 1.0 %kept.1 = f32[128,2048]{1,0:T(8,128)S(1)} custom-call(bf16[256,1024]{1,0:T(8,128)(2,1)S(1)} %copy-done.1, bf16[256,1024]{1,0:T(8,128)(2,1)S(1)} %copy-done.2, bf16[8,128,128]{2,1,0:T(8,128)(2,1)S(1)} %bitcast.5, f32[1,128]{1,0:T(1,128)S(1)} %bitcast.7, bf16[1024,2048]{1,0:T(8,128)(2,1)S(1)} %copy-done), custom_call_target="tpu_custom_call" | custom-call | flops 536870912 | bytes 6554112 | tf_op jit(solution)/shard_map/kept/pallas_call | solution.py:233
  63.6 0.5 collective-permute-done.received
  64.1 0.8 %final.1 = bf16[128,2048]{1,0:T(8,128)(2,1)} custom-call(f32[128,2048]{1,0:T(8,128)S(1)} %kept.1, bf16[128,2048]{1,0:T(8,128)(2,1)S(1)} %collective-permute-done.received), custom_call_target="tpu_custom_call" | custom-call | flops 262144 | bytes 2097152 | tf_op jit(solution)/shard_map/final/pallas_call | solution.py:233
Async XLA Ops:
  3.4 33.2 %all-to-all-start = ((bf16[64,9,2,128]{3,2,1,0:T(2,128)(2,1)}), bf16[64,9,2,128]{3,2,1,0:T(2,128)(2,1)S(1)}, u32[]{:S(2)}, u32[]{:S(2)}) async-start(bf16[64,9,2,128]{3,2,1,0:T(2,128)(2,1)} %state.1), calls=%async_computation | async-start | bytes 589824 | tf_op jit(solution)/shard_map/all_to_all | solution.py:283
  36.6 17.6 %copy-start = (bf16[1024,2048]{1,0:T(8,128)(2,1)S(1)}, bf16[1024,2048]{1,0:T(8,128)(2,1)}, u32[]{:S(2)}) copy-start(bf16[1024,2048]{1,0:T(8,128)(2,1)} %matrix.3) | copy-start | bytes 12582916
  36.6 17.6 %copy-start.1 = (bf16[256,1024]{1,0:T(8,128)(2,1)S(1)}, bf16[256,1024]{1,0:T(8,128)(2,1)}, u32[]{:S(2)}) copy-start(bf16[256,1024]{1,0:T(8,128)(2,1)} %get-tuple-element.12.inside) | copy-start | bytes 1572868
  36.7 17.6 %copy-start.2 = (bf16[256,1024]{1,0:T(8,128)(2,1)S(1)}, bf16[256,1024]{1,0:T(8,128)(2,1)}, u32[]{:S(2)}) copy-start(bf16[256,1024]{1,0:T(8,128)(2,1)} %get-tuple-element.13.reading) | copy-start | bytes 1572868
  36.7 17.6 %copy-start.3 = (f32[128]{0:T(128)S(1)}, f32[128]{0:T(128)}, u32[]{:S(2)}) copy-start(f32[128]{0:T(128)} %param.12) | copy-start | bytes 1540
  55.2 8.9 %collective-permute-start = (bf16[128,2048]{1,0:T(8,128)(2,1)S(1)}, bf16[128,2048]{1,0:T(8,128)(2,1)S(1)}, u32[]{:S(2)}, u32[]{:S(2)}) collective-permute-start(bf16[128,2048]{1,0:T(8,128)(2,1)S(1)} %away.1), channel_id=1, source_target_pairs={{0,1},{1,0},{2,3},{3,2},{4,5},{5,4},{6,7},{7,6},{8,9},{9,8},{10,11... | collective-permute-start | bytes 1572872 | tf_op jit(solution)/shard_map/ppermute | solution.py:320

commit v13 on v9

--- a/solution.py
+++ b/solution.py
@@ -5,14 +5,13 @@
 from jax import lax
 from jax.experimental import pallas as pl
 from jax.experimental.pallas import tpu as pltpu
-from jax.sharding import Mesh
 from jax.sharding import PartitionSpec as P
 
 SPAN = 128
 HEAD = 128
-SP = ("sp_0", "sp_1")
-GRP_SP = ("grp", "sp_0", "sp_1")
-GRP_SP_TP = ("grp", "sp_0", "sp_1", "tp")
+SP = "sp"
+GRP_SP = ("grp", "sp")
+GRP_SP_TP = ("grp", "sp", "tp")
 F32 = jnp.float32
 BF16 = jnp.bfloat16
 
@@ -316,10 +315,6 @@
 
 
 def solution(mesh):
-    finer = Mesh(
-        mesh.devices.reshape(mesh.shape["grp"], 8, 8, mesh.shape["tp"]),
-        ("grp", "sp_0", "sp_1", "tp"),
-    )
     in_specs = (
         P(GRP_SP, "tp"),
         P(GRP_SP, "tp"),
@@ -330,4 +325,4 @@
         P("tp", None),
     )
     out_specs = P(GRP_SP_TP, None)
-    return jax.shard_map(body, mesh=finer, in_specs=in_specs, out_specs=out_specs, check_vma=False)
+    return jax.shard_map(body, mesh=mesh, in_specs=in_specs, out_specs=out_specs, check_vma=False)

time: 65.1 us -> 65.1 us (level)
  no operation moved by 1% of the time
where the time goes in v13:
time: 65.1 us; the launch traced here: 64.8 us
  starting transfers between devices  29.3 us (45%)
  blocking collectives  17 us (26%)
  Pallas kernels  10.5 us (16%)
  waiting for transfers between devices  7.93 us (12%)
    all_to_all x1, starting transfers between devices, body(): lax.all_to_all(message, SP, split_axis=0, concat_axis=0, tiled=True)  21.8 us
    all_to_all x1, blocking collectives, body(): lax.all_to_all(scanned, SP, split_axis=0, concat_axis=0, tiled=True)  17 us
    pallas_call x6, Pallas kernels, call(): pl.pallas_call(kernel, name=name, out_shape=outs, in_specs=[IN_HBM] * len...  10.5 us
    ppermute x1, starting transfers between devices, body(): received = lax.ppermute(projected(True, BF16), 'tp', [(0, 1), (1, 0)])  7.5 us
    all_to_all x1, waiting for transfers between devices, body(): lax.all_to_all(message, SP, split_axis=0, concat_axis=0, tiled=True)  7.38 us
  transfers between devices with their start and end apart: 2, of which 2 were waited for; matrix products, arithmetic and copies ran while one was open for 0% of the time, Pallas kernels for 8%

profile of v13, /device:TPU:513, one launch (start us, length us, event | category | flops | bytes accessed | tf_op | source)
XLA Modules:
  0.0 64.8 jit_solution(9321328702512760004)
XLA Ops:
  0.0 3.2 %state.1 = bf16[64,9,2,128]{3,2,1,0:T(2,128)(2,1)} custom-call(bf16[256,1024]{1,0:T(8,128)(2,1)} %refs_0_.3, f32[8,256]{1,0:T(8,128)} %bitcast.8, f32[1,1024]{1,0:T(1,128)} %bitcast.10, bf16[256,1024]{1,0:T(8,128)(2,1)} %refs_3_.3), custom_call_target="tpu_custom_call" | custom-call | flops 268435456 | bytes 1355776 | tf_op jit(solution)/shard_map/state/pallas_call | solution.py:216
  3.2 21.8 %all-to-all-start = ((bf16[64,9,2,128]{3,2,1,0:T(2,128)(2,1)}), bf16[64,9,2,128]{3,2,1,0:T(2,128)(2,1)S(1)}, u32[]{:S(2)}, u32[]{:S(2)}) async-start(bf16[64,9,2,128]{3,2,1,0:T(2,128)(2,1)} %state.1), calls=%async_computation | async-start | bytes 589824 | tf_op jit(solution)/shard_map/all_to_all | solution.py:266
  25.1 4.0 %local.1 = (bf16[256,1024]{1,0:T(8,128)(2,1)}, bf16[256,1024]{1,0:T(8,128)(2,1)}) custom-call(bf16[256,1024]{1,0:T(8,128)(2,1)} %refs_0_.3, f32[8,256]{1,0:T(8,128)} %bitcast.9, f32[1,1024]{1,0:T(1,128)} %bitcast.11, bf16[256,1024]{1,0:T(8,128)(2,1)} %refs_3_.3, bf16[256,1024]{1,0:T(8,128)(2,1)} %refs_4_.1), custom_call_target="tpu_custom_call" | custom-call | flops 402653184 | bytes 2633728 | tf_op jit(solution)/shard_map/local/pallas_call | solution.py:216
  29.1 7.4 %all-to-all-done.message = bf16[64,9,2,128]{3,2,1,0:T(2,128)(2,1)S(1)} async-done(((bf16[64,9,2,128]{3,2,1,0:T(2,128)(2,1)}), bf16[64,9,2,128]{3,2,1,0:T(2,128)(2,1)S(1)}, u32[]{:S(2)}, u32[]{:S(2)}) %all-to-all-start) | async-done | bytes 294944 | tf_op jit(solution)/shard_map/all_to_all | solution.py:266
  36.5 0.0 copy-start
  36.5 0.0 copy-start.1
  36.5 0.0 copy-start.2
  36.5 0.0 copy-start.3
  36.5 0.5 scan.1
  36.9 17.0 %all_to_all.10 = bf16[64,16,128]{2,1,0:T(8,128)(2,1)S(1)} all-to-all(bf16[64,16,128]{2,1,0:T(8,128)(2,1)S(1)} %scan.1), channel_id=1, replica_groups=mesh['grp'=2,'sp'=64,'tp'=2] {'sp'}, dimensions={0} | all-to-all | bytes 524288 | tf_op jit(solution)/shard_map/all_to_all | solution.py:288
  53.9 0.0 copy-done
  53.9 0.0 copy-done.1
  53.9 0.0 copy-done.2
  53.9 0.0 copy-done.3
  53.9 1.0 %away.1 = bf16[128,2048]{1,0:T(8,128)(2,1)S(1)} custom-call(bf16[256,1024]{1,0:T(8,128)(2,1)S(1)} %copy-done.1, bf16[256,1024]{1,0:T(8,128)(2,1)S(1)} %copy-done.2, bf16[8,128,128]{2,1,0:T(8,128)(2,1)S(1)} %bitcast.4, f32[1,128]{1,0:T(1,128)S(1)} %bitcast.6, bf16[1024,2048]{1,0:T(8,128)(2,1)S(1)} %copy-done), custom_call_target="tpu_custom_call" | custom-call | flops 536870912 | bytes 6029824 | tf_op jit(solution)/shard_map/away/pallas_call | solution.py:216
  54.9 7.5 %collective-permute-start = (bf16[128,2048]{1,0:T(8,128)(2,1)S(1)}, bf16[128,2048]{1,0:T(8,128)(2,1)S(1)}, u32[]{:S(2)}, u32[]{:S(2)}) collective-permute-start(bf16[128,2048]{1,0:T(8,128)(2,1)S(1)} %away.1), channel_id=1, source_target_pairs={{0,1},{1,0},{2,3},{3,2},{4,5},{5,4},{6,7},{7,6},{8,9},{9,8},{10,11... | collective-permute-start | bytes 1572872 | tf_op jit(solution)/shard_map/ppermute | solution.py:303
  62.4 1.0 %kept.1 = f32[128,2048]{1,0:T(8,128)S(1)} custom-call(bf16[256,1024]{1,0:T(8,128)(2,1)S(1)} %copy-done.1, bf16[256,1024]{1,0:T(8,128)(2,1)S(1)} %copy-done.2, bf16[8,128,128]{2,1,0:T(8,128)(2,1)S(1)} %bitcast.5, f32[1,128]{1,0:T(1,128)S(1)} %bitcast.7, bf16[1024,2048]{1,0:T(8,128)(2,1)S(1)} %copy-done), custom_call_target="tpu_custom_call" | custom-call | flops 536870912 | bytes 6554112 | tf_op jit(solution)/shard_map/kept/pallas_call | solution.py:216
  63.4 0.6 collective-permute-done.received
  64.0 0.8 %final.1 = bf16[128,2048]{1,0:T(8,128)(2,1)} custom-call(f32[128,2048]{1,0:T(8,128)S(1)} %kept.1, bf16[128,2048]{1,0:T(8,128)(2,1)S(1)} %collective-permute-done.received), custom_call_target="tpu_custom_call" | custom-call | flops 262144 | bytes 2097152 | tf_op jit(solution)/shard_map/final/pallas_call | solution.py:216
Async XLA Ops:
  3.2 33.2 %all-to-all-start = ((bf16[64,9,2,128]{3,2,1,0:T(2,128)(2,1)}), bf16[64,9,2,128]{3,2,1,0:T(2,128)(2,1)S(1)}, u32[]{:S(2)}, u32[]{:S(2)}) async-start(bf16[64,9,2,128]{3,2,1,0:T(2,128)(2,1)} %state.1), calls=%async_computation | async-start | bytes 589824 | tf_op jit(solution)/shard_map/all_to_all | solution.py:266
  36.5 17.5 %copy-start = (bf16[1024,2048]{1,0:T(8,128)(2,1)S(1)}, bf16[1024,2048]{1,0:T(8,128)(2,1)}, u32[]{:S(2)}) copy-start(bf16[1024,2048]{1,0:T(8,128)(2,1)} %matrix.3) | copy-start | bytes 12582916
  36.5 17.5 %copy-start.1 = (bf16[256,1024]{1,0:T(8,128)(2,1)S(1)}, bf16[256,1024]{1,0:T(8,128)(2,1)}, u32[]{:S(2)}) copy-start(bf16[256,1024]{1,0:T(8,128)(2,1)} %get-tuple-element.12.inside) | copy-start | bytes 1572868
  36.5 17.5 %copy-start.2 = (bf16[256,1024]{1,0:T(8,128)(2,1)S(1)}, bf16[256,1024]{1,0:T(8,128)(2,1)}, u32[]{:S(2)}) copy-start(bf16[256,1024]{1,0:T(8,128)(2,1)} %get-tuple-element.13.reading) | copy-start | bytes 1572868
  36.5 17.5 %copy-start.3 = (f32[128]{0:T(128)S(1)}, f32[128]{0:T(128)}, u32[]{:S(2)}) copy-start(f32[128]{0:T(128)} %param.12) | copy-start | bytes 1540
  54.9 9.0 %collective-permute-start = (bf16[128,2048]{1,0:T(8,128)(2,1)S(1)}, bf16[128,2048]{1,0:T(8,128)(2,1)S(1)}, u32[]{:S(2)}, u32[]{:S(2)}) collective-permute-start(bf16[128,2048]{1,0:T(8,128)(2,1)S(1)} %away.1), channel_id=1, source_target_pairs={{0,1},{1,0},{2,3},{3,2},{4,5},{5,4},{6,7},{7,6},{8,9},{9,8},{10,11... | collective-permute-start | bytes 1572872 | tf_op jit(solution)/shard_map/ppermute | solution.py:303

commit v14 on v13

--- a/solution.py
+++ b/solution.py
@@ -273,7 +273,7 @@
         [jax.ShapeDtypeStruct((tokens, channels), BF16)] * 2,
         6 * flops,
         near(inputs),
-        10300000,
+        11600000,
     )
     arrived, inside, reading = lax.optimization_barrier((arrived, inside, reading))
     scanned = call(

time: 65.1 us -> 65.1 us (level)
  local copies, waits for them, and re-layouts: 0.01 us -> 1.39 us
  Pallas kernels: 10.5 us -> 9.68 us
    unnamed x8, local copies, waits for them, and re-layouts: 0.01 us -> 1.39 us
    pallas_call x6, Pallas kernels: 10.5 us -> 9.68 us  [call(): pl.pallas_call(kernel, name=name, out_shape=outs, in_specs=[IN_HBM] * len...]
  transfers between devices with their start and end apart: 2 -> 2, of which waited for: 2 -> 2; matrix products, arithmetic and copies ran while one was open for 0% -> 0% of each run, Pallas kernels for 8% -> 6%
where the time goes in v14:
time: 65.1 us; the launch traced here: 64.8 us
  starting transfers between devices  29 us (45%)
  blocking collectives  17.4 us (27%)
  Pallas kernels  9.68 us (15%)
  waiting for transfers between devices  7.37 us (11%)
  local copies, waits for them, and re-layouts  1.39 us (2%)
    all_to_all x1, starting transfers between devices, body(): lax.all_to_all(message, SP, split_axis=0, concat_axis=0, tiled=True)  21.8 us
    all_to_all x1, blocking collectives, body(): lax.all_to_all(scanned, SP, split_axis=0, concat_axis=0, tiled=True)  17.4 us
    pallas_call x6, Pallas kernels, call(): pl.pallas_call(kernel, name=name, out_shape=outs, in_specs=[IN_HBM] * len...  9.68 us
    ppermute x1, starting transfers between devices, body(): received = lax.ppermute(projected(True, BF16), 'tp', [(0, 1), (1, 0)])  7.15 us
    all_to_all x1, waiting for transfers between devices, body(): lax.all_to_all(message, SP, split_axis=0, concat_axis=0, tiled=True)  6.82 us
    unnamed x8, local copies, waits for them, and re-layouts  1.39 us
  transfers between devices with their start and end apart: 2, of which 2 were waited for; matrix products, arithmetic and copies ran while one was open for 0% of the time, Pallas kernels for 6%

profile of v14, /device:TPU:513, one launch (start us, length us, event | category | flops | bytes accessed | tf_op | source)
XLA Modules:
  0.0 64.8 jit_solution(14602222703607293767)
XLA Ops:
  0.0 3.2 %state.1 = bf16[64,9,2,128]{3,2,1,0:T(2,128)(2,1)} custom-call(bf16[256,1024]{1,0:T(8,128)(2,1)} %refs_0_.3, f32[8,256]{1,0:T(8,128)} %bitcast.6, f32[1,1024]{1,0:T(1,128)} %bitcast.8, bf16[256,1024]{1,0:T(8,128)(2,1)} %refs_3_.3), custom_call_target="tpu_custom_call" | custom-call | flops 268435456 | bytes 1355776 | tf_op jit(solution)/shard_map/state/pallas_call | solution.py:216
  3.3 21.8 %all-to-all-start = ((bf16[64,9,2,128]{3,2,1,0:T(2,128)(2,1)}), bf16[64,9,2,128]{3,2,1,0:T(2,128)(2,1)S(1)}, u32[]{:S(2)}, u32[]{:S(2)}) async-start(bf16[64,9,2,128]{3,2,1,0:T(2,128)(2,1)} %state.1), calls=%async_computation | async-start | bytes 589824 | tf_op jit(solution)/shard_map/all_to_all | solution.py:266
  25.1 0.0 copy-start.1
  25.1 0.7 %copy-done.1 = f32[256,8]{0,1:T(8,128)S(1)} copy-done((f32[256,8]{0,1:T(8,128)S(1)}, f32[256,8]{0,1:T(8,128)}, u32[]{:S(2)}) %copy-start.1) | copy-done | bytes 8216
  25.8 0.0 copy-start.2
  25.8 0.7 %copy-done.2 = f32[1024]{0:T(1024)S(1)} copy-done((f32[1024]{0:T(1024)S(1)}, f32[1024]{0:T(1024)}, u32[]{:S(2)}) %copy-start.2) | copy-done | bytes 4120
  26.5 3.2 %local.1 = (bf16[256,1024]{1,0:T(8,128)(2,1)S(1)}, bf16[256,1024]{1,0:T(8,128)(2,1)S(1)}) custom-call(bf16[256,1024]{1,0:T(8,128)(2,1)} %refs_0_.3, f32[8,256]{1,0:T(8,128)S(1)} %bitcast.7, f32[1,1024]{1,0:T(1,128)S(1)} %bitcast.9, bf16[256,1024]{1,0:T(8,128)(2,1)} %refs_3_.3, bf16[256,1024]{1,0:T(8,128)(2,1)} %refs_4_.1), custom_call_target="tpu_custom_call" | custom-call | flops 402653184 | bytes 2633728 | tf_op jit(solution)/shard_map/local/pallas_call | solution.py:216
  29.6 6.8 %all-to-all-done.message = bf16[64,9,2,128]{3,2,1,0:T(2,128)(2,1)S(1)} async-done(((bf16[64,9,2,128]{3,2,1,0:T(2,128)(2,1)}), bf16[64,9,2,128]{3,2,1,0:T(2,128)(2,1)S(1)}, u32[]{:S(2)}, u32[]{:S(2)}) %all-to-all-start) | async-done | bytes 294944 | tf_op jit(solution)/shard_map/all_to_all | solution.py:266
  36.5 0.0 copy-start
  36.5 0.0 copy-start.3
  36.5 0.5 scan.1
  36.9 17.4 %all_to_all.10 = bf16[64,16,128]{2,1,0:T(8,128)(2,1)S(1)} all-to-all(bf16[64,16,128]{2,1,0:T(8,128)(2,1)S(1)} %scan.1), channel_id=1, replica_groups=mesh['grp'=2,'sp'=64,'tp'=2] {'sp'}, dimensions={0} | all-to-all | bytes 524288 | tf_op jit(solution)/shard_map/all_to_all | solution.py:288
  54.3 0.0 copy-done
  54.3 0.0 copy-done.3
  54.3 1.0 %away.1 = bf16[128,2048]{1,0:T(8,128)(2,1)S(1)} custom-call(bf16[256,1024]{1,0:T(8,128)(2,1)S(1)} %get-tuple-element.12.inside, bf16[256,1024]{1,0:T(8,128)(2,1)S(1)} %get-tuple-element.13.reading, bf16[8,128,128]{2,1,0:T(8,128)(2,1)S(1)} %bitcast.4, f32[1,128]{1,0:T(1,128)S(1)} %bitcast.10, bf16[1024,2048]{1,0:T(8,128)(2,1)S(1)} %copy-done), custom_call_target="tpu_custom_call" | custom-call | flops 536870912 | bytes 6029824 | tf_op jit(solution)/shard_map/away/pallas_call | solution.py:216
  55.3 7.1 %collective-permute-start = (bf16[128,2048]{1,0:T(8,128)(2,1)S(1)}, bf16[128,2048]{1,0:T(8,128)(2,1)S(1)}, u32[]{:S(2)}, u32[]{:S(2)}) collective-permute-start(bf16[128,2048]{1,0:T(8,128)(2,1)S(1)} %away.1), channel_id=1, source_target_pairs={{0,1},{1,0},{2,3},{3,2},{4,5},{5,4},{6,7},{7,6},{8,9},{9,8},{10,11... | collective-permute-start | bytes 1572872 | tf_op jit(solution)/shard_map/ppermute | solution.py:303
  62.4 1.0 %kept.1 = f32[128,2048]{1,0:T(8,128)S(1)} custom-call(bf16[256,1024]{1,0:T(8,128)(2,1)S(1)} %get-tuple-element.12.inside, bf16[256,1024]{1,0:T(8,128)(2,1)S(1)} %get-tuple-element.13.reading, bf16[8,128,128]{2,1,0:T(8,128)(2,1)S(1)} %bitcast.5, f32[1,128]{1,0:T(1,128)S(1)} %bitcast.11, bf16[1024,2048]{1,0:T(8,128)(2,1)S(1)} %copy-done), custom_call_target="tpu_custom_call" | custom-call | flops 536870912 | bytes 6554112 | tf_op jit(solution)/shard_map/kept/pallas_call | solution.py:216
  63.4 0.6 collective-permute-done.received
  64.0 0.8 %final.1 = bf16[128,2048]{1,0:T(8,128)(2,1)} custom-call(f32[128,2048]{1,0:T(8,128)S(1)} %kept.1, bf16[128,2048]{1,0:T(8,128)(2,1)S(1)} %collective-permute-done.received), custom_call_target="tpu_custom_call" | custom-call | flops 262144 | bytes 2097152 | tf_op jit(solution)/shard_map/final/pallas_call | solution.py:216
Async XLA Ops:
  3.3 33.2 %all-to-all-start = ((bf16[64,9,2,128]{3,2,1,0:T(2,128)(2,1)}), bf16[64,9,2,128]{3,2,1,0:T(2,128)(2,1)S(1)}, u32[]{:S(2)}, u32[]{:S(2)}) async-start(bf16[64,9,2,128]{3,2,1,0:T(2,128)(2,1)} %state.1), calls=%async_computation | async-start | bytes 589824 | tf_op jit(solution)/shard_map/all_to_all | solution.py:266
  25.1 0.7 %copy-start.1 = (f32[256,8]{0,1:T(8,128)S(1)}, f32[256,8]{0,1:T(8,128)}, u32[]{:S(2)}) copy-start(f32[256,8]{0,1:T(8,128)} %param.10) | copy-start | bytes 24580
  25.8 0.7 %copy-start.2 = (f32[1024]{0:T(1024)S(1)}, f32[1024]{0:T(1024)}, u32[]{:S(2)}) copy-start(f32[1024]{0:T(1024)} %param.11) | copy-start | bytes 12292
  36.5 17.8 %copy-start = (bf16[1024,2048]{1,0:T(8,128)(2,1)S(1)}, bf16[1024,2048]{1,0:T(8,128)(2,1)}, u32[]{:S(2)}) copy-start(bf16[1024,2048]{1,0:T(8,128)(2,1)} %matrix.3) | copy-start | bytes 12582916
  36.5 17.8 %copy-start.3 = (f32[128]{0:T(128)S(1)}, f32[128]{0:T(128)}, u32[]{:S(2)}) copy-start(f32[128]{0:T(128)} %param.12) | copy-start | bytes 1540
  55.3 8.7 %collective-permute-start = (bf16[128,2048]{1,0:T(8,128)(2,1)S(1)}, bf16[128,2048]{1,0:T(8,128)(2,1)S(1)}, u32[]{:S(2)}, u32[]{:S(2)}) collective-permute-start(bf16[128,2048]{1,0:T(8,128)(2,1)S(1)} %away.1), channel_id=1, source_target_pairs={{0,1},{1,0},{2,3},{3,2},{4,5},{5,4},{6,7},{7,6},{8,9},{9,8},{10,11... | collective-permute-start | bytes 1572872 | tf_op jit(solution)/shard_map/ppermute | solution.py:303

commit v15 on v13

--- a/solution.py
+++ b/solution.py
@@ -185,11 +185,17 @@
     mine = lax.axis_index("tp")
     half = 1 - mine if away else mine
     rows = pl.ds(pl.multiple_of(half * tokens, tokens), tokens)
-    for h in range(entering.shape[0]):
+
+    def chain(h):
         lanes = slice(h * HEAD, (h + 1) * HEAD)
-        mixer = inside[rows, lanes] + dot(reading[rows, lanes], entering[h], ((1,), (0,)))
+        read = dot(reading[rows, lanes], entering[h], ((1,), (0,)))
+        yield
+        mixer = inside[rows, lanes] + read
         scale = lax.rsqrt(jnp.mean(mixer * mixer, axis=-1, keepdims=True) + 1e-06)
+        yield
         normed[:, lanes] = (mixer * scale * gain[...]).astype(BF16)
+
+    staggered(chain, entering.shape[0])
     out[...] = dot(normed[...], matrix[...], ((1,), (0,))).astype(out.dtype)
 
 

time: 65.1 us -> 65.1 us (level)
  no operation moved by 1% of the time
where the time goes in v15:
time: 65.1 us; the launch traced here: 64.8 us
  starting transfers between devices  29.3 us (45%)
  blocking collectives  17 us (26%)
  Pallas kernels  10.5 us (16%)
  waiting for transfers between devices  7.93 us (12%)
    all_to_all x1, starting transfers between devices, body(): lax.all_to_all(message, SP, split_axis=0, concat_axis=0, tiled=True)  21.8 us
    all_to_all x1, blocking collectives, body(): lax.all_to_all(scanned, SP, split_axis=0, concat_axis=0, tiled=True)  17 us
    pallas_call x6, Pallas kernels, call(): pl.pallas_call(kernel, name=name, out_shape=outs, in_specs=[IN_HBM] * len...  10.5 us
    ppermute x1, starting transfers between devices, body(): received = lax.ppermute(projected(True, BF16), 'tp', [(0, 1), (1, 0)])  7.5 us
    all_to_all x1, waiting for transfers between devices, body(): lax.all_to_all(message, SP, split_axis=0, concat_axis=0, tiled=True)  7.38 us
  transfers between devices with their start and end apart: 2, of which 2 were waited for; matrix products, arithmetic and copies ran while one was open for 0% of the time, Pallas kernels for 8%

profile of v15, /device:TPU:513, one launch (start us, length us, event | category | flops | bytes accessed | tf_op | source)
XLA Modules:
  0.0 64.8 jit_solution(4526320162496697979)
XLA Ops:
  0.0 3.2 %state.1 = bf16[64,9,2,128]{3,2,1,0:T(2,128)(2,1)} custom-call(bf16[256,1024]{1,0:T(8,128)(2,1)} %refs_0_.3, f32[8,256]{1,0:T(8,128)} %bitcast.8, f32[1,1024]{1,0:T(1,128)} %bitcast.10, bf16[256,1024]{1,0:T(8,128)(2,1)} %refs_3_.3), custom_call_target="tpu_custom_call" | custom-call | flops 268435456 | bytes 1355776 | tf_op jit(solution)/shard_map/state/pallas_call | solution.py:222
  3.2 21.8 %all-to-all-start = ((bf16[64,9,2,128]{3,2,1,0:T(2,128)(2,1)}), bf16[64,9,2,128]{3,2,1,0:T(2,128)(2,1)S(1)}, u32[]{:S(2)}, u32[]{:S(2)}) async-start(bf16[64,9,2,128]{3,2,1,0:T(2,128)(2,1)} %state.1), calls=%async_computation | async-start | bytes 589824 | tf_op jit(solution)/shard_map/all_to_all | solution.py:272
  25.1 4.0 %local.1 = (bf16[256,1024]{1,0:T(8,128)(2,1)}, bf16[256,1024]{1,0:T(8,128)(2,1)}) custom-call(bf16[256,1024]{1,0:T(8,128)(2,1)} %refs_0_.3, f32[8,256]{1,0:T(8,128)} %bitcast.9, f32[1,1024]{1,0:T(1,128)} %bitcast.11, bf16[256,1024]{1,0:T(8,128)(2,1)} %refs_3_.3, bf16[256,1024]{1,0:T(8,128)(2,1)} %refs_4_.1), custom_call_target="tpu_custom_call" | custom-call | flops 402653184 | bytes 2633728 | tf_op jit(solution)/shard_map/local/pallas_call | solution.py:222
  29.1 7.4 %all-to-all-done.message = bf16[64,9,2,128]{3,2,1,0:T(2,128)(2,1)S(1)} async-done(((bf16[64,9,2,128]{3,2,1,0:T(2,128)(2,1)}), bf16[64,9,2,128]{3,2,1,0:T(2,128)(2,1)S(1)}, u32[]{:S(2)}, u32[]{:S(2)}) %all-to-all-start) | async-done | bytes 294944 | tf_op jit(solution)/shard_map/all_to_all | solution.py:272
  36.5 0.0 copy-start
  36.5 0.0 copy-start.1
  36.5 0.0 copy-start.2
  36.5 0.0 copy-start.3
  36.5 0.5 scan.1
  36.9 17.0 %all_to_all.10 = bf16[64,16,128]{2,1,0:T(8,128)(2,1)S(1)} all-to-all(bf16[64,16,128]{2,1,0:T(8,128)(2,1)S(1)} %scan.1), channel_id=1, replica_groups=mesh['grp'=2,'sp'=64,'tp'=2] {'sp'}, dimensions={0} | all-to-all | bytes 524288 | tf_op jit(solution)/shard_map/all_to_all | solution.py:294
  53.9 0.0 copy-done
  53.9 0.0 copy-done.1
  53.9 0.0 copy-done.2
  53.9 0.0 copy-done.3
  53.9 1.0 %away.1 = bf16[128,2048]{1,0:T(8,128)(2,1)S(1)} custom-call(bf16[256,1024]{1,0:T(8,128)(2,1)S(1)} %copy-done.1, bf16[256,1024]{1,0:T(8,128)(2,1)S(1)} %copy-done.2, bf16[8,128,128]{2,1,0:T(8,128)(2,1)S(1)} %bitcast.4, f32[1,128]{1,0:T(1,128)S(1)} %bitcast.6, bf16[1024,2048]{1,0:T(8,128)(2,1)S(1)} %copy-done), custom_call_target="tpu_custom_call" | custom-call | flops 536870912 | bytes 6029824 | tf_op jit(solution)/shard_map/away/pallas_call | solution.py:222
  54.9 7.5 %collective-permute-start = (bf16[128,2048]{1,0:T(8,128)(2,1)S(1)}, bf16[128,2048]{1,0:T(8,128)(2,1)S(1)}, u32[]{:S(2)}, u32[]{:S(2)}) collective-permute-start(bf16[128,2048]{1,0:T(8,128)(2,1)S(1)} %away.1), channel_id=1, source_target_pairs={{0,1},{1,0},{2,3},{3,2},{4,5},{5,4},{6,7},{7,6},{8,9},{9,8},{10,11... | collective-permute-start | bytes 1572872 | tf_op jit(solution)/shard_map/ppermute | solution.py:309
  62.4 1.0 %kept.1 = f32[128,2048]{1,0:T(8,128)S(1)} custom-call(bf16[256,1024]{1,0:T(8,128)(2,1)S(1)} %copy-done.1, bf16[256,1024]{1,0:T(8,128)(2,1)S(1)} %copy-done.2, bf16[8,128,128]{2,1,0:T(8,128)(2,1)S(1)} %bitcast.5, f32[1,128]{1,0:T(1,128)S(1)} %bitcast.7, bf16[1024,2048]{1,0:T(8,128)(2,1)S(1)} %copy-done), custom_call_target="tpu_custom_call" | custom-call | flops 536870912 | bytes 6554112 | tf_op jit(solution)/shard_map/kept/pallas_call | solution.py:222
  63.4 0.6 collective-permute-done.received
  64.0 0.8 %final.1 = bf16[128,2048]{1,0:T(8,128)(2,1)} custom-call(f32[128,2048]{1,0:T(8,128)S(1)} %kept.1, bf16[128,2048]{1,0:T(8,128)(2,1)S(1)} %collective-permute-done.received), custom_call_target="tpu_custom_call" | custom-call | flops 262144 | bytes 2097152 | tf_op jit(solution)/shard_map/final/pallas_call | solution.py:222
Async XLA Ops:
  3.2 33.2 %all-to-all-start = ((bf16[64,9,2,128]{3,2,1,0:T(2,128)(2,1)}), bf16[64,9,2,128]{3,2,1,0:T(2,128)(2,1)S(1)}, u32[]{:S(2)}, u32[]{:S(2)}) async-start(bf16[64,9,2,128]{3,2,1,0:T(2,128)(2,1)} %state.1), calls=%async_computation | async-start | bytes 589824 | tf_op jit(solution)/shard_map/all_to_all | solution.py:272
  36.5 17.5 %copy-start = (bf16[1024,2048]{1,0:T(8,128)(2,1)S(1)}, bf16[1024,2048]{1,0:T(8,128)(2,1)}, u32[]{:S(2)}) copy-start(bf16[1024,2048]{1,0:T(8,128)(2,1)} %matrix.3) | copy-start | bytes 12582916
  36.5 17.5 %copy-start.1 = (bf16[256,1024]{1,0:T(8,128)(2,1)S(1)}, bf16[256,1024]{1,0:T(8,128)(2,1)}, u32[]{:S(2)}) copy-start(bf16[256,1024]{1,0:T(8,128)(2,1)} %get-tuple-element.12.inside) | copy-start | bytes 1572868
  36.5 17.5 %copy-start.2 = (bf16[256,1024]{1,0:T(8,128)(2,1)S(1)}, bf16[256,1024]{1,0:T(8,128)(2,1)}, u32[]{:S(2)}) copy-start(bf16[256,1024]{1,0:T(8,128)(2,1)} %get-tuple-element.13.reading) | copy-start | bytes 1572868
  36.5 17.5 %copy-start.3 = (f32[128]{0:T(128)S(1)}, f32[128]{0:T(128)}, u32[]{:S(2)}) copy-start(f32[128]{0:T(128)} %param.12) | copy-start | bytes 1540
  54.9 9.0 %collective-permute-start = (bf16[128,2048]{1,0:T(8,128)(2,1)S(1)}, bf16[128,2048]{1,0:T(8,128)(2,1)S(1)}, u32[]{:S(2)}, u32[]{:S(2)}) collective-permute-start(bf16[128,2048]{1,0:T(8,128)(2,1)S(1)} %away.1), channel_id=1, source_target_pairs={{0,1},{1,0},{2,3},{3,2},{4,5},{5,4},{6,7},{7,6},{8,9},{9,8},{10,11... | collective-permute-start | bytes 1572872 | tf_op jit(solution)/shard_map/ppermute | solution.py:309
